TPU v7x, 128 devices: a whole 4x4x4 slice. The times are simulated.
128 devices in a mesh: ep: 32 (over z, y, core), tp: 4 (over x).
Axes of the slice: x: 4, y: 4, z: 4, core: 2. Of those that a mesh axis runs over, the one named last changes fastest.
Arguments:
- query_rows: bfloat16 [65536, 1024], P('ep', 'tp'), may hold values from -6 to 6
- key_rows: bfloat16 [65536, 1024], P('ep', 'tp'), may hold values from -6 to 6
- value_rows: bfloat16 [65536, 2048], P('ep', 'tp'), may hold values from -6 to 6
- gate_rows: bfloat16 [65536, 2048], P('ep', 'tp'), may hold values from -6 to 6
- log_decay: float32 [8, 65536], P('tp', 'ep'), may hold values from -1 to 0
- out_proj: bfloat16 [2048, 2048], P('tp'), may hold values from -0.125 to 0.125
- moe_input: bfloat16 [16384, 2048], P(('ep', 'tp')), may hold values from -6 to 6
- norm_gain: float32 [2048], replicated, may hold values from 0.1 to 1.9
- routing: int32 [16384, 4], P(('ep', 'tp')), may hold values from 0 to 127, all different within a row; in each aligned block of 128 rows (0 to 127, 128 to 255, ...) at most 8 rows name the same one
- route_weight: float32 [16384, 4], P(('ep', 'tp')), may hold values from 0.2 to 1
- expert_gate: bfloat16 [128, 2048, 512], P(('ep', 'tp')), may hold values from -0.125 to 0.125
- expert_up: bfloat16 [128, 2048, 512], P(('ep', 'tp')), may hold values from -0.125 to 0.125
- expert_down: bfloat16 [128, 512, 2048], P(('ep', 'tp')), may hold values from -0.25 to 0.25
- shared_gate: bfloat16 [2048, 512], replicated, may hold values from -0.125 to 0.125
- shared_up: bfloat16 [2048, 512], replicated, may hold values from -0.125 to 0.125
- shared_down: bfloat16 [512, 2048], replicated, may hold values from -0.25 to 0.25
Outputs:
- mixer_out: bfloat16 [65536, 2048], P(('ep', 'tp'))
- moe_out: bfloat16 [16384, 2048], P(('ep', 'tp'))
Inputs may be any that keep to these rules, and one draw needn't show every extreme that they name: `routing`: within the rows of one device no expert is named more than 8 times.
All inputs are finite; a program needn't handle non-finite values.
Results may differ from a plain program's by a relative error of at most 0.019.
Values may be sent and summed in bfloat16 or wider, within the bound.
No kernel may reach another device: no remote copies, remote signals or barrier semaphores. Data moves between devices by JAX's collectives and lax.ppermute only.
A program may use at most 128 MiB of HBM per device.

v0:
```python
import jax
import jax.numpy as jnp
from jax import lax
from jax.sharding import Mesh
from jax.sharding import PartitionSpec as P

DK = 128
DV = 256
BLOCK = 128
EP = ("ep_0", "ep_1", "ep_2")
EP_TP = ("ep_0", "ep_1", "ep_2", "tp")


EPS = 1e-06


def neutral_like(x, identity):
    return jax.tree.map(
        lambda part, zero: jnp.zeros_like(part) + jnp.asarray(zero, part.dtype), x, identity
    )


def carried_in(x, axes, combine, identity):
    before = start = neutral_like(x, identity)
    subtotal = x
    for axis in reversed(axes):
        peers, place = (lax.axis_size(axis), lax.axis_index(axis))
        pieces = jax.tree.map(
            lambda part, kind: lax.all_gather(part.astype(kind), axis),
            subtotal,
            (jnp.bfloat16, jnp.bfloat16),
        )
        inside, subtotal = (start, start)
        for k in range(peers):
            passed = k < place
            subtotal = combine(
                subtotal, jax.tree.map(lambda part, own: part[k].astype(own.dtype), pieces, x)
            )
            inside = jax.tree.map(lambda new, old: jnp.where(passed, new, old), subtotal, inside)
        before = combine(inside, before)
    return before


def join_states(earlier, later):
    return (earlier[0] * later[0], later[0][:, None, None] * earlier[1] + later[1])


def mixer_half(query_rows, key_rows, value_rows, gate_rows, log_decay, out_proj):
    n_rows = query_rows.shape[0]
    n_heads = query_rows.shape[1] // DK
    n_blocks = n_rows // BLOCK
    score_scale = DK ** (-0.5)
    q_blocks = query_rows.reshape(n_blocks, BLOCK, n_heads, DK)
    k_blocks = key_rows.reshape(n_blocks, BLOCK, n_heads, DK)
    v_blocks = value_rows.reshape(n_blocks, BLOCK, n_heads, DV)
    cum_decay = jnp.cumsum(log_decay.reshape(n_heads, n_blocks, BLOCK), axis=2)
    block_count = cum_decay[:, :, -1]
    causal = jnp.arange(BLOCK)[:, None] >= jnp.arange(BLOCK)[None, :]
    log_gap = jnp.where(causal, cum_decay[:, :, :, None] - cum_decay[:, :, None, :], 0.0)
    decay_mat = jnp.where(causal, jnp.exp(log_gap), 0.0)
    retention_scores = jnp.einsum(
        "bnhd,bmhd->hbnm", q_blocks, k_blocks, preferred_element_type=jnp.float32
    )
    weight = (retention_scores * score_scale * decay_mat).astype(jnp.bfloat16)
    inner_out = jnp.einsum("hbnm,bmhe->bnhe", weight, v_blocks, preferred_element_type=jnp.float32)
    key_scale = (score_scale * jnp.exp(block_count[:, :, None] - cum_decay)).transpose(1, 2, 0)
    decayed_key_rows = (k_blocks.astype(jnp.float32) * key_scale[..., None]).astype(jnp.bfloat16)
    update = jnp.einsum(
        "bmhd,bmhe->bhde", decayed_key_rows, v_blocks, preferred_element_type=jnp.float32
    )

    def advance(carried_state, block_in):
        shrink_by, added = block_in
        return (carried_state * shrink_by[:, None, None] + added, carried_state)

    local_end, local_prev = lax.scan(
        advance, jnp.zeros((n_heads, DK, DV), jnp.float32), (jnp.exp(block_count).T, update)
    )
    device_shrink = jnp.exp(jnp.sum(block_count, axis=1))
    prefix = carried_in(
        (device_shrink, local_end),
        EP,
        join_states,
        (jnp.ones_like(device_shrink), jnp.zeros_like(local_end)),
    )
    incoming = prefix[1]
    block_start = jnp.cumsum(block_count, axis=1) - block_count
    state_prev = local_prev + jnp.exp(block_start).T[:, :, None, None] * incoming[None]
    cross_out = jnp.einsum(
        "bnhd,bhde->bnhe",
        q_blocks,
        state_prev.astype(jnp.bfloat16),
        preferred_element_type=jnp.float32,
    )
    cross_out = cross_out * jnp.exp(cum_decay).transpose(1, 2, 0)[..., None]
    raw_out = (inner_out + cross_out).reshape(n_rows, n_heads, DV)
    avg_out = jnp.mean(raw_out, axis=-1, keepdims=True)
    spread = jnp.mean(jnp.square(raw_out - avg_out), axis=-1, keepdims=True)
    normed = (raw_out - avg_out) * lax.rsqrt(spread + EPS)
    gate_act = jax.nn.silu(gate_rows.astype(jnp.float32).reshape(n_rows, n_heads, DV))
    retained = (gate_act * normed).reshape(n_rows, n_heads * DV).astype(jnp.bfloat16)
    return lax.psum_scatter(
        jnp.dot(retained, out_proj, preferred_element_type=jnp.float32).astype(jnp.bfloat16),
        "tp",
        scatter_dimension=0,
        tiled=True,
    )


def expert_apply(inputs, w_gate, w_up, w_down):
    gate_act = jnp.dot(inputs, w_gate, preferred_element_type=jnp.float32)
    up_act = jnp.dot(inputs, w_up, preferred_element_type=jnp.float32)
    hidden = (jax.nn.silu(gate_act) * up_act).astype(jnp.bfloat16)
    return jnp.dot(hidden, w_down, preferred_element_type=jnp.float32)


def moe_half(
    moe_input,
    norm_gain,
    routing,
    route_weight,
    expert_gate,
    expert_up,
    expert_down,
    shared_gate,
    shared_up,
    shared_down,
):
    as_float = moe_input.astype(jnp.float32)
    moe_normed = (
        as_float
        * lax.rsqrt(jnp.mean(as_float * as_float, axis=-1, keepdims=True) + EPS)
        * norm_gain
    ).astype(jnp.bfloat16)
    n_tokens = routing.shape[0]
    n_visits = routing.shape[1]
    model_width = moe_normed.shape[1]
    experts = lax.axis_size(EP) * lax.axis_size("tp")
    capacity = 2 * n_tokens * n_visits // experts
    flat_route = routing.reshape(-1)
    onehot = (flat_route[:, None] == jnp.arange(experts, dtype=jnp.int32)[None, :]).astype(
        jnp.int32
    )
    slot_rank = jnp.sum(jnp.cumsum(onehot, axis=0) * onehot, axis=1) - 1
    slot_index = flat_route * capacity + slot_rank
    source = jnp.arange(n_tokens * n_visits, dtype=jnp.int32) // n_visits
    outgoing = (
        jnp.zeros((experts * capacity, model_width), jnp.bfloat16)
        .at[slot_index]
        .set(moe_normed[source])
    )
    w_gate = expert_gate[0]
    w_up = expert_up[0]
    w_down = expert_down[0]
    received = lax.all_to_all(
        outgoing.reshape(experts, capacity, model_width),
        EP_TP,
        split_axis=0,
        concat_axis=0,
        tiled=True,
    )
    served = (
        expert_apply(received.reshape(-1, model_width), w_gate, w_up, w_down)
        .astype(jnp.bfloat16)
        .reshape(received.shape)
    )
    returned = lax.all_to_all(served, EP_TP, split_axis=0, concat_axis=0, tiled=True)
    picked = returned.reshape(experts * capacity, model_width)[slot_index].astype(jnp.float32)
    weighted = picked * route_weight.reshape(-1)[:, None]
    routed = jnp.sum(weighted.reshape(n_tokens, n_visits, model_width), axis=1)
    shared = expert_apply(moe_normed, shared_gate, shared_up, shared_down)
    return (routed + shared).astype(jnp.bfloat16)


def local(
    query_rows,
    key_rows,
    value_rows,
    gate_rows,
    log_decay,
    out_proj,
    moe_input,
    norm_gain,
    routing,
    route_weight,
    expert_gate,
    expert_up,
    expert_down,
    shared_gate,
    shared_up,
    shared_down,
):
    mixer_out = mixer_half(query_rows, key_rows, value_rows, gate_rows, log_decay, out_proj)
    moe_out = moe_half(
        moe_input,
        norm_gain,
        routing,
        route_weight,
        expert_gate,
        expert_up,
        expert_down,
        shared_gate,
        shared_up,
        shared_down,
    )
    return (mixer_out, moe_out)


def solution(mesh):
    split = Mesh(mesh.devices.reshape(4, 4, 2, mesh.shape["tp"]), ("ep_0", "ep_1", "ep_2", "tp"))
    return jax.shard_map(
        local,
        mesh=split,
        in_specs=(
            P(EP, "tp"),
            P(EP, "tp"),
            P(EP, "tp"),
            P(EP, "tp"),
            P("tp", EP),
            P("tp", None),
            P(EP_TP, None),
            P(),
            P(EP_TP, None),
            P(EP_TP, None),
            P(EP_TP, None, None),
            P(EP_TP, None, None),
            P(EP_TP, None, None),
            P(),
            P(),
            P(),
        ),
        out_specs=(P(EP_TP, None), P(EP_TP, None)),
        check_vma=False,
    )
```

profile of v0, /device:TPU:1, one launch (start us, length us, event | category | flops | bytes accessed | tf_op | source)
XLA Modules:
  0.0 368.9 jit_solution(16505537645563051957)
XLA Ops:
  8.8 1.2 dynamic-slice
  11.0 3.5 all-reduce
  14.6 8.1 %all-gather.2 = bf16[4,1,2]{2,1,0:T(2,128)(2,1)S(1)} all-gather(bf16[1,1,2]{2,1,0:T(2,128)(2,1)S(1)} %convert_bitcast_fusion.1), channel_id=1, replica_groups=mesh['ep_0'=4,'ep_1'=4,'ep_2'=2,'tp'=4] {'ep_1'}, dimensions={0}, use_global_device_ids=true | all-gather | bytes 20 | tf_op jit(solution)/shard_map/all_gather | solution.py:29
  22.7 9.0 %all-gather.3 = bf16[4,1,2]{2,1,0:T(2,128)(2,1)S(1)} all-gather(bf16[1,1,2]{2,1,0:T(2,128)(2,1)S(1)} %fusion.74), channel_id=1, replica_groups=mesh['ep_0'=4,'ep_1'=4,'ep_2'=2,'tp'=4] {'ep_0'}, dimensions={0}, use_global_device_ids=true | all-gather | bytes 20 | tf_op jit(solution)/shard_map/all_gather | solution.py:29
  32.1 4.0 %reshape.306 = bf16[16,128,2,256]{3,2,1,0:T(2,128)(2,1)} reshape(bf16[2048,512]{1,0:T(8,128)(2,1)} %param.20) | data formatting | bytes 4194304 | tf_op jit(solution)/shard_map/reshape | solution.py:55
  36.2 1.1 reshape.304
  37.3 2.5 copy.58
  39.8 4.6 %fusion.21 = f32[16,2,128,256]{3,2,1,0:T(8,128)} fusion(bf16[16,128,2,256]{3,2,1,0:T(2,128)(2,1)} %reshape.306, bf16[16,128,2,128]{1,3,2,0:T(8,128)(2,1)S(1)} %copy.58, f32[16,128,2]{1,2,0:T(2,128)S(1)} %copy.59), kind=kOutput, calls=%fused_computation.40 | convolution fusion | flops 270008320 | bytes 7356416 | tf_op jit(solution)/shard_map/bmhd,bmhe->bhde/dot_general | solution.py:68
  44.4 28.7 %while.13 = (s32[]{:T(128)}, f32[2,128,256]{2,1,0:T(8,128)S(1)}, f32[16,2,128,256]{3,2,1,0:T(8,128)}, f32[16,2]{1,0:T(8,128)S(1)}, f32[16,2,128,256]{3,2,1,0:T(8,128)}, /*index=5*/s32[]{:T(128)}, s32[]{:T(128)}) while((s32[]{:T(128)}, f32[2,128,256]{2,1,0:T(8,128)S(1)}, f32[16,2,128,256]{3,2,1,0:T(8,128)}, f32[16,2]{1,0:T(8,128)S(1)}, ...), condition=%wide.region_2.3_spmd.clone, body=%wide.region_1.2_spmd.clone.sunk | while | flops 262147 | bytes 1310852 | solution.py:76
  45.1 1.0 bitcast_add_fusion.2
  73.2 6.0 %all-gather.1 = bf16[4,128,256]{2,1,0:T(8,128)(2,1)S(1)} all-gather(bf16[2,128,256]{2,1,0:T(8,128)(2,1)S(1)} %convert_element_type.302), channel_id=3, replica_groups=mesh['ep_0'=4,'ep_1'=4,'ep_2'=2,'tp'=4] {'ep_2'}, dimensions={0}, use_global_device_ids=true | all-gather | bytes 393216 | tf_op jit(solution)/shard_map/all_gather | solution.py:29
  79.4 9.9 %all_gather.31 = bf16[4,2,128,256]{3,2,1,0:T(8,128)(2,1)S(1)} all-gather(bf16[1,2,128,256]{3,2,1,0:T(8,128)(2,1)S(1)} %fusion.62), channel_id=1, replica_groups=mesh['ep_0'=4,'ep_1'=4,'ep_2'=2,'tp'=4] {'ep_1'}, dimensions={0}, use_global_device_ids=true | all-gather | bytes 655360 | tf_op jit(solution)/shard_map/all_gather | solution.py:29
  89.4 11.6 %all_gather.32 = bf16[4,2,128,256]{3,2,1,0:T(8,128)(2,1)S(1)} all-gather(bf16[1,2,128,256]{3,2,1,0:T(8,128)(2,1)S(1)} %fusion.61), channel_id=1, replica_groups=mesh['ep_0'=4,'ep_1'=4,'ep_2'=2,'tp'=4] {'ep_0'}, dimensions={0}, use_global_device_ids=true | all-gather | bytes 655360 | tf_op jit(solution)/shard_map/all_gather | solution.py:29
  101.1 2.1 reshape.303
  103.2 5.5 %fusion.23 = f32[16,2,128,256]{3,2,1,0:T(8,128)} fusion(bf16[16,128,2,256]{3,2,1,0:T(2,128)(2,1)} %reshape.306, bf16[16,128,2,128]{1,3,2,0:T(8,128)(2,1)} %copy-done.3, f32[2,16,128]{2,0,1:T(2,128)S(1)} %copy.55, pred[128,128]{1,0:T(8,128)(4,1)S(1)} %iota_compare_fusion.3, bf16[16,128,2,128]{3,2,1,0:T(2,128)(2,1)} %reshape.303), kind=kOutput, calls=%fused_computation.42 | convolution fusion | flops 405798912 | bytes 8421376 | tf_op jit(solution)/shard_map/hbnm,bmhe->bnhe/dot_general | solution.py:65
  110.0 6.7 %fusion.83 = (f32[16,128,2]{1,2,0:T(2,128)S(1)}, f32[16,128,2,256]{3,1,2,0:T(8,128)}) fusion(f32[16,128,2]{1,2,0:T(2,128)S(1)} %copy.66, f32[16,2,128,256]{3,2,1,0:T(8,128)} %get-tuple-element.30, f32[2,128,256]{2,1,0:T(8,128)S(1)} %fusion.53, f32[16,2]{1,0:T(8,128)S(1)} %copy.62, bf16[16,128,2,128]{3,2,1,0:T(2,128)(2,1)S(1)} %copy-done.4, ...), kind=kOutput, calls=%fused_computation.152 | convolution fusion | flops 274722816 | bytes 13926528 | tf_op jit(solution)/shard_map/bnhd,bhde->bnhe/dot_general | solution.py:89
  116.6 5.5 %copy.67 = f32[16,128,2,256]{1,0,3,2:T(8,128)} copy(f32[16,128,2,256]{3,1,2,0:T(8,128)} %get-tuple-element.94) | data formatting | bytes 8388608 | tf_op jit(solution)/shard_map/add | solution.py:96
  122.1 3.9 %copy.52 = bf16[2048,512]{0,1:T(8,128)(2,1)} copy(bf16[2048,512]{1,0:T(8,128)(2,1)} %param.21) | data formatting | bytes 4194304 | tf_op args[3]
  126.1 3.0 multiply_reduce_fusion.1
  129.5 4.1 %fusion.11 = bf16[2048,512]{0,1:T(8,128)(2,1)S(1)} fusion(f32[64,8,16,128]{3,2,1,0:T(8,128)S(1)} %bitcast.170, bf16[2048,512]{0,1:T(8,128)(2,1)} %copy.52, f32[2048,2]{0,1:T(2,128)S(1)} %rsqrt_bitcast_fusion, f32[2048,2]{0,1:T(2,128)S(1)} %get-tuple-element.79), kind=kLoop, calls=%fused_computation.26 | loop fusion | flops 9437184 | bytes 8421376 | tf_op jit(solution)/shard_map/convert_element_type | solution.py:101
  133.6 7.0 %convolution_convert_fusion = bf16[2048,2048]{1,0:T(8,128)(2,1)} fusion(bf16[2048,512]{0,1:T(8,128)(2,1)S(1)} %fusion.11, bf16[512,2048]{1,0:T(8,128)(2,1)S(1)} %copy-done), kind=kOutput, calls=%fused_computation.7 | convolution fusion | flops 4299161600 | bytes 12582912 | tf_op jit(solution)/shard_map/dot_general | solution.py:103
  143.0 13.0 %scatter_custom_fusion = bf16[1024,2048]{1,0:T(8,128)(2,1)} fusion(s32[512]{0:T(512)S(1)} %bitcast.178, bf16[128,2048]{1,0:T(8,128)(2,1)S(1)} %fusion.36, s32[1024]{0:T(1024)S(1)} %pad_clamp_fusion.1, bf16[]{:T(256)} %constant.87.clone.1), kind=kCustom, calls=%fused_computation.32 | custom fusion | bytes 4194306 | tf_op jit(solution)/shard_map/scatter | solution.py:150
  156.1 110.1 %all_to_all.10 = bf16[128,8,2048]{2,1,0:T(8,128)(2,1)S(1)} all-to-all(bf16[128,8,2048]{2,1,0:T(8,128)(2,1)} %bitcast.171), channel_id=1, replica_groups=mesh['ep_0'=4,'ep_1'=4,'ep_2'=2,'tp'=4] {'ep_0','ep_1','ep_2','tp'}, dimensions={0} | all-to-all | bytes 8388608 | tf_op jit(solution)/shard_map/all_to_all | solution.py:155
  266.2 2.0 copy-done.5
  268.1 3.7 fusion.8
  271.8 10.6 %convert_bitcast_fusion = bf16[128,8,2048]{2,1,0:T(8,128)(2,1)} fusion(bf16[1,512,2048]{2,1,0:T(8,128)(2,1)} %param.30, f32[1024,512]{1,0:T(8,128)} %fusion.8, bf16[1,2048,512]{2,1,0:T(8,128)(2,1)} %param.29, bf16[128,8,2048]{2,1,0:T(8,128)(2,1)} %copy-done.5), kind=kOutput, calls=%fused_computation.23 | convolution fusion | flops 4300210176 | bytes 14680064 | tf_op jit(solution)/shard_map/dot_general | solution.py:114
  282.4 5.5 %all-to-all-start.1 = ((bf16[128,8,2048]{2,1,0:T(8,128)(2,1)}), bf16[128,8,2048]{2,1,0:T(8,128)(2,1)}, u32[]{:S(2)}, u32[]{:S(2)}) async-start(bf16[128,8,2048]{2,1,0:T(8,128)(2,1)} %convert_bitcast_fusion), calls=%async_computation.2 | async-start | bytes 8388608 | tf_op jit(solution)/shard_map/all_to_all | solution.py:167
  288.5 52.3 %all-to-all-done.1 = bf16[128,8,2048]{2,1,0:T(8,128)(2,1)} async-done(((bf16[128,8,2048]{2,1,0:T(8,128)(2,1)}), bf16[128,8,2048]{2,1,0:T(8,128)(2,1)}, u32[]{:S(2)}, u32[]{:S(2)}) %all-to-all-start.1) | async-done | bytes 4194336 | tf_op jit(solution)/shard_map/all_to_all | solution.py:167
  340.9 7.1 %gather_fusion = bf16[512,2048]{1,0:T(8,128)(2,1)S(1)} fusion(bf16[1024,2048]{1,0:T(8,128)(2,1)} %bitcast.38, s32[1024]{0:T(1024)S(1)} %pad_clamp_fusion), kind=kCustom, calls=%fused_computation.1 | custom fusion | bytes 4196352 | tf_op jit(solution)/shard_map/gather | solution.py:168
  348.0 3.1 reshape.322
  351.1 6.5 %multiply_reduce_fusion = f32[128,2048]{1,0:T(8,128)} fusion(f32[128,4,2048]{2,1,0:T(4,128)} %reshape.322, f32[128,4]{1,0:T(8,128)S(1)} %copy.73), kind=kLoop, calls=%fused_computation.22 | loop fusion | flops 1835008 | bytes 5244928 | tf_op jit(solution)/shard_map/reduce_sum | solution.py:170
  357.6 4.1 %fusion.12 = bf16[128,2048]{1,0:T(8,128)(2,1)} fusion(f32[128,2048]{1,0:T(8,128)} %multiply_reduce_fusion, bf16[512,2048]{1,0:T(8,128)(2,1)} %param.33, bf16[128,2048]{1,0:T(8,128)(2,1)S(1)} %fusion.36, bf16[2048,512]{1,0:T(8,128)(2,1)} %param.32, f32[128,512]{1,0:T(8,128)S(1)} %fusion.84), kind=kOutput, calls=%fused_computation.28 | convolution fusion | flops 537788416 | bytes 6553600 | tf_op jit(solution)/shard_map/dot_general | solution.py:114
  (130 shorter events, 34.8 us)
Async XLA Ops:
  7.2 126.5 %copy-start = (bf16[512,2048]{1,0:T(8,128)(2,1)S(1)}, bf16[512,2048]{1,0:T(8,128)(2,1)}, u32[]{:S(2)}) copy-start(bf16[512,2048]{1,0:T(8,128)(2,1)} %param.23) | copy-start | bytes 6291460
  7.2 354.6 %reduce-scatter.2.cloned.1.call-start = ((), (), s32[]{:S(2)}) async-start(), calls=%async_computation.3 | async-start | bytes 10485760 | tf_op jit(solution)/shard_map/reduce_scatter | solution.py:102
  32.1 4.0 %copy-start.8 = (bf16[2048,256]{1,0:T(8,128)(2,1)S(1)}, bf16[2048,256]{1,0:T(8,128)(2,1)}, u32[]{:S(2)}) copy-start(bf16[2048,256]{1,0:T(8,128)(2,1)} %param.19) | copy-start | bytes 3145732
  39.8 4.6 %copy-start.3 = (bf16[16,128,2,128]{1,3,2,0:T(8,128)(2,1)}, bf16[16,128,2,128]{1,3,2,0:T(8,128)(2,1)S(1)}, u32[]{:S(2)}) copy-start(bf16[16,128,2,128]{1,3,2,0:T(8,128)(2,1)S(1)} %copy.58) | copy-start | bytes 3145732
  108.7 1.2 copy-start.4
  126.1 3.5 copy-start.2
  140.6 0.7 copy-start.10
  141.3 1.3 copy-start.7
  141.3 1.5 copy-start.9
  156.1 112.1 %copy-start.12 = (bf16[1,2048,512]{2,1,0:T(8,128)(2,1)S(1)}, bf16[1,2048,512]{2,1,0:T(8,128)(2,1)}, u32[]{:S(2)}) copy-start(bf16[1,2048,512]{2,1,0:T(8,128)(2,1)} %param.28) | copy-start | bytes 6291460
  266.2 2.0 copy-start.5
  282.4 5.5 %copy-start.11 = (f32[128,4]{0,1:T(4,128)S(1)}, f32[128,4]{0,1:T(4,128)}, u32[]{:S(2)}) copy-start(f32[128,4]{0,1:T(4,128)} %param.27) | copy-start | bytes 6148
  282.4 5.6 %copy-start.6 = (bf16[2048,512]{1,0:T(8,128)(2,1)S(1)}, bf16[2048,512]{1,0:T(8,128)(2,1)}, u32[]{:S(2)}) copy-start(bf16[2048,512]{1,0:T(8,128)(2,1)} %param.31) | copy-start | bytes 6291460
  282.4 58.4 %all-to-all-start.1 = ((bf16[128,8,2048]{2,1,0:T(8,128)(2,1)}), bf16[128,8,2048]{2,1,0:T(8,128)(2,1)}, u32[]{:S(2)}, u32[]{:S(2)}) async-start(bf16[128,8,2048]{2,1,0:T(8,128)(2,1)} %convert_bitcast_fusion), calls=%async_computation.2 | async-start | bytes 8388608 | tf_op jit(solution)/shard_map/all_to_all | solution.py:167
  351.1 10.7 %copy-start.1 = (bf16[512,2048]{1,0:T(8,128)(2,1)S(1)}, bf16[512,2048]{1,0:T(8,128)(2,1)}, u32[]{:S(2)}) copy-start(bf16[512,2048]{1,0:T(8,128)(2,1)} %param.23) | copy-start | bytes 6291460
Sparse Core Ops, SparseCore 0:
  140.8 128.4 reduce-scatter.1
where the time goes:
time: 373 us; the launch traced here: 369 us
  blocking collectives  158 us (42%)
  waiting for transfers between devices  52.4 us (14%)
  local copies, waits for them, and re-layouts  49.7 us (13%)
  other arithmetic  45 us (12%)
  matrix products  42.6 us (11%)
  between operations  15.3 us (4%)
  starting transfers between devices  5.53 us (1%)
    all_to_all x1, blocking collectives, moe_half(): lax.all_to_all(outgoing.reshape(experts, capacity, model_width), EP_TP, s...  110 us
    all_to_all x1, waiting for transfers between devices, moe_half(): lax.all_to_all(served, EP_TP, split_axis=0, concat_axis=0, tiled=True)  52.3 us
    all_gather x5, blocking collectives, carried_in(): lax.all_gather(part.astype(kind), axis)  44.5 us
    add x16, other arithmetic, advance(): return (carried_state * shrink_by[:, None, None] + added, carried_state)  16.6 us
    dot_general x2, matrix products, expert_apply(): return jnp.dot(hidden, w_down, preferred_element_type=jnp.float32)  14.7 us
    scatter x1, local copies, waits for them, and re-layouts, moe_half(): outgoing = jnp.zeros((experts * capacity, model_width), jnp.bfloat16).at[...  13 us
    dynamic_update_slice x16, other arithmetic, mixer_half(): lax.scan(advance, jnp.zeros((n_heads, DK, DV), jnp.float32), (jnp.exp(blo...  11.7 us
    unnamed x35, local copies, waits for them, and re-layouts  10.4 us
  transfers between devices with their start and end apart: 2, of which 1 were waited for; matrix products, arithmetic and copies ran while one was open for 14% of the time, Pallas kernels for 0%

commit v1 on v0

v1 whole, which is shorter than its diff:
```python
import functools

import jax
import jax.numpy as jnp
from jax import lax
from jax.experimental import pallas as pl
from jax.experimental.pallas import tpu as pltpu
from jax.sharding import Mesh
from jax.sharding import PartitionSpec as P


DK = 128
DV = 256
BLOCK = 128
CAP = 8
NOTE = 16
EP = ("ep_0", "ep_1", "ep_2")
EP_TP = ("ep_0", "ep_1", "ep_2", "tp")
EPS = 1e-06
SCALE = DK ** (-0.5)
F32 = jnp.float32
BF16 = jnp.bfloat16
HIGHEST = lax.Precision.HIGHEST


def iota(shape, dim):
    return lax.broadcasted_iota(jnp.int32, shape, dim)


def dot(a, b):
    return jnp.dot(a, b, preferred_element_type=F32)


def dot_nt(a, b, precision=None):
    return lax.dot_general(
        a, b, (((1,), (1,)), ((), ())), preferred_element_type=F32, precision=precision
    )


def dot_tn(a, b):
    return lax.dot_general(a, b, (((0,), (0,)), ((), ())), preferred_element_type=F32)


def silu(v):
    return v / (1.0 + jnp.exp(-v))


def block_sums(a, inclusive):
    t, s = iota((BLOCK, BLOCK), 0), iota((BLOCK, BLOCK), 1)
    pick = jnp.where(s <= t if inclusive else s > t, 1.0, 0.0)
    return dot_nt(pick, a, HIGHEST)


def write_message(ref, h, state, total):
    whole = jnp.broadcast_to(total, (NOTE, DV))
    high = whole.astype(BF16).astype(F32)
    middle = (whole - high).astype(BF16).astype(F32)
    row = iota((NOTE, DV), 0)
    note = jnp.where(row == 0, high, jnp.where(row == 1, middle, whole - high - middle))
    ref[h, :DK] = state.astype(BF16)
    ref[h, DK:] = note.astype(BF16)


def read_message(ref, k, h):
    note = ref[k, h, DK:].astype(F32)
    return ref[k, h, :DK].astype(F32), note[0:1] + note[1:2] + note[2:3]


def end_state_body(k_ref, v_ref, a_ref, out_ref, state, total):
    step = pl.program_id(0)

    @pl.when(step == 0)
    def _():
        state[...] = jnp.zeros_like(state)
        total[...] = jnp.zeros_like(total)

    n_heads = a_ref.shape[0]
    for b in range(k_ref.shape[0] // BLOCK):
        rows = pl.ds(b * BLOCK, BLOCK)
        a = a_ref[:, rows]
        left = block_sums(a, False)
        gone = jnp.sum(a, axis=1, keepdims=True)
        for h in range(n_heads):
            k = k_ref[rows, h * DK : (h + 1) * DK].astype(F32)
            v = v_ref[rows, h * DV : (h + 1) * DV]
            k = (k * (SCALE * jnp.exp(left[:, h : h + 1]))).astype(BF16)
            gone_h = gone[h : h + 1, :]
            state[h] = state[h] * jnp.exp(gone_h) + dot_tn(k, v)
            total[h] = total[h] + gone_h

    @pl.when(step == pl.num_programs(0) - 1)
    def _():
        for h in range(n_heads):
            write_message(out_ref, h, state[h], total[h, 0:1, 0:1])


def end_state(key_rows, value_rows, log_decay):
    n_rows, n_heads = key_rows.shape[0], log_decay.shape[0]
    tile = min(512, n_rows)
    return pl.pallas_call(
        end_state_body,
        grid=(n_rows // tile,),
        in_specs=[
            pl.BlockSpec((tile, n_heads * DK), lambda i: (i, 0)),
            pl.BlockSpec((tile, n_heads * DV), lambda i: (i, 0)),
            pl.BlockSpec((n_heads, tile), lambda i: (0, i)),
        ],
        out_specs=pl.BlockSpec((n_heads, DK + NOTE, DV), lambda i: (0, 0, 0)),
        out_shape=jax.ShapeDtypeStruct((n_heads, DK + NOTE, DV), BF16),
        scratch_shapes=[
            pltpu.VMEM((n_heads, DK, DV), F32),
            pltpu.VMEM((n_heads, 8, 128), F32),
        ],
        cost_estimate=pl.CostEstimate(
            flops=2 * n_rows * n_heads * DK * DV, bytes_accessed=4 << 20, transcendentals=0
        ),
        name="end_state",
    )(key_rows, value_rows, log_decay)


def join_body(axis, peers, last, *refs):
    messages, before_ref, refs = refs[:peers], refs[peers], refs[peers + 1 :]
    ordered = refs[-1]
    me = lax.axis_index(axis)
    for d in range(peers):
        ordered[(me - d + peers) % peers] = messages[d][...]
    for h in range(before_ref.shape[0]):
        running, ahead = jnp.zeros((DK, DV), F32), jnp.zeros((DK, DV), F32)
        total, ahead_total = jnp.zeros((1, DV), F32), jnp.zeros((1, DV), F32)
        for k in range(peers):
            ahead = jnp.where(k == me, running, ahead)
            ahead_total = jnp.where(k == me, total, ahead_total)
            if last and k == peers - 1:
                break
            state, gone = read_message(ordered, k, h)
            running = running * jnp.exp(gone) + state
            total = total + gone
        gone = before_ref[h, DK : DK + 1]
        refs[0][h, :DK] = ahead * jnp.exp(gone) + before_ref[h, :DK]
        refs[0][h, DK:] = jnp.broadcast_to(ahead_total + gone, (8, DV))
        if not last:
            write_message(refs[1], h, running, total)


def join(axis, messages, before, last):
    peers = len(messages)
    n_heads = messages[0].shape[0]
    out = [jax.ShapeDtypeStruct((n_heads, DK + 8, DV), F32)]
    if not last:
        out.append(jax.ShapeDtypeStruct(messages[0].shape, BF16))
    return pl.pallas_call(
        functools.partial(join_body, axis, peers, last),
        out_shape=out,
        scratch_shapes=[pltpu.VMEM((peers,) + messages[0].shape, BF16)],
        cost_estimate=pl.CostEstimate(flops=1 << 22, bytes_accessed=2 << 20, transcendentals=0),
        name="join",
    )(*messages, before)


def shift(x, axis, d):
    peers = lax.axis_size(axis)
    return lax.ppermute(x, axis, [(k, (k + d) % peers) for k in range(peers)])


def all_shifts(x, axis):
    return [x] + [shift(x, axis, d) for d in range(1, lax.axis_size(axis))]


def mixer_body(q_ref, k_ref, v_ref, g_ref, a_ref, first_ref, out_ref, state):
    @pl.when(pl.program_id(0) == 0)
    def _():
        state[...] = first_ref[:, :DK]

    n_heads = a_ref.shape[0]
    t, m = iota((BLOCK, BLOCK), 0), iota((BLOCK, BLOCK), 1)
    causal = t >= m
    upto = jnp.where(t <= m, 1.0, 0.0)
    for b in range(q_ref.shape[0] // BLOCK):
        rows = pl.ds(b * BLOCK, BLOCK)
        a = a_ref[:, rows]
        down = block_sums(a, True)
        across = jnp.dot(a, upto, preferred_element_type=F32, precision=HIGHEST)
        for h in range(n_heads):
            q = q_ref[rows, h * DK : (h + 1) * DK]
            k = k_ref[rows, h * DK : (h + 1) * DK]
            v = v_ref[rows, h * DV : (h + 1) * DV]
            gate = g_ref[rows, h * DV : (h + 1) * DV].astype(F32)
            col, row = down[:, h : h + 1], across[h : h + 1, :]
            whole = row[:, BLOCK - 1 : BLOCK]
            decay = jnp.where(causal, jnp.exp(jnp.where(causal, col - row, 0.0)), 0.0)
            weight = (dot_nt(q, k) * SCALE * decay).astype(BF16)
            before = state[h]
            raw = dot(weight, v) + dot(q, before.astype(BF16)) * jnp.exp(col)
            faded = (k.astype(F32) * (SCALE * jnp.exp(whole - col))).astype(BF16)
            state[h] = before * jnp.exp(whole) + dot_tn(faded, v)
            centered = raw - jnp.mean(raw, axis=1, keepdims=True)
            spread = jnp.mean(centered * centered, axis=1, keepdims=True)
            normed = centered * lax.rsqrt(spread + EPS)
            out_ref[rows, h * DV : (h + 1) * DV] = (silu(gate) * normed).astype(BF16)


def mixer(query_rows, key_rows, value_rows, gate_rows, log_decay, incoming):
    n_rows, n_heads = query_rows.shape[0], log_decay.shape[0]
    tile = min(256, n_rows)
    return pl.pallas_call(
        mixer_body,
        grid=(n_rows // tile,),
        in_specs=[
            pl.BlockSpec((tile, n_heads * DK), lambda i: (i, 0)),
            pl.BlockSpec((tile, n_heads * DK), lambda i: (i, 0)),
            pl.BlockSpec((tile, n_heads * DV), lambda i: (i, 0)),
            pl.BlockSpec((tile, n_heads * DV), lambda i: (i, 0)),
            pl.BlockSpec((n_heads, tile), lambda i: (0, i)),
            pl.BlockSpec((n_heads, DK + 8, DV), lambda i: (0, 0, 0)),
        ],
        out_specs=pl.BlockSpec((tile, n_heads * DV), lambda i: (i, 0)),
        out_shape=jax.ShapeDtypeStruct((n_rows, n_heads * DV), BF16),
        scratch_shapes=[pltpu.VMEM((n_heads, DK, DV), F32)],
        cost_estimate=pl.CostEstimate(
            flops=12 * n_rows * n_heads * DK * DV, bytes_accessed=8 << 20, transcendentals=0
        ),
        name="mixer",
    )(query_rows, key_rows, value_rows, gate_rows, log_decay, incoming)


def project_body(*refs):
    heads, weights, out_ref, lhs, rhs, sems = refs[:4], refs[4:20], *refs[20:]
    x, core = lax.axis_index("tp"), lax.axis_index("ep_2")
    up, out_of = lax.axis_index("ep_1"), lax.axis_index("ep_0")
    copies = [pltpu.make_async_copy(heads[0].at[x], lhs.at[0], sems.at[16])]
    for d in range(1, 4):
        copies.append(pltpu.make_async_copy(heads[d], lhs.at[d], sems.at[16 + d]))
    for part in range(4):
        me = up if part % 2 == 0 else out_of
        for d in range(4):
            n = part * 4 + d
            to = rhs.at[part, :, (me - d + 4) % 4]
            copies.append(pltpu.make_async_copy(weights[n], to, sems.at[n]))
    for copy in copies:
        copy.start()
    for copy in copies[:4]:
        copy.wait()
    _, width = lhs.shape[1:]
    fine = rhs.shape[-1]
    for part in range(4):
        for d in range(4):
            copies[4 + part * 4 + d].wait()
        total = dot(lhs[0], rhs[part, 0].reshape(width, fine))
        for d in range(1, 4):
            total = total + dot(lhs[d], rhs[part, d].reshape(width, fine))
        whose = core if part < 2 else 1 - core
        at = pl.multiple_of((part % 2) * 2 * fine + whose * fine, fine)
        out_ref[:, pl.ds(at, fine)] = total.astype(BF16)


def project(retained, received, own, other):
    groups, n_rows, width = retained.shape
    fine = own[0].shape[-1]
    arrays = [retained, *received, *own, *other]
    return pl.pallas_call(
        project_body,
        in_specs=[pl.BlockSpec(memory_space=pl.ANY)] * len(arrays),
        out_shape=jax.ShapeDtypeStruct((n_rows, 4 * fine), BF16),
        scratch_shapes=[
            pltpu.VMEM((groups, n_rows, width), BF16),
            pltpu.VMEM((4, groups, 4) + own[0].shape[1:], BF16),
            pltpu.SemaphoreType.DMA((20,)),
        ],
        cost_estimate=pl.CostEstimate(
            flops=8 * n_rows * groups * width * fine, bytes_accessed=12 << 20, transcendentals=0
        ),
        name="project",
    )(*arrays)


def gather_projection(out_proj):
    n_rows, width = out_proj.shape
    core = lax.axis_index("ep_2")
    rows, cols = n_rows // 4, width // 4
    left = lax.dynamic_slice(
        out_proj, (lax.axis_index("ep_1") * rows, core * cols), (rows, cols)
    )
    right = lax.dynamic_slice(
        out_proj, (lax.axis_index("ep_0") * rows, (2 + core) * cols), (rows, cols)
    )
    over_x = all_shifts(jnp.stack([left, right]), "tp")
    own = all_shifts(jnp.stack([part[0] for part in over_x]), "ep_1")
    own = own + all_shifts(jnp.stack([part[1] for part in over_x]), "ep_0")
    other = [shift(part, "ep_2", 1) for part in own]
    return own, other


def dispatch_body(x_ref, gain_ref, route_ref, weight_ref, normed_ref, out_ref, high_ref, low_ref):
    x = x_ref[...].astype(F32)
    mean = jnp.mean(x * x, axis=1, keepdims=True)
    normed = (x * lax.rsqrt(mean + EPS) * gain_ref[...]).astype(BF16)
    normed_ref[...] = normed
    n_tokens, n_visits = route_ref.shape
    n_slots = out_ref.shape[0]
    experts = n_slots // CAP
    route, weight = route_ref[...], weight_ref[...]
    lane = iota((n_tokens, experts), 1)
    named = jnp.zeros((n_tokens, experts), F32)
    weighed = jnp.zeros((n_tokens, experts), F32)
    for k in range(n_visits):
        hit = route[:, k : k + 1] == lane
        named = jnp.where(hit, 1.0, named)
        weighed = jnp.where(hit, weight[:, k : k + 1], weighed)
    earlier = iota((n_tokens, n_tokens), 0) > iota((n_tokens, n_tokens), 1)
    rank = dot(jnp.where(earlier, 1.0, 0.0).astype(BF16), named.astype(BF16))
    rank = jnp.where(named > 0.0, rank, float(CAP))
    spread = jnp.where(iota((experts, n_slots), 1) // CAP == iota((experts, n_slots), 0), 1.0, 0.0)
    spread = spread.astype(BF16)
    place = (iota((n_tokens, n_slots), 1) % CAP).astype(F32)
    here = dot(rank.astype(BF16), spread) == place
    high = weighed.astype(BF16)
    low = (weighed - high.astype(F32)).astype(BF16)
    high_ref[...] = jnp.where(here, dot(high, spread), 0.0).astype(BF16)
    low_ref[...] = jnp.where(here, dot(low, spread), 0.0).astype(BF16)
    pick = jnp.where(here, 1.0, 0.0).astype(BF16)
    out_ref[...] = dot_tn(pick, normed).astype(BF16)


def dispatch(moe_input, norm_gain, routing, route_weight, experts):
    n_tokens, width = moe_input.shape
    n_slots = experts * CAP
    return pl.pallas_call(
        dispatch_body,
        out_shape=(
            jax.ShapeDtypeStruct((n_tokens, width), BF16),
            jax.ShapeDtypeStruct((n_slots, width), BF16),
            jax.ShapeDtypeStruct((n_tokens, n_slots), BF16),
            jax.ShapeDtypeStruct((n_tokens, n_slots), BF16),
        ),
        cost_estimate=pl.CostEstimate(
            flops=2 * n_tokens * n_slots * width, bytes_accessed=6 << 20, transcendentals=0
        ),
        name="dispatch",
    )(moe_input, norm_gain.reshape(1, width), routing, route_weight)


def expert_body(x_ref, gate_ref, up_ref, down_ref, out_ref):
    x = x_ref[...]
    hidden = (silu(dot(x, gate_ref[...])) * dot(x, up_ref[...])).astype(BF16)
    out_ref[...] = dot(hidden, down_ref[...]).astype(out_ref.dtype)


def expert_apply(rows, w_gate, w_up, w_down, dtype):
    n_rows, width = rows.shape
    hidden = w_gate.shape[1]
    tile = min(256, n_rows)
    return pl.pallas_call(
        expert_body,
        grid=(n_rows // tile,),
        in_specs=[
            pl.BlockSpec((tile, width), lambda i: (i, 0)),
            pl.BlockSpec((width, hidden), lambda i: (0, 0)),
            pl.BlockSpec((width, hidden), lambda i: (0, 0)),
            pl.BlockSpec((hidden, width), lambda i: (0, 0)),
        ],
        out_specs=pl.BlockSpec((tile, width), lambda i: (i, 0)),
        out_shape=jax.ShapeDtypeStruct((n_rows, width), dtype),
        cost_estimate=pl.CostEstimate(
            flops=6 * n_rows * width * hidden, bytes_accessed=14 << 20, transcendentals=0
        ),
        name="expert",
    )(rows, w_gate, w_up, w_down)


def combine_body(high_ref, low_ref, rows_ref, shared_ref, out_ref):
    rows = rows_ref[...]
    total = dot(high_ref[...], rows) + dot(low_ref[...], rows) + shared_ref[...]
    out_ref[...] = total.astype(BF16)


def combine(high, low, rows, shared):
    n_tokens, n_slots = high.shape
    width = rows.shape[1]
    tile = width // 4
    return pl.pallas_call(
        combine_body,
        grid=(width // tile,),
        in_specs=[
            pl.BlockSpec((n_tokens, n_slots), lambda i: (0, 0)),
            pl.BlockSpec((n_tokens, n_slots), lambda i: (0, 0)),
            pl.BlockSpec((n_slots, tile), lambda i: (0, i)),
            pl.BlockSpec((n_tokens, tile), lambda i: (0, i)),
        ],
        out_specs=pl.BlockSpec((n_tokens, tile), lambda i: (0, i)),
        out_shape=jax.ShapeDtypeStruct((n_tokens, width), BF16),
        cost_estimate=pl.CostEstimate(
            flops=4 * n_tokens * n_slots * width, bytes_accessed=6 << 20, transcendentals=0
        ),
        name="combine",
    )(high, low, rows, shared)


def exchange(x, axes):
    return lax.all_to_all(x, axes, split_axis=0, concat_axis=0, tiled=True)


def local(
    query_rows,
    key_rows,
    value_rows,
    gate_rows,
    log_decay,
    out_proj,
    moe_input,
    norm_gain,
    routing,
    route_weight,
    expert_gate,
    expert_up,
    expert_down,
    shared_gate,
    shared_up,
    shared_down,
):
    n_rows = query_rows.shape[0]
    width = moe_input.shape[1]
    tp = lax.axis_size("tp")
    experts = lax.axis_size(EP) * tp

    normed, outgoing, high, low = dispatch(moe_input, norm_gain, routing, route_weight, experts)
    received = exchange(outgoing.reshape(experts, CAP, width), EP_TP)

    message = end_state(key_rows, value_rows, log_decay)
    before = jnp.zeros((message.shape[0], DK + 8, DV), F32)
    for axis in reversed(EP):
        messages = all_shifts(message, axis)
        before, *message = join(axis, messages, before, axis == EP[0])
        message = message[0] if message else None

    own, other = gather_projection(out_proj)

    shared = expert_apply(normed, shared_gate, shared_up, shared_down, F32)
    retained = mixer(query_rows, key_rows, value_rows, gate_rows, log_decay, before)
    retained = retained.reshape(tp, n_rows // tp, -1)
    place = lax.axis_index("tp")
    heads = []
    for d in range(1, tp):
        block = lax.dynamic_index_in_dim(retained, (place + d) % tp, keepdims=False)
        heads.append(shift(block, "tp", d))

    served = expert_apply(
        received.reshape(-1, width), expert_gate[0], expert_up[0], expert_down[0], BF16
    )
    returned = exchange(served.reshape(experts, CAP, width), EP_TP)

    mixer_out = project(retained, heads, own, other)
    moe_out = combine(high, low, returned.reshape(-1, width), shared)
    return (mixer_out, moe_out)


def solution(mesh):
    split = Mesh(mesh.devices.reshape(4, 4, 2, mesh.shape["tp"]), ("ep_0", "ep_1", "ep_2", "tp"))
    return jax.shard_map(
        local,
        mesh=split,
        in_specs=(
            P(EP, "tp"),
            P(EP, "tp"),
            P(EP, "tp"),
            P(EP, "tp"),
            P("tp", EP),
            P("tp", None),
            P(EP_TP, None),
            P(),
            P(EP_TP, None),
            P(EP_TP, None),
            P(EP_TP, None, None),
            P(EP_TP, None, None),
            P(EP_TP, None, None),
            P(),
            P(),
            P(),
        ),
        out_specs=(P(EP_TP, None), P(EP_TP, None)),
        check_vma=False,
    )
```

time: 373 us -> 268 us (0.72)
  blocking collectives: 158 us -> 64.9 us
  Pallas kernels: 0 us -> 64.6 us
  other arithmetic: 45 us -> 0.17 us
  starting transfers between devices: 5.53 us -> 49.5 us
  matrix products: 42.6 us -> 0 us
  local copies, waits for them, and re-layouts: 49.7 us -> 8.61 us
  waiting for transfers between devices: 52.4 us -> 78.5 us
  between operations: 15.3 us -> 0.85 us
    ppermute x0 -> x27, waiting for transfers between devices: none -> 78.5 us  [shift(): return lax.ppermute(x, axis, [(k, (k + d) % peers) for k in range(peers)])]
    pallas_call x0 -> x10, Pallas kernels: none -> 64.6 us  [the longest x2 16.9 us: expert_apply(): pl.pallas_call(expert_body, grid=(n_rows // tile,), in_specs=[pl.BlockSpe...]
    all_to_all x1, waiting for transfers between devices: 52.3 us -> 0.01 us  [exchange(): return lax.all_to_all(x, axes, split_axis=0, concat_axis=0, tiled=True)]
    all_to_all x1, blocking collectives: 110 us -> 64.9 us  [exchange(): return lax.all_to_all(x, axes, split_axis=0, concat_axis=0, tiled=True)]
    all_gather x5 -> x0, blocking collectives: 44.5 us -> none  [carried_in(): lax.all_gather(part.astype(kind), axis)]
    ppermute x0 -> x27, starting transfers between devices: none -> 44.4 us  [shift(): return lax.ppermute(x, axis, [(k, (k + d) % peers) for k in range(peers)])]
    dot_general x8 -> x0, matrix products: 42.6 us -> none  [the longest x2 14.7 us: expert_apply(): return jnp.dot(hidden, w_down, preferred_element_type=jnp.float32)]
    add x16 -> x0, other arithmetic: 16.6 us -> none  [advance(): return (carried_state * shrink_by[:, None, None] + added, carried_state)]
  transfers between devices with their start and end apart: 2 -> 28, of which waited for: 1 -> 9; matrix products, arithmetic and copies ran while one was open for 14% -> 1% of each run, Pallas kernels for 0% -> 16%
where the time goes in v1:
time: 268 us; the launch traced here: 267 us
  waiting for transfers between devices  78.5 us (29%)
  blocking collectives  64.9 us (24%)
  Pallas kernels  64.6 us (24%)
  starting transfers between devices  49.5 us (18%)
  local copies, waits for them, and re-layouts  8.61 us (3%)
    ppermute x27, waiting for transfers between devices, shift(): return lax.ppermute(x, axis, [(k, (k + d) % peers) for k in range(peers)])  78.5 us
    all_to_all x1, blocking collectives, exchange(): return lax.all_to_all(x, axes, split_axis=0, concat_axis=0, tiled=True)  64.9 us
    ppermute x27, starting transfers between devices, shift(): return lax.ppermute(x, axis, [(k, (k + d) % peers) for k in range(peers)])  44.4 us
    pallas_call x2, Pallas kernels, expert_apply(): pl.pallas_call(expert_body, grid=(n_rows // tile,), in_specs=[pl.BlockSpe...  16.9 us
    pallas_call x1, Pallas kernels, mixer(): pl.pallas_call(mixer_body, grid=(n_rows // tile,), in_specs=[pl.BlockSpec...  13.9 us
    pallas_call x1, Pallas kernels, end_state(): pl.pallas_call(end_state_body, grid=(n_rows // tile,), in_specs=[pl.Block...  8.76 us
    pallas_call x1, Pallas kernels, project(): pl.pallas_call(project_body, in_specs=[pl.BlockSpec(memory_space=pl.ANY)]...  8.64 us
    pallas_call x3, Pallas kernels, join(): pl.pallas_call(functools.partial(join_body, axis, peers, last), out_shape...  6.42 us
  transfers between devices with their start and end apart: 28, of which 9 were waited for; matrix products, arithmetic and copies ran while one was open for 1% of the time, Pallas kernels for 16%

profile of v1, /device:TPU:1, one launch (start us, length us, event | category | flops | bytes accessed | tf_op | source)
XLA Modules:
  0.0 267.1 jit_solution(14404523109033910308)
XLA Ops:
  0.6 1.4 copy.18.route_ref
  3.5 4.9 %dispatch.1 = (bf16[128,2048]{1,0:T(8,128)(2,1)}, bf16[1024,2048]{1,0:T(8,128)(2,1)}, bf16[128,1024]{1,0:T(8,128)(2,1)}, bf16[128,1024]{1,0:T(8,128)(2,1)}) custom-call(bf16[128,2048]{1,0:T(8,128)(2,1)} %x_ref.1, f32[1,2048]{1,0:T(1,128)} %bitcast.27, s32[128,4]{1,0:T(8,128)} %copy.18.route_ref, f32[128,4]{1,0:T(8,128)} %copy.19.weight_ref), custom_call_target="tpu_custom_call" | custom-call | flops 536870912 | bytes 6291456 | tf_op jit(solution)/shard_map/dispatch/pallas_call | solution.py:327
  8.4 64.9 %all_to_all.10 = bf16[128,8,2048]{2,1,0:T(8,128)(2,1)} all-to-all(bf16[128,8,2048]{2,1,0:T(8,128)(2,1)} %bitcast.22), channel_id=1, replica_groups=mesh['ep_0'=4,'ep_1'=4,'ep_2'=2,'tp'=4] {'ep_0','ep_1','ep_2','tp'}, dimensions={0} | all-to-all | bytes 8388608 | tf_op jit(solution)/shard_map/all_to_all | solution.py:399
  73.3 11.8 %expert.2 = bf16[1024,2048]{1,0:T(8,128)(2,1)} custom-call(bf16[1024,2048]{1,0:T(8,128)(2,1)} %bitcast.23, bf16[2048,512]{1,0:T(8,128)(2,1)} %bitcast.24, bf16[2048,512]{1,0:T(8,128)(2,1)} %bitcast.25, bf16[512,2048]{1,0:T(8,128)(2,1)} %bitcast.26), custom_call_target="tpu_custom_call" | custom-call | flops 6442450944 | bytes 14680064 | tf_op jit(solution)/shard_map/expert/pallas_call | solution.py:352
  85.1 5.0 %all-to-all-start.1 = ((bf16[128,8,2048]{2,1,0:T(8,128)(2,1)}), bf16[128,8,2048]{2,1,0:T(8,128)(2,1)}, u32[]{:S(2)}, u32[]{:S(2)}) async-start(bf16[128,8,2048]{2,1,0:T(8,128)(2,1)} %bitcast.21), calls=%async_computation.1 | async-start | bytes 8388608 | tf_op jit(solution)/shard_map/all_to_all | solution.py:399
  91.2 1.4 collective-permute-start.10
  92.7 2.4 collective-permute-start.11
  96.3 46.8 %collective-permute-done.10 = bf16[2,128,512]{2,1,0:T(8,128)(2,1)S(1)} collective-permute-done((bf16[2,128,512]{2,1,0:T(8,128)(2,1)S(1)}, bf16[2,128,512]{2,1,0:T(8,128)(2,1)S(1)}, u32[]{:S(2)}, u32[]{:S(2)}) %collective-permute-start.10) | collective-permute-done | bytes 262176 | tf_op jit(solution)/shard_map/ppermute | solution.py:162
  143.0 5.8 %collective-permute-done.11 = bf16[2,128,512]{2,1,0:T(8,128)(2,1)S(1)} collective-permute-done((bf16[2,128,512]{2,1,0:T(8,128)(2,1)S(1)}, bf16[2,128,512]{2,1,0:T(8,128)(2,1)S(1)}, u32[]{:S(2)}, u32[]{:S(2)}) %collective-permute-start.11) | collective-permute-done | bytes 262176 | tf_op jit(solution)/shard_map/ppermute | solution.py:162
  150.3 2.5 collective-permute-start.14
  152.8 8.8 %end_state.1.refs_0_ = bf16[2,144,256]{2,1,0:T(8,128)(2,1)} custom-call(bf16[2048,256]{1,0:T(8,128)(2,1)} %k_ref.3, bf16[2048,512]{1,0:T(8,128)(2,1)} %v_ref.3, f32[2,2048]{1,0:T(2,128)} %a_ref.3), custom_call_target="tpu_custom_call" | custom-call | flops 268435456 | bytes 4194304 | tf_op jit(solution)/shard_map/end_state/pallas_call | solution.py:100
  161.6 1.5 collective-permute-start
  165.1 2.0 join.3
  167.1 2.5 collective-permute-start.2
  169.8 11.1 %collective-permute-done.1.refs_1_ = bf16[2,144,256]{2,1,0:T(8,128)(2,1)S(1)} collective-permute-done((bf16[2,144,256]{2,1,0:T(8,128)(2,1)}, bf16[2,144,256]{2,1,0:T(8,128)(2,1)S(1)}, u32[]{:S(2)}, u32[]{:S(2)}) %collective-permute-start.1) | collective-permute-done | bytes 147488 | tf_op jit(solution)/shard_map/ppermute | solution.py:162
  182.2 2.2 join.4
  184.4 1.5 collective-permute-start.4
  185.9 2.9 %collective-permute-start.5 = (bf16[2,144,256]{2,1,0:T(8,128)(2,1)}, bf16[2,144,256]{2,1,0:T(8,128)(2,1)S(1)}, u32[]{:S(2)}, u32[]{:S(2)}) collective-permute-start(bf16[2,144,256]{2,1,0:T(8,128)(2,1)} %get-tuple-element.12.refs_0_), channel_id=1, source_target_pairs={{0,64},{32,96},{64,0},{96,32},{1,65},{33,97},{65,1},{97,33},{2,66}... | collective-permute-start | bytes 442376 | tf_op jit(solution)/shard_map/ppermute | solution.py:162
  190.3 3.6 %collective-permute-done.5.refs_2_ = bf16[2,144,256]{2,1,0:T(8,128)(2,1)S(1)} collective-permute-done((bf16[2,144,256]{2,1,0:T(8,128)(2,1)}, bf16[2,144,256]{2,1,0:T(8,128)(2,1)S(1)}, u32[]{:S(2)}, u32[]{:S(2)}) %collective-permute-start.5) | collective-permute-done | bytes 147488 | tf_op jit(solution)/shard_map/ppermute | solution.py:162
  194.4 1.8 collective-permute-start.17
  196.2 1.6 collective-permute-start.18
  197.8 3.4 %collective-permute-start.19 = (bf16[4,128,512]{2,1,0:T(8,128)(2,1)S(1)}, bf16[4,128,512]{2,1,0:T(8,128)(2,1)}, u32[]{:S(2)}, u32[]{:S(2)}) collective-permute-start(bf16[4,128,512]{2,1,0:T(8,128)(2,1)S(1)} %pad_maximum_fusion.refs_4_), channel_id=1, source_target_pairs={{0,4},{4,0},{1,5},{5,1},{2,6},{6,2},{3,7},{7,3},{8,12},{12,8},{9,1... | collective-permute-start | bytes 1572872 | tf_op jit(solution)/shard_map/ppermute | solution.py:162
  201.2 2.2 join.5.first_ref
  203.4 13.9 %mixer.1 = bf16[2048,512]{1,0:T(8,128)(2,1)} custom-call(bf16[2048,256]{1,0:T(8,128)(2,1)} %q_ref.1, bf16[2048,256]{1,0:T(8,128)(2,1)} %k_ref.3, bf16[2048,512]{1,0:T(8,128)(2,1)} %v_ref.3, bf16[2048,512]{1,0:T(8,128)(2,1)} %g_ref.1, f32[2,2048]{1,0:T(2,128)} %a_ref.3, f32[2,136,256]{2,1,0:T(8,128)} %join.5.first_ref), custom_call_target="tpu_custom_call" | custom-call | flops 1610612736 | bytes 8388608 | tf_op jit(solution)/shard_map/mixer/pallas_call | solution.py:205
  217.3 1.5 dynamic-slice_bitcast_fusion
  220.1 1.8 collective-permute-start.9
  221.9 2.8 %collective-permute-start.20 = (bf16[4,128,512]{2,1,0:T(8,128)(2,1)S(1)}, bf16[4,128,512]{2,1,0:T(8,128)(2,1)S(1)}, u32[]{:S(2)}, u32[]{:S(2)}) collective-permute-start(bf16[4,128,512]{2,1,0:T(8,128)(2,1)S(1)} %collective-permute-done.13.refs_5_), channel_id=1, source_target_pairs={{0,4},{4,0},{1,5},{5,1},{2,6},{6,2},{3,7},{7,3},{8,12},{12,8},{9,1... | collective-permute-start | bytes 1572872 | tf_op jit(solution)/shard_map/ppermute | solution.py:162
  224.8 8.5 %collective-permute-done.7.refs_1_ = bf16[512,512]{1,0:T(8,128)(2,1)S(1)} collective-permute-done((bf16[512,512]{1,0:T(8,128)(2,1)S(1)}, bf16[512,512]{1,0:T(8,128)(2,1)S(1)}, u32[]{:S(2)}, u32[]{:S(2)}) %collective-permute-start.7) | collective-permute-done | bytes 524320 | tf_op jit(solution)/shard_map/ppermute | solution.py:162
  233.3 12.4 %collective-permute-start.22 = (bf16[4,128,512]{2,1,0:T(8,128)(2,1)}, bf16[4,128,512]{2,1,0:T(8,128)(2,1)}, u32[]{:S(2)}, u32[]{:S(2)}) collective-permute-start(bf16[4,128,512]{2,1,0:T(8,128)(2,1)} %collective-permute-done.15.refs_7_), channel_id=1, source_target_pairs={{0,4},{4,0},{1,5},{5,1},{2,6},{6,2},{3,7},{7,3},{8,12},{12,8},{9,1... | collective-permute-start | bytes 1572872 | tf_op jit(solution)/shard_map/ppermute | solution.py:162
  246.7 5.1 %expert.3.shared_ref = f32[128,2048]{1,0:T(8,128)} custom-call(bf16[128,2048]{1,0:T(8,128)(2,1)} %get-tuple-element.17.x_ref, bf16[2048,512]{1,0:T(8,128)(2,1)} %gate_ref.1, bf16[2048,512]{1,0:T(8,128)(2,1)} %up_ref.1, bf16[512,2048]{1,0:T(8,128)(2,1)} %down_ref.1), custom_call_target="tpu_custom_call" | custom-call | flops 805306368 | bytes 14680064 | tf_op jit(solution)/shard_map/expert/pallas_call | solution.py:352
  253.4 8.6 %project.1 = bf16[512,2048]{1,0:T(8,128)(2,1)} custom-call(bf16[4,512,512]{2,1,0:T(8,128)(2,1)} %bitcast.20, bf16[512,512]{1,0:T(8,128)(2,1)} %copy-done.12, bf16[512,512]{1,0:T(8,128)(2,1)} %copy-done.13, bf16[512,512]{1,0:T(8,128)(2,1)} %copy-done.14, bf16[4,128,512]{2,1,0:T(8,128)(2,1)} %copy-done, bf16[4,128,512]{2,1,0:T(8,128)(2,1)} %copy-done.9, ...), custom_call_target="tpu_custom_call" | custom-call | flops 4294967296 | bytes 12582912 | tf_op jit(solution)/shard_map/project/pallas_call | solution.py:260
  262.1 5.0 %combine.1 = bf16[128,2048]{1,0:T(8,128)(2,1)} custom-call(bf16[128,1024]{1,0:T(8,128)(2,1)} %get-tuple-element.14.high_ref, bf16[128,1024]{1,0:T(8,128)(2,1)} %get-tuple-element.15.low_ref, bf16[1024,2048]{1,0:T(8,128)(2,1)} %bitcast.13.rows_ref, f32[128,2048]{1,0:T(8,128)} %expert.3.shared_ref), custom_call_target="tpu_custom_call" | custom-call | flops 1073741824 | bytes 6291456 | tf_op jit(solution)/shard_map/combine/pallas_call | solution.py:380
  (82 shorter events, 14.4 us)
Async XLA Ops:
  85.1 177.0 %all-to-all-start.1 = ((bf16[128,8,2048]{2,1,0:T(8,128)(2,1)}), bf16[128,8,2048]{2,1,0:T(8,128)(2,1)}, u32[]{:S(2)}, u32[]{:S(2)}) async-start(bf16[128,8,2048]{2,1,0:T(8,128)(2,1)} %bitcast.21), calls=%async_computation.1 | async-start | bytes 8388608 | tf_op jit(solution)/shard_map/all_to_all | solution.py:399
  91.2 51.8 %collective-permute-start.10 = (bf16[2,128,512]{2,1,0:T(8,128)(2,1)S(1)}, bf16[2,128,512]{2,1,0:T(8,128)(2,1)S(1)}, u32[]{:S(2)}, u32[]{:S(2)}) collective-permute-start(bf16[2,128,512]{2,1,0:T(8,128)(2,1)S(1)} %pad_maximum_fusion.2), channel_id=1, source_target_pairs={{0,1},{1,2},{2,3},{3,0},{4,5},{5,6},{6,7},{7,4},{8,9},{9,10},{10,1... | collective-permute-start | bytes 786440 | tf_op jit(solution)/shard_map/ppermute | solution.py:162
  92.7 56.1 %collective-permute-start.11 = (bf16[2,128,512]{2,1,0:T(8,128)(2,1)S(1)}, bf16[2,128,512]{2,1,0:T(8,128)(2,1)S(1)}, u32[]{:S(2)}, u32[]{:S(2)}) collective-permute-start(bf16[2,128,512]{2,1,0:T(8,128)(2,1)S(1)} %pad_maximum_fusion.2), channel_id=1, source_target_pairs={{0,2},{1,3},{2,0},{3,1},{4,6},{5,7},{6,4},{7,5},{8,10},{9,11},{10,... | collective-permute-start | bytes 786440 | tf_op jit(solution)/shard_map/ppermute | solution.py:162
  95.1 53.7 %collective-permute-start.12 = (bf16[2,128,512]{2,1,0:T(8,128)(2,1)S(1)}, bf16[2,128,512]{2,1,0:T(8,128)(2,1)S(1)}, u32[]{:S(2)}, u32[]{:S(2)}) collective-permute-start(bf16[2,128,512]{2,1,0:T(8,128)(2,1)S(1)} %pad_maximum_fusion.2), channel_id=1, source_target_pairs={{0,3},{1,0},{2,1},{3,2},{4,7},{5,4},{6,5},{7,6},{8,11},{9,8},{10,9... | collective-permute-start | bytes 786440 | tf_op jit(solution)/shard_map/ppermute | solution.py:162
  148.9 48.9 %copy-start = (bf16[4,128,512]{2,1,0:T(8,128)(2,1)}, bf16[4,128,512]{2,1,0:T(8,128)(2,1)S(1)}, u32[]{:S(2)}) copy-start(bf16[4,128,512]{2,1,0:T(8,128)(2,1)S(1)} %pad_maximum_fusion.refs_4_) | copy-start | bytes 1572868
  149.0 47.2 %collective-permute-start.13 = (bf16[4,128,512]{2,1,0:T(8,128)(2,1)S(1)}, bf16[4,128,512]{2,1,0:T(8,128)(2,1)S(1)}, u32[]{:S(2)}, u32[]{:S(2)}) collective-permute-start(bf16[4,128,512]{2,1,0:T(8,128)(2,1)S(1)} %pad_maximum_fusion.refs_4_), channel_id=1, source_target_pairs={{0,8},{8,16},{16,24},{24,0},{1,9},{9,17},{17,25},{25,1},{2,10},{10... | collective-permute-start | bytes 1572872 | tf_op jit(solution)/shard_map/ppermute | solution.py:162
  150.3 47.6 %collective-permute-start.14 = (bf16[4,128,512]{2,1,0:T(8,128)(2,1)S(1)}, bf16[4,128,512]{2,1,0:T(8,128)(2,1)S(1)}, u32[]{:S(2)}, u32[]{:S(2)}) collective-permute-start(bf16[4,128,512]{2,1,0:T(8,128)(2,1)S(1)} %pad_maximum_fusion.refs_4_), channel_id=1, source_target_pairs={{0,16},{8,24},{16,0},{24,8},{1,17},{9,25},{17,1},{25,9},{2,18},{10... | collective-permute-start | bytes 1572872 | tf_op jit(solution)/shard_map/ppermute | solution.py:162
  161.6 2.7 %collective-permute-start = (bf16[2,144,256]{2,1,0:T(8,128)(2,1)}, bf16[2,144,256]{2,1,0:T(8,128)(2,1)S(1)}, u32[]{:S(2)}, u32[]{:S(2)}) collective-permute-start(bf16[2,144,256]{2,1,0:T(8,128)(2,1)} %end_state.1.refs_0_), channel_id=1, source_target_pairs={{0,4},{4,0},{1,5},{5,1},{2,6},{6,2},{3,7},{7,3},{8,12},{12,8},{9,1... | collective-permute-start | bytes 442376 | tf_op jit(solution)/shard_map/ppermute | solution.py:162
  167.1 13.8 %collective-permute-start.1 = (bf16[2,144,256]{2,1,0:T(8,128)(2,1)}, bf16[2,144,256]{2,1,0:T(8,128)(2,1)S(1)}, u32[]{:S(2)}, u32[]{:S(2)}) collective-permute-start(bf16[2,144,256]{2,1,0:T(8,128)(2,1)} %get-tuple-element.10.refs_0_), channel_id=1, source_target_pairs={{0,8},{8,16},{16,24},{24,0},{1,9},{9,17},{17,25},{25,1},{2,10},{10... | collective-permute-start | bytes 442376 | tf_op jit(solution)/shard_map/ppermute | solution.py:162
  167.1 14.4 %collective-permute-start.2 = (bf16[2,144,256]{2,1,0:T(8,128)(2,1)}, bf16[2,144,256]{2,1,0:T(8,128)(2,1)S(1)}, u32[]{:S(2)}, u32[]{:S(2)}) collective-permute-start(bf16[2,144,256]{2,1,0:T(8,128)(2,1)} %get-tuple-element.10.refs_0_), channel_id=1, source_target_pairs={{0,16},{8,24},{16,0},{24,8},{1,17},{9,25},{17,1},{25,9},{2,18},{10... | collective-permute-start | bytes 442376 | tf_op jit(solution)/shard_map/ppermute | solution.py:162
  169.6 11.9 %collective-permute-start.3 = (bf16[2,144,256]{2,1,0:T(8,128)(2,1)}, bf16[2,144,256]{2,1,0:T(8,128)(2,1)S(1)}, u32[]{:S(2)}, u32[]{:S(2)}) collective-permute-start(bf16[2,144,256]{2,1,0:T(8,128)(2,1)} %get-tuple-element.10.refs_0_), channel_id=1, source_target_pairs={{0,24},{8,0},{16,8},{24,16},{1,25},{9,1},{17,9},{25,17},{2,26},{10... | collective-permute-start | bytes 442376 | tf_op jit(solution)/shard_map/ppermute | solution.py:162
  184.4 5.9 %collective-permute-start.4 = (bf16[2,144,256]{2,1,0:T(8,128)(2,1)}, bf16[2,144,256]{2,1,0:T(8,128)(2,1)S(1)}, u32[]{:S(2)}, u32[]{:S(2)}) collective-permute-start(bf16[2,144,256]{2,1,0:T(8,128)(2,1)} %get-tuple-element.12.refs_0_), channel_id=1, source_target_pairs={{0,32},{32,64},{64,96},{96,0},{1,33},{33,65},{65,97},{97,1},{2,34}... | collective-permute-start | bytes 442376 | tf_op jit(solution)/shard_map/ppermute | solution.py:162
  185.9 8.1 %collective-permute-start.5 = (bf16[2,144,256]{2,1,0:T(8,128)(2,1)}, bf16[2,144,256]{2,1,0:T(8,128)(2,1)S(1)}, u32[]{:S(2)}, u32[]{:S(2)}) collective-permute-start(bf16[2,144,256]{2,1,0:T(8,128)(2,1)} %get-tuple-element.12.refs_0_), channel_id=1, source_target_pairs={{0,64},{32,96},{64,0},{96,32},{1,65},{33,97},{65,1},{97,33},{2,66}... | collective-permute-start | bytes 442376 | tf_op jit(solution)/shard_map/ppermute | solution.py:162
  188.8 5.6 %collective-permute-start.6 = (bf16[2,144,256]{2,1,0:T(8,128)(2,1)}, bf16[2,144,256]{2,1,0:T(8,128)(2,1)S(1)}, u32[]{:S(2)}, u32[]{:S(2)}) collective-permute-start(bf16[2,144,256]{2,1,0:T(8,128)(2,1)} %get-tuple-element.12.refs_0_), channel_id=1, source_target_pairs={{0,96},{32,0},{64,32},{96,64},{1,97},{33,1},{65,33},{97,65},{2,98}... | collective-permute-start | bytes 442376 | tf_op jit(solution)/shard_map/ppermute | solution.py:162
  189.8 29.0 %copy-start.1 = (bf16[4,128,512]{2,1,0:T(8,128)(2,1)}, bf16[4,128,512]{2,1,0:T(8,128)(2,1)S(1)}, u32[]{:S(2)}) copy-start(bf16[4,128,512]{2,1,0:T(8,128)(2,1)S(1)} %pad_maximum_fusion.1.refs_8_) | copy-start | bytes 1572868
  190.3 28.4 %collective-permute-start.15 = (bf16[4,128,512]{2,1,0:T(8,128)(2,1)S(1)}, bf16[4,128,512]{2,1,0:T(8,128)(2,1)}, u32[]{:S(2)}, u32[]{:S(2)}) collective-permute-start(bf16[4,128,512]{2,1,0:T(8,128)(2,1)S(1)} %pad_maximum_fusion.refs_4_), channel_id=1, source_target_pairs={{0,24},{8,0},{16,8},{24,16},{1,25},{9,1},{17,9},{25,17},{2,26},{10... | collective-permute-start | bytes 1572872 | tf_op jit(solution)/shard_map/ppermute | solution.py:162
  194.0 25.0 %collective-permute-start.16 = (bf16[4,128,512]{2,1,0:T(8,128)(2,1)S(1)}, bf16[4,128,512]{2,1,0:T(8,128)(2,1)}, u32[]{:S(2)}, u32[]{:S(2)}) collective-permute-start(bf16[4,128,512]{2,1,0:T(8,128)(2,1)S(1)} %pad_maximum_fusion.1.refs_8_), channel_id=1, source_target_pairs={{0,32},{32,64},{64,96},{96,0},{1,33},{33,65},{65,97},{97,1},{2,34}... | collective-permute-start | bytes 1572872 | tf_op jit(solution)/shard_map/ppermute | solution.py:162
  194.4 24.6 %collective-permute-start.17 = (bf16[4,128,512]{2,1,0:T(8,128)(2,1)S(1)}, bf16[4,128,512]{2,1,0:T(8,128)(2,1)}, u32[]{:S(2)}, u32[]{:S(2)}) collective-permute-start(bf16[4,128,512]{2,1,0:T(8,128)(2,1)S(1)} %pad_maximum_fusion.1.refs_8_), channel_id=1, source_target_pairs={{0,64},{32,96},{64,0},{96,32},{1,65},{33,97},{65,1},{97,33},{2,66}... | collective-permute-start | bytes 1572872 | tf_op jit(solution)/shard_map/ppermute | solution.py:162
  196.2 23.9 %collective-permute-start.18 = (bf16[4,128,512]{2,1,0:T(8,128)(2,1)S(1)}, bf16[4,128,512]{2,1,0:T(8,128)(2,1)}, u32[]{:S(2)}, u32[]{:S(2)}) collective-permute-start(bf16[4,128,512]{2,1,0:T(8,128)(2,1)S(1)} %pad_maximum_fusion.1.refs_8_), channel_id=1, source_target_pairs={{0,96},{32,0},{64,32},{96,64},{1,97},{33,1},{65,33},{97,65},{2,98}... | collective-permute-start | bytes 1572872 | tf_op jit(solution)/shard_map/ppermute | solution.py:162
  197.8 26.8 %copy-start.10 = (bf16[4,128,512]{2,1,0:T(8,128)(2,1)}, bf16[4,128,512]{2,1,0:T(8,128)(2,1)S(1)}, u32[]{:S(2)}) copy-start(bf16[4,128,512]{2,1,0:T(8,128)(2,1)S(1)} %collective-permute-done.14.refs_6_) | copy-start | bytes 1572868
  197.8 24.1 %collective-permute-start.19 = (bf16[4,128,512]{2,1,0:T(8,128)(2,1)S(1)}, bf16[4,128,512]{2,1,0:T(8,128)(2,1)}, u32[]{:S(2)}, u32[]{:S(2)}) collective-permute-start(bf16[4,128,512]{2,1,0:T(8,128)(2,1)S(1)} %pad_maximum_fusion.refs_4_), channel_id=1, source_target_pairs={{0,4},{4,0},{1,5},{5,1},{2,6},{6,2},{3,7},{7,3},{8,12},{12,8},{9,1... | collective-permute-start | bytes 1572872 | tf_op jit(solution)/shard_map/ppermute | solution.py:162
  218.8 5.9 %collective-permute-start.23 = (bf16[4,128,512]{2,1,0:T(8,128)(2,1)S(1)}, bf16[4,128,512]{2,1,0:T(8,128)(2,1)S(1)}, u32[]{:S(2)}, u32[]{:S(2)}) collective-permute-start(bf16[4,128,512]{2,1,0:T(8,128)(2,1)S(1)} %pad_maximum_fusion.1.refs_8_), channel_id=1, source_target_pairs={{0,4},{4,0},{1,5},{5,1},{2,6},{6,2},{3,7},{7,3},{8,12},{12,8},{9,1... | collective-permute-start | bytes 1572872 | tf_op jit(solution)/shard_map/ppermute | solution.py:162
  219.0 14.3 %collective-permute-start.7 = (bf16[512,512]{1,0:T(8,128)(2,1)S(1)}, bf16[512,512]{1,0:T(8,128)(2,1)S(1)}, u32[]{:S(2)}, u32[]{:S(2)}) collective-permute-start(bf16[512,512]{1,0:T(8,128)(2,1)S(1)} %get-tuple-element.22), channel_id=1, source_target_pairs={{0,1},{1,2},{2,3},{3,0},{4,5},{5,6},{6,7},{7,4},{8,9},{9,10},{10,1... | collective-permute-start | bytes 1572872 | tf_op jit(solution)/shard_map/ppermute | solution.py:162
  219.0 26.8 %collective-permute-start.8 = (bf16[512,512]{1,0:T(8,128)(2,1)S(1)}, bf16[512,512]{1,0:T(8,128)(2,1)S(1)}, u32[]{:S(2)}, u32[]{:S(2)}) collective-permute-start(bf16[512,512]{1,0:T(8,128)(2,1)S(1)} %get-tuple-element.21), channel_id=1, source_target_pairs={{0,2},{1,3},{2,0},{3,1},{4,6},{5,7},{6,4},{7,5},{8,10},{9,11},{10,... | collective-permute-start | bytes 1572872 | tf_op jit(solution)/shard_map/ppermute | solution.py:162
  220.1 25.8 %collective-permute-start.9 = (bf16[512,512]{1,0:T(8,128)(2,1)S(1)}, bf16[512,512]{1,0:T(8,128)(2,1)S(1)}, u32[]{:S(2)}, u32[]{:S(2)}) collective-permute-start(bf16[512,512]{1,0:T(8,128)(2,1)S(1)} %get-tuple-element.20), channel_id=1, source_target_pairs={{0,3},{1,0},{2,1},{3,2},{4,7},{5,4},{6,5},{7,6},{8,11},{9,8},{10,9... | collective-permute-start | bytes 1572872 | tf_op jit(solution)/shard_map/ppermute | solution.py:162
  221.9 24.5 %collective-permute-start.20 = (bf16[4,128,512]{2,1,0:T(8,128)(2,1)S(1)}, bf16[4,128,512]{2,1,0:T(8,128)(2,1)S(1)}, u32[]{:S(2)}, u32[]{:S(2)}) collective-permute-start(bf16[4,128,512]{2,1,0:T(8,128)(2,1)S(1)} %collective-permute-done.13.refs_5_), channel_id=1, source_target_pairs={{0,4},{4,0},{1,5},{5,1},{2,6},{6,2},{3,7},{7,3},{8,12},{12,8},{9,1... | collective-permute-start | bytes 1572872 | tf_op jit(solution)/shard_map/ppermute | solution.py:162
  224.7 27.2 %copy-start.11 = (bf16[4,128,512]{2,1,0:T(8,128)(2,1)}, bf16[4,128,512]{2,1,0:T(8,128)(2,1)S(1)}, u32[]{:S(2)}) copy-start(bf16[4,128,512]{2,1,0:T(8,128)(2,1)S(1)} %collective-permute-done.23.refs_16_) | copy-start | bytes 1572868
  224.7 27.2 %collective-permute-start.21 = (bf16[4,128,512]{2,1,0:T(8,128)(2,1)S(1)}, bf16[4,128,512]{2,1,0:T(8,128)(2,1)S(1)}, u32[]{:S(2)}, u32[]{:S(2)}) collective-permute-start(bf16[4,128,512]{2,1,0:T(8,128)(2,1)S(1)} %collective-permute-done.14.refs_6_), channel_id=1, source_target_pairs={{0,4},{4,0},{1,5},{5,1},{2,6},{6,2},{3,7},{7,3},{8,12},{12,8},{9,1... | collective-permute-start | bytes 1572872 | tf_op jit(solution)/shard_map/ppermute | solution.py:162
  233.3 18.5 %collective-permute-start.22 = (bf16[4,128,512]{2,1,0:T(8,128)(2,1)}, bf16[4,128,512]{2,1,0:T(8,128)(2,1)}, u32[]{:S(2)}, u32[]{:S(2)}) collective-permute-start(bf16[4,128,512]{2,1,0:T(8,128)(2,1)} %collective-permute-done.15.refs_7_), channel_id=1, source_target_pairs={{0,4},{4,0},{1,5},{5,1},{2,6},{6,2},{3,7},{7,3},{8,12},{12,8},{9,1... | collective-permute-start | bytes 1572872 | tf_op jit(solution)/shard_map/ppermute | solution.py:162
  245.8 6.1 %collective-permute-start.24 = (bf16[4,128,512]{2,1,0:T(8,128)(2,1)}, bf16[4,128,512]{2,1,0:T(8,128)(2,1)}, u32[]{:S(2)}, u32[]{:S(2)}) collective-permute-start(bf16[4,128,512]{2,1,0:T(8,128)(2,1)} %collective-permute-done.16.refs_9_), channel_id=1, source_target_pairs={{0,4},{4,0},{1,5},{5,1},{2,6},{6,2},{3,7},{7,3},{8,12},{12,8},{9,1... | collective-permute-start | bytes 1572872 | tf_op jit(solution)/shard_map/ppermute | solution.py:162
  245.9 6.0 %collective-permute-start.25 = (bf16[4,128,512]{2,1,0:T(8,128)(2,1)}, bf16[4,128,512]{2,1,0:T(8,128)(2,1)}, u32[]{:S(2)}, u32[]{:S(2)}) collective-permute-start(bf16[4,128,512]{2,1,0:T(8,128)(2,1)} %collective-permute-done.17.refs_10_), channel_id=1, source_target_pairs={{0,4},{4,0},{1,5},{5,1},{2,6},{6,2},{3,7},{7,3},{8,12},{12,8},{9,1... | collective-permute-start | bytes 1572872 | tf_op jit(solution)/shard_map/ppermute | solution.py:162
  246.4 5.5 %collective-permute-start.26 = (bf16[4,128,512]{2,1,0:T(8,128)(2,1)}, bf16[4,128,512]{2,1,0:T(8,128)(2,1)S(1)}, u32[]{:S(2)}, u32[]{:S(2)}) collective-permute-start(bf16[4,128,512]{2,1,0:T(8,128)(2,1)} %collective-permute-done.18.refs_11_), channel_id=1, source_target_pairs={{0,4},{4,0},{1,5},{5,1},{2,6},{6,2},{3,7},{7,3},{8,12},{12,8},{9,1... | collective-permute-start | bytes 1572872 | tf_op jit(solution)/shard_map/ppermute | solution.py:162
  (14 other events, 75.4 us)

commit v2 on v1

v2 whole, which is shorter than its diff:
```python
import jax
import jax.numpy as jnp
from jax import lax
from jax.experimental import pallas as pl
from jax.experimental.pallas import tpu as pltpu
from jax.sharding import Mesh
from jax.sharding import PartitionSpec as P


DK = 128
DV = 256
BLOCK = 128
CAP = 8
NOTE = 16
EP = ("ep_0", "ep_1", "ep_2")
EP_TP = ("ep_0", "ep_1", "ep_2", "tp")
EPS = 1e-06
SCALE = DK ** (-0.5)
F32 = jnp.float32
BF16 = jnp.bfloat16


def iota(shape, dim):
    return lax.broadcasted_iota(jnp.int32, shape, dim)


def dot(a, b):
    return jnp.dot(a, b, preferred_element_type=F32)


def dot_nt(a, b):
    return lax.dot_general(a, b, (((1,), (1,)), ((), ())), preferred_element_type=F32)


def dot_tn(a, b):
    return lax.dot_general(a, b, (((0,), (0,)), ((), ())), preferred_element_type=F32)


def silu(v):
    return v / (1.0 + jnp.exp(-v))


def thirds(a):
    high = a.astype(BF16)
    rest = a - high.astype(F32)
    middle = rest.astype(BF16)
    return high, middle, (rest - middle.astype(F32)).astype(BF16)


def sums_down(pick, a):
    return sum(dot_nt(pick, part) for part in thirds(a))


def sums_across(a, pick):
    return sum(dot(part, pick) for part in thirds(a))


def end_state_body(k_ref, v_ref, a_ref, out_ref, state, total):
    step = pl.program_id(0)

    @pl.when(step == 0)
    def _():
        state[...] = jnp.zeros_like(state)
        total[...] = jnp.zeros_like(total)

    n_heads = a_ref.shape[0]
    n_blocks = k_ref.shape[0] // BLOCK
    after = iota((BLOCK, BLOCK), 1) > iota((BLOCK, BLOCK), 0)
    pick = jnp.where(after, 1.0, 0.0).astype(BF16)
    later = jnp.zeros((n_heads, 1), F32)
    keys = [[] for _ in range(n_heads)]
    for b in reversed(range(n_blocks)):
        rows = pl.ds(b * BLOCK, BLOCK)
        a = a_ref[:, rows]
        left = sums_down(pick, a)
        for h in range(n_heads):
            k = k_ref[rows, h * DK : (h + 1) * DK].astype(F32)
            fade = SCALE * jnp.exp(left[:, h : h + 1] + later[h : h + 1, :])
            keys[h].insert(0, (k * fade).astype(BF16))
        later = later + jnp.sum(a, axis=1, keepdims=True)
    for h in range(n_heads):
        gone = later[h : h + 1, :]
        added = dot_tn(jnp.concatenate(keys[h], axis=0), v_ref[:, h * DV : (h + 1) * DV])
        state[h] = state[h] * jnp.exp(gone) + added
        total[h] = total[h] + gone

    @pl.when(step == pl.num_programs(0) - 1)
    def _():
        parts = DK // 8
        for h in range(n_heads):
            whole = jnp.broadcast_to(total[h, 0:1, 0:1], (8, DV))
            high, middle, low = (part.astype(F32) for part in thirds(whole))
            row = iota((8, DV), 0)
            note = jnp.where(row == 0, high, jnp.where(row == 1, middle, low))
            note = jnp.broadcast_to(note[None], (parts, 8, DV))
            both = jnp.concatenate([state[h].reshape(parts, 8, DV), note], axis=1)
            out_ref[h * parts : (h + 1) * parts] = both.astype(BF16)


def end_state(key_rows, value_rows, log_decay):
    n_rows, n_heads = key_rows.shape[0], log_decay.shape[0]
    tile = min(512, n_rows)
    parts = n_heads * DK // 8
    return pl.pallas_call(
        end_state_body,
        grid=(n_rows // tile,),
        in_specs=[
            pl.BlockSpec((tile, n_heads * DK), lambda i: (i, 0)),
            pl.BlockSpec((tile, n_heads * DV), lambda i: (i, 0)),
            pl.BlockSpec((n_heads, tile), lambda i: (0, i)),
        ],
        out_specs=pl.BlockSpec((parts, 16, DV), lambda i: (0, 0, 0)),
        out_shape=jax.ShapeDtypeStruct((parts, 16, DV), BF16),
        scratch_shapes=[
            pltpu.VMEM((n_heads, DK, DV), F32),
            pltpu.VMEM((n_heads, 8, 128), F32),
        ],
        cost_estimate=pl.CostEstimate(
            flops=2 * n_rows * n_heads * DK * DV, bytes_accessed=4 << 20, transcendentals=0
        ),
        name="end_state",
    )(key_rows, value_rows, log_decay)


def prefix_body(in_ref, out_ref):
    before = jnp.zeros((8, DV), F32)
    for j in range(in_ref.shape[0]):
        out_ref[j] = before.astype(BF16)
        both = in_ref[j].astype(F32)
        total = both[8:9] + both[9:10] + both[10:11]
        before = before * jnp.exp(total) + both[0:8]


def prefixes(pieces):
    return pl.pallas_call(
        prefix_body,
        out_shape=jax.ShapeDtypeStruct((pieces.shape[0], 8, DV), BF16),
        name="prefixes",
    )(pieces)


def shift(x, axis, d):
    peers = lax.axis_size(axis)
    return lax.ppermute(x, axis, [(k, (k + d) % peers) for k in range(peers)])


def all_shifts(x, axis):
    return [x] + [shift(x, axis, d) for d in range(1, lax.axis_size(axis))]


def mixer_body(q_ref, k_ref, v_ref, g_ref, a_ref, first_ref, out_ref, state):
    @pl.when(pl.program_id(0) == 0)
    def _():
        state[...] = first_ref[...].astype(F32).reshape(state.shape)

    n_heads = a_ref.shape[0]
    t, m = iota((BLOCK, BLOCK), 0), iota((BLOCK, BLOCK), 1)
    causal = t >= m
    upto = jnp.where(t <= m, 1.0, 0.0).astype(BF16)
    downto = jnp.where(causal, 1.0, 0.0).astype(BF16)
    for b in range(q_ref.shape[0] // BLOCK):
        rows = pl.ds(b * BLOCK, BLOCK)
        a = a_ref[:, rows]
        down = sums_down(downto, a)
        across = sums_across(a, upto)
        for h in range(n_heads):
            q = q_ref[rows, h * DK : (h + 1) * DK]
            k = k_ref[rows, h * DK : (h + 1) * DK]
            v = v_ref[rows, h * DV : (h + 1) * DV]
            gate = g_ref[rows, h * DV : (h + 1) * DV].astype(F32)
            col, row = down[:, h : h + 1], across[h : h + 1, :]
            whole = row[:, BLOCK - 1 : BLOCK]
            decay = jnp.where(causal, jnp.exp(jnp.where(causal, col - row, 0.0)), 0.0)
            weight = (dot_nt(q, k) * SCALE * decay).astype(BF16)
            before = state[h]
            raw = dot(weight, v) + dot(q, before.astype(BF16)) * jnp.exp(col)
            faded = (k.astype(F32) * (SCALE * jnp.exp(whole - col))).astype(BF16)
            state[h] = before * jnp.exp(whole) + dot_tn(faded, v)
            centered = raw - jnp.mean(raw, axis=1, keepdims=True)
            spread = jnp.mean(centered * centered, axis=1, keepdims=True)
            normed = centered * lax.rsqrt(spread + EPS)
            out_ref[rows, h * DV : (h + 1) * DV] = (silu(gate) * normed).astype(BF16)


def mixer(query_rows, key_rows, value_rows, gate_rows, log_decay, incoming):
    n_rows, n_heads = query_rows.shape[0], log_decay.shape[0]
    tile = min(256, n_rows)
    return pl.pallas_call(
        mixer_body,
        grid=(n_rows // tile,),
        in_specs=[
            pl.BlockSpec((tile, n_heads * DK), lambda i: (i, 0)),
            pl.BlockSpec((tile, n_heads * DK), lambda i: (i, 0)),
            pl.BlockSpec((tile, n_heads * DV), lambda i: (i, 0)),
            pl.BlockSpec((tile, n_heads * DV), lambda i: (i, 0)),
            pl.BlockSpec((n_heads, tile), lambda i: (0, i)),
            pl.BlockSpec((n_heads * DK, DV), lambda i: (0, 0)),
        ],
        out_specs=pl.BlockSpec((tile, n_heads * DV), lambda i: (i, 0)),
        out_shape=jax.ShapeDtypeStruct((n_rows, n_heads * DV), BF16),
        scratch_shapes=[pltpu.VMEM((n_heads, DK, DV), F32)],
        cost_estimate=pl.CostEstimate(
            flops=12 * n_rows * n_heads * DK * DV, bytes_accessed=8 << 20, transcendentals=0
        ),
        name="mixer",
    )(query_rows, key_rows, value_rows, gate_rows, log_decay, incoming)


def project_body(*refs):
    heads, whole, own, other, out_ref, lhs, rhs, sems = (
        refs[:4],
        refs[4],
        refs[5:8],
        refs[8:11],
        *refs[11:],
    )
    x, core = lax.axis_index("tp"), lax.axis_index("ep_2")
    half = rhs.shape[-1]
    pairs = [(heads[0].at[x], lhs.at[0])]
    for d in range(1, 4):
        pairs.append((heads[d], lhs.at[d]))
    for side in range(2):
        pairs.append((whole.at[:, side * half : (side + 1) * half], rhs.at[0, side]))
    for d in range(1, 4):
        pairs.append((own[d - 1], rhs.at[d, core]))
        pairs.append((other[d - 1], rhs.at[d, 1 - core]))
    copies = [
        pltpu.make_async_copy(source, target, sems.at[n])
        for n, (source, target) in enumerate(pairs)
    ]
    for copy in copies:
        copy.start()
    for copy in copies:
        copy.wait()
    fine = half // 2
    for side in range(2):
        for part in range(2):
            at = slice(part * fine, (part + 1) * fine)
            total = dot(lhs[0], rhs[0, side, :, at])
            for d in range(1, 4):
                total = total + dot(lhs[d], rhs[d, side, :, at])
            start = side * half + part * fine
            out_ref[:, start : start + fine] = total.astype(BF16)


def project(retained, received, whole, own, other):
    groups, n_rows, width = retained.shape
    half = whole.shape[1] // 2
    arrays = [retained, *received, whole, *own, *other]
    return pl.pallas_call(
        project_body,
        in_specs=[pl.BlockSpec(memory_space=pl.ANY)] * len(arrays),
        out_shape=jax.ShapeDtypeStruct((n_rows, 2 * half), BF16),
        scratch_shapes=[
            pltpu.VMEM((groups, n_rows, width), BF16),
            pltpu.VMEM((groups, 2, width, half), BF16),
            pltpu.SemaphoreType.DMA((12,)),
        ],
        cost_estimate=pl.CostEstimate(
            flops=4 * n_rows * groups * width * half, bytes_accessed=12 << 20, transcendentals=0
        ),
        name="project",
    )(*arrays)


def gather_projection(out_proj):
    n_rows, width = out_proj.shape
    half = width // 2
    mine = lax.dynamic_slice(out_proj, (0, lax.axis_index("ep_2") * half), (n_rows, half))
    own = all_shifts(mine, "tp")[1:]
    other = [shift(part, "ep_2", 1) for part in own]
    return own, other


def norm_body(x_ref, gain_ref, route_ref, out_ref):
    x = x_ref[...].astype(F32)
    n_tokens = x.shape[0]
    mean = jnp.mean(x * x, axis=1, keepdims=True)
    out_ref[:n_tokens] = (x * lax.rsqrt(mean + EPS) * gain_ref[...]).astype(BF16)
    row = iota((NOTE, n_tokens), 0)
    note = jnp.zeros((NOTE, n_tokens), F32)
    for k in range(route_ref.shape[0]):
        note = jnp.where(row == k, route_ref[k : k + 1].astype(F32), note)
    out_ref[n_tokens:, :n_tokens] = note.astype(BF16)
    rest = (NOTE, x.shape[1] - n_tokens)
    out_ref[n_tokens:, n_tokens:] = jnp.zeros(rest, BF16)


def norm(moe_input, norm_gain, routes):
    n_tokens, width = moe_input.shape
    return pl.pallas_call(
        norm_body,
        out_shape=jax.ShapeDtypeStruct((n_tokens + NOTE, width), BF16),
        name="norm",
    )(moe_input, norm_gain.reshape(1, width), routes)


def ranked(hits, n_tokens):
    earlier = iota((n_tokens, n_tokens), 0) < iota((n_tokens, n_tokens), 1)
    rank = dot(hits.astype(BF16), jnp.where(earlier, 1.0, 0.0).astype(BF16))
    return jnp.where(hits > 0.0, rank, float(CAP)).astype(BF16)


def dispatch_body(*refs):
    messages, out_ref = refs[:-1], refs[-1]
    groups = len(messages)
    n_slots = out_ref.shape[0]
    each = groups * CAP
    experts = n_slots // each
    n_tokens = messages[0].shape[0] - NOTE
    x = lax.axis_index("tp")
    expert = (iota((experts, n_tokens), 0) * groups + x).astype(F32)
    spread = jnp.where(iota((n_slots, experts), 0) // each == iota((n_slots, experts), 1), 1.0, 0.0)
    spread = spread.astype(BF16)
    slot = iota((n_slots, n_tokens), 0)
    place = (slot % CAP).astype(F32)
    block = (slot // CAP) % groups
    picks = []
    for d in range(groups):
        named = messages[d][n_tokens:, :n_tokens].astype(F32)
        hits = jnp.zeros((experts, n_tokens), F32)
        for k in range(4):
            hits = jnp.where(named[k : k + 1] == expert, 1.0, hits)
        here = dot(spread, ranked(hits, n_tokens)) == place
        here = here & (block == (x - d + groups) % groups)
        picks.append(jnp.where(here, 1.0, 0.0).astype(BF16))
    for d in range(0, groups, 2):
        pick = jnp.concatenate([picks[d], picks[d + 1]], axis=1)
        rows = jnp.concatenate([messages[d][:n_tokens], messages[d + 1][:n_tokens]], axis=0)
        part = dot(pick, rows)
        total = part if d == 0 else total + part
    out_ref[...] = total.astype(BF16)


def dispatch(messages, n_slots):
    width = messages[0].shape[1]
    return pl.pallas_call(
        dispatch_body,
        out_shape=jax.ShapeDtypeStruct((n_slots, width), BF16),
        cost_estimate=pl.CostEstimate(
            flops=1024 * n_slots * width, bytes_accessed=6 << 20, transcendentals=0
        ),
        name="dispatch",
    )(*messages)


def weights_body(route_ref, weight_ref, high_ref, low_ref):
    n_visits, n_tokens = route_ref.shape
    n_slots = high_ref.shape[0]
    experts = n_slots // CAP
    expert = iota((experts, n_tokens), 0)
    hits = jnp.zeros((experts, n_tokens), F32)
    weighed = jnp.zeros((experts, n_tokens), F32)
    for k in range(n_visits):
        hit = route_ref[k : k + 1] == expert
        hits = jnp.where(hit, 1.0, hits)
        weighed = jnp.where(hit, weight_ref[k : k + 1], weighed)
    spread = jnp.where(iota((n_slots, experts), 0) // CAP == iota((n_slots, experts), 1), 1.0, 0.0)
    spread = spread.astype(BF16)
    place = (iota((n_slots, n_tokens), 0) % CAP).astype(F32)
    here = dot(spread, ranked(hits, n_tokens)) == place
    high = weighed.astype(BF16)
    low = (weighed - high.astype(F32)).astype(BF16)
    high_ref[...] = jnp.where(here, dot(spread, high), 0.0).astype(BF16)
    low_ref[...] = jnp.where(here, dot(spread, low), 0.0).astype(BF16)


def slot_weights(routes, route_weights, n_slots):
    n_tokens = routes.shape[1]
    return pl.pallas_call(
        weights_body,
        out_shape=[jax.ShapeDtypeStruct((n_slots, n_tokens), BF16)] * 2,
        cost_estimate=pl.CostEstimate(flops=1 << 27, bytes_accessed=1 << 20, transcendentals=0),
        name="weights",
    )(routes, route_weights)


def expert_body(x_ref, gate_ref, up_ref, down_ref, out_ref):
    x = x_ref[...]
    hidden = (silu(dot(x, gate_ref[...])) * dot(x, up_ref[...])).astype(BF16)
    out_ref[...] = dot(hidden, down_ref[...]).astype(out_ref.dtype)


def expert_apply(rows, w_gate, w_up, w_down, dtype, n_rows=None):
    n_rows, width = n_rows or rows.shape[0], rows.shape[1]
    hidden = w_gate.shape[1]
    tile = min(256, n_rows)
    return pl.pallas_call(
        expert_body,
        grid=(n_rows // tile,),
        in_specs=[
            pl.BlockSpec((tile, width), lambda i: (i, 0)),
            pl.BlockSpec((width, hidden), lambda i: (0, 0)),
            pl.BlockSpec((width, hidden), lambda i: (0, 0)),
            pl.BlockSpec((hidden, width), lambda i: (0, 0)),
        ],
        out_specs=pl.BlockSpec((tile, width), lambda i: (i, 0)),
        out_shape=jax.ShapeDtypeStruct((n_rows, width), dtype),
        cost_estimate=pl.CostEstimate(
            flops=6 * n_rows * width * hidden, bytes_accessed=14 << 20, transcendentals=0
        ),
        name="expert",
    )(rows, w_gate, w_up, w_down)


def combine_body(high_ref, low_ref, rows_ref, shared_ref, out_ref):
    rows = rows_ref[...]
    total = dot_tn(high_ref[...], rows) + dot_tn(low_ref[...], rows) + shared_ref[...]
    out_ref[...] = total.astype(BF16)


def combine(high, low, rows, shared):
    n_slots, n_tokens = high.shape
    width = rows.shape[1]
    tile = width // 4
    return pl.pallas_call(
        combine_body,
        grid=(width // tile,),
        in_specs=[
            pl.BlockSpec((n_slots, n_tokens), lambda i: (0, 0)),
            pl.BlockSpec((n_slots, n_tokens), lambda i: (0, 0)),
            pl.BlockSpec((n_slots, tile), lambda i: (0, i)),
            pl.BlockSpec((n_tokens, tile), lambda i: (0, i)),
        ],
        out_specs=pl.BlockSpec((n_tokens, tile), lambda i: (0, i)),
        out_shape=jax.ShapeDtypeStruct((n_tokens, width), BF16),
        cost_estimate=pl.CostEstimate(
            flops=4 * n_tokens * n_slots * width, bytes_accessed=6 << 20, transcendentals=0
        ),
        name="combine",
    )(high, low, rows, shared)


def exchange(x, axes):
    return lax.all_to_all(x, axes, split_axis=0, concat_axis=0, tiled=True)


def local(
    query_rows,
    key_rows,
    value_rows,
    gate_rows,
    log_decay,
    out_proj,
    moe_input,
    norm_gain,
    routing,
    route_weight,
    expert_gate,
    expert_up,
    expert_down,
    shared_gate,
    shared_up,
    shared_down,
):
    n_rows = query_rows.shape[0]
    width = moe_input.shape[1]
    tp = lax.axis_size("tp")
    experts = lax.axis_size(EP) * tp

    n_tokens = moe_input.shape[0]
    places = lax.axis_size(EP)
    routes, route_weights = routing.T, route_weight.T
    message = norm(moe_input, norm_gain, routes)
    messages = all_shifts(message, "tp")

    pieces = end_state(key_rows, value_rows, log_decay)
    pieces = exchange(pieces, EP)
    pieces = prefixes(pieces)
    incoming = exchange(pieces, EP).reshape(-1, DV)

    outgoing = dispatch(messages, experts * CAP)
    received = exchange(outgoing.reshape(places, tp * CAP, width), EP)

    own, other = gather_projection(out_proj)

    retained = mixer(query_rows, key_rows, value_rows, gate_rows, log_decay, incoming)
    retained = retained.reshape(tp, n_rows // tp, -1)
    place = lax.axis_index("tp")
    heads = []
    for d in range(1, tp):
        block = lax.dynamic_index_in_dim(retained, (place + d) % tp, keepdims=False)
        heads.append(shift(block, "tp", d))

    shared = expert_apply(message, shared_gate, shared_up, shared_down, F32, n_tokens)
    high, low = slot_weights(routes, route_weights, experts * CAP)

    served = expert_apply(
        received.reshape(-1, width), expert_gate[0], expert_up[0], expert_down[0], BF16
    )
    returned = exchange(served.reshape(experts, CAP, width), EP_TP)

    mixer_out = project(retained, heads, out_proj, own, other)
    moe_out = combine(high, low, returned.reshape(-1, width), shared)
    return (mixer_out, moe_out)


def solution(mesh):
    split = Mesh(mesh.devices.reshape(4, 4, 2, mesh.shape["tp"]), ("ep_0", "ep_1", "ep_2", "tp"))
    return jax.shard_map(
        local,
        mesh=split,
        in_specs=(
            P(EP, "tp"),
            P(EP, "tp"),
            P(EP, "tp"),
            P(EP, "tp"),
            P("tp", EP),
            P("tp", None),
            P(EP_TP, None),
            P(),
            P(EP_TP, None),
            P(EP_TP, None),
            P(EP_TP, None, None),
            P(EP_TP, None, None),
            P(EP_TP, None, None),
            P(),
            P(),
            P(),
        ),
        out_specs=(P(EP_TP, None), P(EP_TP, None)),
        check_vma=False,
    )
```

time: 268 us -> 265 us (0.989)
  blocking collectives: 64.9 us -> 0 us
  waiting for transfers between devices: 78.5 us -> 123 us
  starting transfers between devices: 49.5 us -> 72.1 us
  local copies, waits for them, and re-layouts: 8.61 us -> 5.01 us
    all_to_all x1 -> x0, blocking collectives: 64.9 us -> none  [exchange(): return lax.all_to_all(x, axes, split_axis=0, concat_axis=0, tiled=True)]
    all_to_all x1 -> x4, waiting for transfers between devices: 0.01 us -> 49 us  [exchange(): return lax.all_to_all(x, axes, split_axis=0, concat_axis=0, tiled=True)]
    all_to_all x1 -> x4, starting transfers between devices: 5.05 us -> 35.8 us  [exchange(): return lax.all_to_all(x, axes, split_axis=0, concat_axis=0, tiled=True)]
    ppermute x27 -> x12, starting transfers between devices: 44.4 us -> 36.4 us  [shift(): return lax.ppermute(x, axis, [(k, (k + d) % peers) for k in range(peers)])]
    ppermute x27 -> x12, waiting for transfers between devices: 78.5 us -> 73.8 us  [shift(): return lax.ppermute(x, axis, [(k, (k + d) % peers) for k in range(peers)])]
    pallas_call x1, Pallas kernels: 8.76 us -> 5.19 us  [end_state(): pl.pallas_call(end_state_body, grid=(n_rows // tile,), in_specs=[pl.Block...]
  transfers between devices with their start and end apart: 28 -> 16, of which waited for: 9 -> 7; matrix products, arithmetic and copies ran while one was open for 1% -> 1% of each run, Pallas kernels for 16% -> 21%
where the time goes in v2:
time: 265 us; the launch traced here: 263 us
  waiting for transfers between devices  123 us (46%)
  starting transfers between devices  72.1 us (27%)
  Pallas kernels  62 us (23%)
  local copies, waits for them, and re-layouts  5.01 us (2%)
    ppermute x12, waiting for transfers between devices, shift(): return lax.ppermute(x, axis, [(k, (k + d) % peers) for k in range(peers)])  73.8 us
    all_to_all x4, waiting for transfers between devices, exchange(): return lax.all_to_all(x, axes, split_axis=0, concat_axis=0, tiled=True)  49 us
    ppermute x12, starting transfers between devices, shift(): return lax.ppermute(x, axis, [(k, (k + d) % peers) for k in range(peers)])  36.4 us
    all_to_all x4, starting transfers between devices, exchange(): return lax.all_to_all(x, axes, split_axis=0, concat_axis=0, tiled=True)  35.8 us
    pallas_call x2, Pallas kernels, expert_apply(): pl.pallas_call(expert_body, grid=(n_rows // tile,), in_specs=[pl.BlockSpe...  16.8 us
    pallas_call x1, Pallas kernels, mixer(): pl.pallas_call(mixer_body, grid=(n_rows // tile,), in_specs=[pl.BlockSpec...  12.6 us
    pallas_call x1, Pallas kernels, project(): pl.pallas_call(project_body, in_specs=[pl.BlockSpec(memory_space=pl.ANY)]...  9.92 us
    pallas_call x1, Pallas kernels, dispatch(): pl.pallas_call(dispatch_body, out_shape=jax.ShapeDtypeStruct((n_slots, wi...  6.51 us
  transfers between devices with their start and end apart: 16, of which 7 were waited for; matrix products, arithmetic and copies ran while one was open for 1% of the time, Pallas kernels for 21%

profile of v2, /device:TPU:1, one launch (start us, length us, event | category | flops | bytes accessed | tf_op | source)
XLA Modules:
  0.0 262.7 jit_solution(2367674911075845272)
XLA Ops:
  0.6 2.1 norm.1.refs_0_.x_ref
  2.7 3.6 %collective-permute-start.10 = (bf16[144,2048]{1,0:T(8,128)(2,1)}, bf16[144,2048]{1,0:T(8,128)(2,1)S(1)}, u32[]{:S(2)}, u32[]{:S(2)}) collective-permute-start(bf16[144,2048]{1,0:T(8,128)(2,1)} %norm.1.refs_0_.x_ref), channel_id=1, source_target_pairs={{0,2},{1,3},{2,0},{3,1},{4,6},{5,7},{6,4},{7,5},{8,10},{9,11},{10,... | collective-permute-start | bytes 1769480 | tf_op jit(solution)/shard_map/ppermute | solution.py:144
  6.3 0.9 collective-permute-start.11
  7.8 5.2 %end_state.1 = bf16[32,16,256]{2,1,0:T(8,128)(2,1)} custom-call(bf16[2048,256]{1,0:T(8,128)(2,1)} %k_ref.3, bf16[2048,512]{1,0:T(8,128)(2,1)} %v_ref.3, f32[2,2048]{1,0:T(2,128)} %a_ref.3), custom_call_target="tpu_custom_call" | custom-call | flops 268435456 | bytes 4194304 | tf_op jit(solution)/shard_map/end_state/pallas_call | solution.py:104
  12.9 9.6 %all-to-all-start = ((bf16[32,16,256]{2,1,0:T(8,128)(2,1)}), bf16[32,16,256]{2,1,0:T(8,128)(2,1)S(1)}, u32[]{:S(2)}, u32[]{:S(2)}) async-start(bf16[32,16,256]{2,1,0:T(8,128)(2,1)} %end_state.1), calls=%async_computation | async-start | bytes 524288 | tf_op jit(solution)/shard_map/all_to_all | solution.py:435
  22.6 9.7 %collective-permute-done.11.refs_3_ = bf16[144,2048]{1,0:T(8,128)(2,1)S(1)} collective-permute-done((bf16[144,2048]{1,0:T(8,128)(2,1)}, bf16[144,2048]{1,0:T(8,128)(2,1)S(1)}, u32[]{:S(2)}, u32[]{:S(2)}) %collective-permute-start.11) | collective-permute-done | bytes 589856 | tf_op jit(solution)/shard_map/ppermute | solution.py:144
  33.1 0.8 copy-done.7
  34.0 6.5 %dispatch.1 = bf16[1024,2048]{1,0:T(8,128)(2,1)} custom-call(bf16[144,2048]{1,0:T(8,128)(2,1)} %norm.1.refs_0_.x_ref, bf16[144,2048]{1,0:T(8,128)(2,1)} %copy-done.7, bf16[144,2048]{1,0:T(8,128)(2,1)} %copy-done.5, bf16[144,2048]{1,0:T(8,128)(2,1)} %copy-done.6), custom_call_target="tpu_custom_call" | custom-call | flops 2147483648 | bytes 6291456 | tf_op jit(solution)/shard_map/dispatch/pallas_call | solution.py:337
  41.2 9.6 %all-to-all-start.2 = ((bf16[32,32,2048]{2,1,0:T(8,128)(2,1)}), bf16[32,32,2048]{2,1,0:T(8,128)(2,1)}, u32[]{:S(2)}, u32[]{:S(2)}) async-start(bf16[32,32,2048]{2,1,0:T(8,128)(2,1)} %bitcast.21), calls=%async_computation.2 | async-start | bytes 8388608 | tf_op jit(solution)/shard_map/all_to_all | solution.py:435
  50.8 1.7 prefixes.1
  52.5 49.0 %all-to-all-done.2 = bf16[32,32,2048]{2,1,0:T(8,128)(2,1)} async-done(((bf16[32,32,2048]{2,1,0:T(8,128)(2,1)}), bf16[32,32,2048]{2,1,0:T(8,128)(2,1)}, u32[]{:S(2)}, u32[]{:S(2)}) %all-to-all-start.2) | async-done | bytes 4194336 | tf_op jit(solution)/shard_map/all_to_all | solution.py:435
  101.5 7.1 %all-to-all-start.1 = ((bf16[32,8,256]{2,1,0:T(8,128)(2,1)}), bf16[32,8,256]{2,1,0:T(8,128)(2,1)S(1)}, u32[]{:S(2)}, u32[]{:S(2)}) async-start(bf16[32,8,256]{2,1,0:T(8,128)(2,1)} %prefixes.1), calls=%async_computation.1 | async-start | bytes 262144 | tf_op jit(solution)/shard_map/all_to_all | solution.py:435
  108.6 11.7 %expert.2 = bf16[1024,2048]{1,0:T(8,128)(2,1)} custom-call(bf16[1024,2048]{1,0:T(8,128)(2,1)} %bitcast.9.x_ref, bf16[2048,512]{1,0:T(8,128)(2,1)} %bitcast.26, bf16[2048,512]{1,0:T(8,128)(2,1)} %bitcast.27, bf16[512,2048]{1,0:T(8,128)(2,1)} %bitcast.28), custom_call_target="tpu_custom_call" | custom-call | flops 6442450944 | bytes 14680064 | tf_op jit(solution)/shard_map/expert/pallas_call | solution.py:388
  121.0 9.4 %all-to-all-start.3 = ((bf16[128,8,2048]{2,1,0:T(8,128)(2,1)}), bf16[128,8,2048]{2,1,0:T(8,128)(2,1)}, u32[]{:S(2)}, u32[]{:S(2)}) async-start(bf16[128,8,2048]{2,1,0:T(8,128)(2,1)} %bitcast.20), calls=%async_computation.3 | async-start | bytes 8388608 | tf_op jit(solution)/shard_map/all_to_all | solution.py:435
  130.6 1.4 collective-permute-start.3
  132.0 2.4 collective-permute-start.4
  134.4 1.2 collective-permute-start.5
  135.6 12.6 %mixer.1 = bf16[2048,512]{1,0:T(8,128)(2,1)} custom-call(bf16[2048,256]{1,0:T(8,128)(2,1)} %q_ref.1, bf16[2048,256]{1,0:T(8,128)(2,1)} %k_ref.3, bf16[2048,512]{1,0:T(8,128)(2,1)} %v_ref.3, bf16[2048,512]{1,0:T(8,128)(2,1)} %g_ref.1, f32[2,2048]{1,0:T(2,128)} %a_ref.3, bf16[256,256]{1,0:T(8,128)(2,1)} %bitcast.22), custom_call_target="tpu_custom_call" | custom-call | flops 1610612736 | bytes 8388608 | tf_op jit(solution)/shard_map/mixer/pallas_call | solution.py:188
  148.2 1.5 dynamic-slice_bitcast_fusion
  150.0 50.0 %collective-permute-done.3.refs_5_ = bf16[512,1024]{1,0:T(8,128)(2,1)S(1)} collective-permute-done((bf16[512,1024]{1,0:T(8,128)(2,1)S(1)}, bf16[512,1024]{1,0:T(8,128)(2,1)S(1)}, u32[]{:S(2)}, u32[]{:S(2)}) %collective-permute-start.3) | collective-permute-done | bytes 1048608 | tf_op jit(solution)/shard_map/ppermute | solution.py:144
  200.0 23.7 %collective-permute-start.6 = (bf16[512,1024]{1,0:T(8,128)(2,1)S(1)}, bf16[512,1024]{1,0:T(8,128)(2,1)}, u32[]{:S(2)}, u32[]{:S(2)}) collective-permute-start(bf16[512,1024]{1,0:T(8,128)(2,1)S(1)} %collective-permute-done.3.refs_5_), channel_id=1, source_target_pairs={{0,4},{4,0},{1,5},{5,1},{2,6},{6,2},{3,7},{7,3},{8,12},{12,8},{9,1... | collective-permute-start | bytes 3145736 | tf_op jit(solution)/shard_map/ppermute | solution.py:144
  223.6 0.8 collective-permute-start.7
  224.4 0.8 collective-permute-start.1
  225.2 8.4 %collective-permute-done.refs_1_ = bf16[512,512]{1,0:T(8,128)(2,1)S(1)} collective-permute-done((bf16[512,512]{1,0:T(8,128)(2,1)S(1)}, bf16[512,512]{1,0:T(8,128)(2,1)S(1)}, u32[]{:S(2)}, u32[]{:S(2)}) %collective-permute-start) | collective-permute-done | bytes 524320 | tf_op jit(solution)/shard_map/ppermute | solution.py:144
  233.7 0.7 collective-permute-start.2
  234.5 2.0 weights.1
  236.5 5.1 %expert.3.shared_ref = f32[128,2048]{1,0:T(8,128)} custom-call(bf16[144,2048]{1,0:T(8,128)(2,1)} %norm.1.refs_0_.x_ref, bf16[2048,512]{1,0:T(8,128)(2,1)} %gate_ref.1, bf16[2048,512]{1,0:T(8,128)(2,1)} %up_ref.1, bf16[512,2048]{1,0:T(8,128)(2,1)} %down_ref.1), custom_call_target="tpu_custom_call" | custom-call | flops 805306368 | bytes 14680064 | tf_op jit(solution)/shard_map/expert/pallas_call | solution.py:388
  241.6 3.8 %collective-permute-done.1.refs_2_ = bf16[512,512]{1,0:T(8,128)(2,1)} collective-permute-done((bf16[512,512]{1,0:T(8,128)(2,1)S(1)}, bf16[512,512]{1,0:T(8,128)(2,1)}, u32[]{:S(2)}, u32[]{:S(2)}) %collective-permute-start.1) | collective-permute-done | bytes 524320 | tf_op jit(solution)/shard_map/ppermute | solution.py:144
  245.4 1.3 collective-permute-done.2.refs_3_
  246.7 1.0 copy-done.4
  247.7 9.9 %project.1 = bf16[512,2048]{1,0:T(8,128)(2,1)} custom-call(bf16[4,512,512]{2,1,0:T(8,128)(2,1)} %bitcast.19, bf16[512,512]{1,0:T(8,128)(2,1)} %copy-done.8, bf16[512,512]{1,0:T(8,128)(2,1)} %collective-permute-done.1.refs_2_, bf16[512,512]{1,0:T(8,128)(2,1)} %collective-permute-done.2.refs_3_, bf16[512,2048]{1,0:T(8,128)(2,1)} %refs_4_.1, ...), custom_call_target="tpu_custom_call" | custom-call | flops 4294967296 | bytes 12582912 | tf_op jit(solution)/shard_map/project/pallas_call | solution.py:250
  257.6 5.1 %combine.1 = bf16[128,2048]{1,0:T(8,128)(2,1)} custom-call(bf16[1024,128]{1,0:T(8,128)(2,1)} %get-tuple-element.4.high_ref, bf16[1024,128]{1,0:T(8,128)(2,1)} %get-tuple-element.5.low_ref, bf16[1024,2048]{1,0:T(8,128)(2,1)} %bitcast.14.rows_ref, f32[128,2048]{1,0:T(8,128)} %expert.3.shared_ref), custom_call_target="tpu_custom_call" | custom-call | flops 1073741824 | bytes 6291456 | tf_op jit(solution)/shard_map/combine/pallas_call | solution.py:416
  (30 shorter events, 3.3 us)
Async XLA Ops:
  2.7 19.8 %collective-permute-start.10 = (bf16[144,2048]{1,0:T(8,128)(2,1)}, bf16[144,2048]{1,0:T(8,128)(2,1)S(1)}, u32[]{:S(2)}, u32[]{:S(2)}) collective-permute-start(bf16[144,2048]{1,0:T(8,128)(2,1)} %norm.1.refs_0_.x_ref), channel_id=1, source_target_pairs={{0,2},{1,3},{2,0},{3,1},{4,6},{5,7},{6,4},{7,5},{8,10},{9,11},{10,... | collective-permute-start | bytes 1769480 | tf_op jit(solution)/shard_map/ppermute | solution.py:144
  6.3 26.0 %collective-permute-start.11 = (bf16[144,2048]{1,0:T(8,128)(2,1)}, bf16[144,2048]{1,0:T(8,128)(2,1)S(1)}, u32[]{:S(2)}, u32[]{:S(2)}) collective-permute-start(bf16[144,2048]{1,0:T(8,128)(2,1)} %norm.1.refs_0_.x_ref), channel_id=1, source_target_pairs={{0,3},{1,0},{2,1},{3,2},{4,7},{5,4},{6,5},{7,6},{8,11},{9,8},{10,9... | collective-permute-start | bytes 1769480 | tf_op jit(solution)/shard_map/ppermute | solution.py:144
  7.2 25.8 %collective-permute-start.9 = (bf16[144,2048]{1,0:T(8,128)(2,1)}, bf16[144,2048]{1,0:T(8,128)(2,1)S(1)}, u32[]{:S(2)}, u32[]{:S(2)}) collective-permute-start(bf16[144,2048]{1,0:T(8,128)(2,1)} %norm.1.refs_0_.x_ref), channel_id=1, source_target_pairs={{0,1},{1,2},{2,3},{3,0},{4,5},{5,6},{6,7},{7,4},{8,9},{9,10},{10,1... | collective-permute-start | bytes 1769480 | tf_op jit(solution)/shard_map/ppermute | solution.py:144
  12.9 27.5 %all-to-all-start = ((bf16[32,16,256]{2,1,0:T(8,128)(2,1)}), bf16[32,16,256]{2,1,0:T(8,128)(2,1)S(1)}, u32[]{:S(2)}, u32[]{:S(2)}) async-start(bf16[32,16,256]{2,1,0:T(8,128)(2,1)} %end_state.1), calls=%async_computation | async-start | bytes 524288 | tf_op jit(solution)/shard_map/all_to_all | solution.py:435
  22.6 10.4 %copy-start.5 = (bf16[144,2048]{1,0:T(8,128)(2,1)}, bf16[144,2048]{1,0:T(8,128)(2,1)S(1)}, u32[]{:S(2)}) copy-start(bf16[144,2048]{1,0:T(8,128)(2,1)S(1)} %collective-permute-done.10.refs_2_) | copy-start | bytes 1769476
  32.3 0.8 copy-start.6
  33.1 0.8 copy-start.7
  40.5 0.7 copy-start
  41.2 60.3 %all-to-all-start.2 = ((bf16[32,32,2048]{2,1,0:T(8,128)(2,1)}), bf16[32,32,2048]{2,1,0:T(8,128)(2,1)}, u32[]{:S(2)}, u32[]{:S(2)}) async-start(bf16[32,32,2048]{2,1,0:T(8,128)(2,1)} %bitcast.21), calls=%async_computation.2 | async-start | bytes 8388608 | tf_op jit(solution)/shard_map/all_to_all | solution.py:435
  101.5 18.8 %all-to-all-start.1 = ((bf16[32,8,256]{2,1,0:T(8,128)(2,1)}), bf16[32,8,256]{2,1,0:T(8,128)(2,1)S(1)}, u32[]{:S(2)}, u32[]{:S(2)}) async-start(bf16[32,8,256]{2,1,0:T(8,128)(2,1)} %prefixes.1), calls=%async_computation.1 | async-start | bytes 262144 | tf_op jit(solution)/shard_map/all_to_all | solution.py:435
  120.3 0.7 copy-start.1
  120.3 10.1 %copy-start.2 = (bf16[512,2048]{1,0:T(8,128)(2,1)S(1)}, bf16[512,2048]{1,0:T(8,128)(2,1)}, u32[]{:S(2)}) copy-start(bf16[512,2048]{1,0:T(8,128)(2,1)} %refs_4_.1) | copy-start | bytes 6291460
  121.0 136.6 %all-to-all-start.3 = ((bf16[128,8,2048]{2,1,0:T(8,128)(2,1)}), bf16[128,8,2048]{2,1,0:T(8,128)(2,1)}, u32[]{:S(2)}, u32[]{:S(2)}) async-start(bf16[128,8,2048]{2,1,0:T(8,128)(2,1)} %bitcast.20), calls=%async_computation.3 | async-start | bytes 8388608 | tf_op jit(solution)/shard_map/all_to_all | solution.py:435
  130.6 69.4 %collective-permute-start.3 = (bf16[512,1024]{1,0:T(8,128)(2,1)S(1)}, bf16[512,1024]{1,0:T(8,128)(2,1)S(1)}, u32[]{:S(2)}, u32[]{:S(2)}) collective-permute-start(bf16[512,1024]{1,0:T(8,128)(2,1)S(1)} %constant_dynamic-slice_fusion), channel_id=1, source_target_pairs={{0,1},{1,2},{2,3},{3,0},{4,5},{5,6},{6,7},{7,4},{8,9},{9,10},{10,1... | collective-permute-start | bytes 3145736 | tf_op jit(solution)/shard_map/ppermute | solution.py:144
  132.0 91.7 %collective-permute-start.4 = (bf16[512,1024]{1,0:T(8,128)(2,1)S(1)}, bf16[512,1024]{1,0:T(8,128)(2,1)}, u32[]{:S(2)}, u32[]{:S(2)}) collective-permute-start(bf16[512,1024]{1,0:T(8,128)(2,1)S(1)} %constant_dynamic-slice_fusion), channel_id=1, source_target_pairs={{0,2},{1,3},{2,0},{3,1},{4,6},{5,7},{6,4},{7,5},{8,10},{9,11},{10,... | collective-permute-start | bytes 3145736 | tf_op jit(solution)/shard_map/ppermute | solution.py:144
  134.4 90.0 %collective-permute-start.5 = (bf16[512,1024]{1,0:T(8,128)(2,1)S(1)}, bf16[512,1024]{1,0:T(8,128)(2,1)}, u32[]{:S(2)}, u32[]{:S(2)}) collective-permute-start(bf16[512,1024]{1,0:T(8,128)(2,1)S(1)} %constant_dynamic-slice_fusion), channel_id=1, source_target_pairs={{0,3},{1,0},{2,1},{3,2},{4,7},{5,4},{6,5},{7,6},{8,11},{9,8},{10,9... | collective-permute-start | bytes 3145736 | tf_op jit(solution)/shard_map/ppermute | solution.py:144
  149.6 84.0 %collective-permute-start = (bf16[512,512]{1,0:T(8,128)(2,1)S(1)}, bf16[512,512]{1,0:T(8,128)(2,1)S(1)}, u32[]{:S(2)}, u32[]{:S(2)}) collective-permute-start(bf16[512,512]{1,0:T(8,128)(2,1)S(1)} %get-tuple-element.8), channel_id=1, source_target_pairs={{0,1},{1,2},{2,3},{3,0},{4,5},{5,6},{6,7},{7,4},{8,9},{9,10},{10,1... | collective-permute-start | bytes 1572872 | tf_op jit(solution)/shard_map/ppermute | solution.py:144
  200.0 41.6 %copy-start.3 = (bf16[512,1024]{1,0:T(8,128)(2,1)}, bf16[512,1024]{1,0:T(8,128)(2,1)S(1)}, u32[]{:S(2)}) copy-start(bf16[512,1024]{1,0:T(8,128)(2,1)S(1)} %collective-permute-done.3.refs_5_) | copy-start | bytes 3145732
  200.0 46.7 %collective-permute-start.6 = (bf16[512,1024]{1,0:T(8,128)(2,1)S(1)}, bf16[512,1024]{1,0:T(8,128)(2,1)}, u32[]{:S(2)}, u32[]{:S(2)}) collective-permute-start(bf16[512,1024]{1,0:T(8,128)(2,1)S(1)} %collective-permute-done.3.refs_5_), channel_id=1, source_target_pairs={{0,4},{4,0},{1,5},{5,1},{2,6},{6,2},{3,7},{7,3},{8,12},{12,8},{9,1... | collective-permute-start | bytes 3145736 | tf_op jit(solution)/shard_map/ppermute | solution.py:144
  223.6 23.0 %collective-permute-start.7 = (bf16[512,1024]{1,0:T(8,128)(2,1)}, bf16[512,1024]{1,0:T(8,128)(2,1)}, u32[]{:S(2)}, u32[]{:S(2)}) collective-permute-start(bf16[512,1024]{1,0:T(8,128)(2,1)} %collective-permute-done.4.refs_6_), channel_id=1, source_target_pairs={{0,4},{4,0},{1,5},{5,1},{2,6},{6,2},{3,7},{7,3},{8,12},{12,8},{9,1... | collective-permute-start | bytes 3145736 | tf_op jit(solution)/shard_map/ppermute | solution.py:144
  224.4 22.2 %collective-permute-start.8 = (bf16[512,1024]{1,0:T(8,128)(2,1)}, bf16[512,1024]{1,0:T(8,128)(2,1)S(1)}, u32[]{:S(2)}, u32[]{:S(2)}) collective-permute-start(bf16[512,1024]{1,0:T(8,128)(2,1)} %collective-permute-done.5.refs_7_), channel_id=1, source_target_pairs={{0,4},{4,0},{1,5},{5,1},{2,6},{6,2},{3,7},{7,3},{8,12},{12,8},{9,1... | collective-permute-start | bytes 3145736 | tf_op jit(solution)/shard_map/ppermute | solution.py:144
  224.4 20.9 %collective-permute-start.1 = (bf16[512,512]{1,0:T(8,128)(2,1)S(1)}, bf16[512,512]{1,0:T(8,128)(2,1)}, u32[]{:S(2)}, u32[]{:S(2)}) collective-permute-start(bf16[512,512]{1,0:T(8,128)(2,1)S(1)} %get-tuple-element.7), channel_id=1, source_target_pairs={{0,2},{1,3},{2,0},{3,1},{4,6},{5,7},{6,4},{7,5},{8,10},{9,11},{10,... | collective-permute-start | bytes 1572872 | tf_op jit(solution)/shard_map/ppermute | solution.py:144
  233.7 0.8 copy-start.8
  233.7 13.0 %collective-permute-start.2 = (bf16[512,512]{1,0:T(8,128)(2,1)S(1)}, bf16[512,512]{1,0:T(8,128)(2,1)}, u32[]{:S(2)}, u32[]{:S(2)}) collective-permute-start(bf16[512,512]{1,0:T(8,128)(2,1)S(1)} %get-tuple-element.6), channel_id=1, source_target_pairs={{0,3},{1,0},{2,1},{3,2},{4,7},{5,4},{6,5},{7,6},{8,11},{9,8},{10,9... | collective-permute-start | bytes 1572872 | tf_op jit(solution)/shard_map/ppermute | solution.py:144
  246.7 1.0 copy-start.4

commit v3 on v2

--- a/solution.py
+++ b/solution.py
@@ -1,3 +1,5 @@
+import functools
+
 import jax
 import jax.numpy as jnp
 from jax import lax
@@ -15,6 +17,7 @@
 EP = ("ep_0", "ep_1", "ep_2")
 EP_TP = ("ep_0", "ep_1", "ep_2", "tp")
 EPS = 1e-06
+ALL_VMEM = pltpu.CompilerParams(vmem_limit_bytes=67043328)
 SCALE = DK ** (-0.5)
 F32 = jnp.float32
 BF16 = jnp.bfloat16
@@ -53,6 +56,21 @@
 
 def sums_across(a, pick):
     return sum(dot(part, pick) for part in thirds(a))
+
+
+def write_message(ref, h, state, total):
+    whole = jnp.broadcast_to(total, (NOTE, DV))
+    high = whole.astype(BF16).astype(F32)
+    middle = (whole - high).astype(BF16).astype(F32)
+    row = iota((NOTE, DV), 0)
+    note = jnp.where(row == 0, high, jnp.where(row == 1, middle, whole - high - middle))
+    ref[h, :DK] = state.astype(BF16)
+    ref[h, DK:] = note.astype(BF16)
+
+
+def read_message(ref, k, h):
+    note = ref[k, h, DK:].astype(F32)
+    return ref[k, h, :DK].astype(F32), note[0:1] + note[1:2] + note[2:3]
 
 
 def end_state_body(k_ref, v_ref, a_ref, out_ref, state, total):
@@ -86,21 +104,13 @@
 
     @pl.when(step == pl.num_programs(0) - 1)
     def _():
-        parts = DK // 8
         for h in range(n_heads):
-            whole = jnp.broadcast_to(total[h, 0:1, 0:1], (8, DV))
-            high, middle, low = (part.astype(F32) for part in thirds(whole))
-            row = iota((8, DV), 0)
-            note = jnp.where(row == 0, high, jnp.where(row == 1, middle, low))
-            note = jnp.broadcast_to(note[None], (parts, 8, DV))
-            both = jnp.concatenate([state[h].reshape(parts, 8, DV), note], axis=1)
-            out_ref[h * parts : (h + 1) * parts] = both.astype(BF16)
+            write_message(out_ref, h, state[h], total[h, 0:1, 0:1])
 
 
 def end_state(key_rows, value_rows, log_decay):
     n_rows, n_heads = key_rows.shape[0], log_decay.shape[0]
     tile = min(512, n_rows)
-    parts = n_heads * DK // 8
     return pl.pallas_call(
         end_state_body,
         grid=(n_rows // tile,),
@@ -109,8 +119,8 @@
             pl.BlockSpec((tile, n_heads * DV), lambda i: (i, 0)),
             pl.BlockSpec((n_heads, tile), lambda i: (0, i)),
         ],
-        out_specs=pl.BlockSpec((parts, 16, DV), lambda i: (0, 0, 0)),
-        out_shape=jax.ShapeDtypeStruct((parts, 16, DV), BF16),
+        out_specs=pl.BlockSpec((n_heads, DK + NOTE, DV), lambda i: (0, 0, 0)),
+        out_shape=jax.ShapeDtypeStruct((n_heads, DK + NOTE, DV), BF16),
         scratch_shapes=[
             pltpu.VMEM((n_heads, DK, DV), F32),
             pltpu.VMEM((n_heads, 8, 128), F32),
@@ -118,25 +128,54 @@
         cost_estimate=pl.CostEstimate(
             flops=2 * n_rows * n_heads * DK * DV, bytes_accessed=4 << 20, transcendentals=0
         ),
+        compiler_params=ALL_VMEM,
         name="end_state",
     )(key_rows, value_rows, log_decay)
 
 
-def prefix_body(in_ref, out_ref):
-    before = jnp.zeros((8, DV), F32)
-    for j in range(in_ref.shape[0]):
-        out_ref[j] = before.astype(BF16)
-        both = in_ref[j].astype(F32)
-        total = both[8:9] + both[9:10] + both[10:11]
-        before = before * jnp.exp(total) + both[0:8]
-
-
-def prefixes(pieces):
-    return pl.pallas_call(
-        prefix_body,
-        out_shape=jax.ShapeDtypeStruct((pieces.shape[0], 8, DV), BF16),
-        name="prefixes",
-    )(pieces)
+def join_body(axis, peers, first, last, *refs):
+    messages, refs = refs[:peers], refs[peers:]
+    if not first:
+        before_ref, refs = refs[0], refs[1:]
+    ordered = refs[-1]
+    me = lax.axis_index(axis)
+    for d in range(peers):
+        ordered[(me - d + peers) % peers] = messages[d][...]
+    for h in range(refs[0].shape[0]):
+        running, ahead = jnp.zeros((DK, DV), F32), jnp.zeros((DK, DV), F32)
+        total, ahead_total = jnp.zeros((1, DV), F32), jnp.zeros((1, DV), F32)
+        for k in range(peers):
+            ahead = jnp.where(k == me, running, ahead)
+            ahead_total = jnp.where(k == me, total, ahead_total)
+            if last and k == peers - 1:
+                break
+            state, gone = read_message(ordered, k, h)
+            running = running * jnp.exp(gone) + state
+            total = total + gone
+        if not first:
+            gone = before_ref[h, DK : DK + 1]
+            ahead = ahead * jnp.exp(gone) + before_ref[h, :DK]
+            ahead_total = ahead_total + gone
+        refs[0][h, :DK] = ahead
+        refs[0][h, DK:] = jnp.broadcast_to(ahead_total, (8, DV))
+        if not last:
+            write_message(refs[1], h, running, total)
+
+
+def join(axis, messages, before, last):
+    peers = len(messages)
+    n_heads = messages[0].shape[0]
+    out = [jax.ShapeDtypeStruct((n_heads, DK + 8, DV), F32)]
+    if not last:
+        out.append(jax.ShapeDtypeStruct(messages[0].shape, BF16))
+    return pl.pallas_call(
+        functools.partial(join_body, axis, peers, before is None, last),
+        out_shape=out,
+        scratch_shapes=[pltpu.VMEM((peers,) + messages[0].shape, BF16)],
+        cost_estimate=pl.CostEstimate(flops=1 << 22, bytes_accessed=2 << 20, transcendentals=0),
+        compiler_params=ALL_VMEM,
+        name="join",
+    )(*messages, *([] if before is None else [before]))
 
 
 def shift(x, axis, d):
@@ -151,7 +190,7 @@
 def mixer_body(q_ref, k_ref, v_ref, g_ref, a_ref, first_ref, out_ref, state):
     @pl.when(pl.program_id(0) == 0)
     def _():
-        state[...] = first_ref[...].astype(F32).reshape(state.shape)
+        state[...] = first_ref[:, :DK]
 
     n_heads = a_ref.shape[0]
     t, m = iota((BLOCK, BLOCK), 0), iota((BLOCK, BLOCK), 1)
@@ -194,7 +233,7 @@
             pl.BlockSpec((tile, n_heads * DV), lambda i: (i, 0)),
             pl.BlockSpec((tile, n_heads * DV), lambda i: (i, 0)),
             pl.BlockSpec((n_heads, tile), lambda i: (0, i)),
-            pl.BlockSpec((n_heads * DK, DV), lambda i: (0, 0)),
+            pl.BlockSpec((n_heads, DK + 8, DV), lambda i: (0, 0, 0)),
         ],
         out_specs=pl.BlockSpec((tile, n_heads * DV), lambda i: (i, 0)),
         out_shape=jax.ShapeDtypeStruct((n_rows, n_heads * DV), BF16),
@@ -202,6 +241,7 @@
         cost_estimate=pl.CostEstimate(
             flops=12 * n_rows * n_heads * DK * DV, bytes_accessed=8 << 20, transcendentals=0
         ),
+        compiler_params=ALL_VMEM,
         name="mixer",
     )(query_rows, key_rows, value_rows, gate_rows, log_decay, incoming)
 
@@ -210,9 +250,9 @@
     heads, whole, own, other, out_ref, lhs, rhs, sems = (
         refs[:4],
         refs[4],
-        refs[5:8],
-        refs[8:11],
-        *refs[11:],
+        refs[5:9],
+        refs[9:13],
+        *refs[13:],
     )
     x, core = lax.axis_index("tp"), lax.axis_index("ep_2")
     half = rhs.shape[-1]
@@ -221,9 +261,12 @@
         pairs.append((heads[d], lhs.at[d]))
     for side in range(2):
         pairs.append((whole.at[:, side * half : (side + 1) * half], rhs.at[0, side]))
-    for d in range(1, 4):
-        pairs.append((own[d - 1], rhs.at[d, core]))
-        pairs.append((other[d - 1], rhs.at[d, 1 - core]))
+    cut = rhs.shape[2] // 2
+    for parts, side in ((own, core), (other, 1 - core)):
+        pairs.append((parts[0], rhs.at[1, side]))
+        pairs.append((parts[1], rhs.at[2, side, :cut]))
+        pairs.append((parts[2], rhs.at[2, side, cut:]))
+        pairs.append((parts[3], rhs.at[3, side]))
     copies = [
         pltpu.make_async_copy(source, target, sems.at[n])
         for n, (source, target) in enumerate(pairs)
@@ -254,20 +297,23 @@
         scratch_shapes=[
             pltpu.VMEM((groups, n_rows, width), BF16),
             pltpu.VMEM((groups, 2, width, half), BF16),
-            pltpu.SemaphoreType.DMA((12,)),
+            pltpu.SemaphoreType.DMA((14,)),
         ],
         cost_estimate=pl.CostEstimate(
             flops=4 * n_rows * groups * width * half, bytes_accessed=12 << 20, transcendentals=0
         ),
+        compiler_params=ALL_VMEM,
         name="project",
     )(*arrays)
 
 
 def gather_projection(out_proj):
     n_rows, width = out_proj.shape
-    half = width // 2
+    half, cut = width // 2, n_rows // 2
     mine = lax.dynamic_slice(out_proj, (0, lax.axis_index("ep_2") * half), (n_rows, half))
-    own = all_shifts(mine, "tp")[1:]
+    below, above = shift(mine, "tp", 1), shift(mine, "tp", 3)
+    far = [shift(below[:cut], "tp", 1), shift(above[cut:], "tp", 3)]
+    own = [below, *far, above]
     other = [shift(part, "ep_2", 1) for part in own]
     return own, other
 
@@ -291,52 +337,60 @@
     return pl.pallas_call(
         norm_body,
         out_shape=jax.ShapeDtypeStruct((n_tokens + NOTE, width), BF16),
+        compiler_params=ALL_VMEM,
         name="norm",
     )(moe_input, norm_gain.reshape(1, width), routes)
 
 
-def ranked(hits, n_tokens):
+def ranked(hits, n_tokens, none=float(CAP)):
     earlier = iota((n_tokens, n_tokens), 0) < iota((n_tokens, n_tokens), 1)
     rank = dot(hits.astype(BF16), jnp.where(earlier, 1.0, 0.0).astype(BF16))
-    return jnp.where(hits > 0.0, rank, float(CAP)).astype(BF16)
+    return jnp.where(hits > 0.0, rank, none).astype(BF16)
 
 
 def dispatch_body(*refs):
-    messages, out_ref = refs[:-1], refs[-1]
+    messages, out_ref, picks = refs[:-2], refs[-2], refs[-1]
     groups = len(messages)
     n_slots = out_ref.shape[0]
     each = groups * CAP
     experts = n_slots // each
     n_tokens = messages[0].shape[0] - NOTE
-    x = lax.axis_index("tp")
-    expert = (iota((experts, n_tokens), 0) * groups + x).astype(F32)
-    spread = jnp.where(iota((n_slots, experts), 0) // each == iota((n_slots, experts), 1), 1.0, 0.0)
-    spread = spread.astype(BF16)
-    slot = iota((n_slots, n_tokens), 0)
-    place = (slot % CAP).astype(F32)
-    block = (slot // CAP) % groups
-    picks = []
-    for d in range(groups):
-        named = messages[d][n_tokens:, :n_tokens].astype(F32)
-        hits = jnp.zeros((experts, n_tokens), F32)
-        for k in range(4):
-            hits = jnp.where(named[k : k + 1] == expert, 1.0, hits)
-        here = dot(spread, ranked(hits, n_tokens)) == place
-        here = here & (block == (x - d + groups) % groups)
-        picks.append(jnp.where(here, 1.0, 0.0).astype(BF16))
-    for d in range(0, groups, 2):
-        pick = jnp.concatenate([picks[d], picks[d + 1]], axis=1)
-        rows = jnp.concatenate([messages[d][:n_tokens], messages[d + 1][:n_tokens]], axis=0)
-        part = dot(pick, rows)
-        total = part if d == 0 else total + part
-    out_ref[...] = total.astype(BF16)
+
+    @pl.when(pl.program_id(0) == 0)
+    def _():
+        x = lax.axis_index("tp")
+        expert = (iota((experts, n_tokens), 0) * groups + x).astype(F32)
+        shape = (n_slots, experts)
+        low = iota(shape, 1) * each
+        row = iota(shape, 0)
+        owner = jnp.where((row >= low) & (row < low + each), 1.0, 0.0).astype(BF16)
+        slot = iota((n_slots, n_tokens), 0)
+        spot = slot & (each - 1)
+        for d in range(groups):
+            named = messages[d][n_tokens:, :n_tokens].astype(F32)
+            hits = jnp.zeros((experts, n_tokens), F32)
+            for k in range(4):
+                hits = jnp.where(named[k : k + 1] == expert, 1.0, hits)
+            start = ((x - d + groups) % groups) * CAP
+            rank = dot(owner, ranked(hits, n_tokens, 64.0))
+            pick = jnp.where(rank == (spot - start).astype(F32), 1.0, 0.0).astype(BF16)
+            picks[:, d * n_tokens : (d + 1) * n_tokens] = pick
+
+    rows = jnp.concatenate([message[:n_tokens] for message in messages], axis=0)
+    out_ref[...] = dot(picks[...], rows).astype(BF16)
 
 
 def dispatch(messages, n_slots):
-    width = messages[0].shape[1]
+    n_rows, width = messages[0].shape
+    groups, tile = len(messages), width // 4
     return pl.pallas_call(
         dispatch_body,
+        grid=(width // tile,),
+        in_specs=[pl.BlockSpec((n_rows, tile), lambda i: (0, i))] * groups,
+        out_specs=pl.BlockSpec((n_slots, tile), lambda i: (0, i)),
         out_shape=jax.ShapeDtypeStruct((n_slots, width), BF16),
+        scratch_shapes=[pltpu.VMEM((n_slots, groups * (n_rows - NOTE)), BF16)],
+        compiler_params=ALL_VMEM,
         cost_estimate=pl.CostEstimate(
             flops=1024 * n_slots * width, bytes_accessed=6 << 20, transcendentals=0
         ),
@@ -344,9 +398,9 @@
     )(*messages)
 
 
-def weights_body(route_ref, weight_ref, high_ref, low_ref):
+def weights_body(route_ref, weight_ref, out_ref):
     n_visits, n_tokens = route_ref.shape
-    n_slots = high_ref.shape[0]
+    n_slots = out_ref.shape[1]
     experts = n_slots // CAP
     expert = iota((experts, n_tokens), 0)
     hits = jnp.zeros((experts, n_tokens), F32)
@@ -361,15 +415,16 @@
     here = dot(spread, ranked(hits, n_tokens)) == place
     high = weighed.astype(BF16)
     low = (weighed - high.astype(F32)).astype(BF16)
-    high_ref[...] = jnp.where(here, dot(spread, high), 0.0).astype(BF16)
-    low_ref[...] = jnp.where(here, dot(spread, low), 0.0).astype(BF16)
+    out_ref[:n_tokens] = jnp.where(here, dot(spread, high), 0.0).T.astype(BF16)
+    out_ref[n_tokens:] = jnp.where(here, dot(spread, low), 0.0).T.astype(BF16)
 
 
 def slot_weights(routes, route_weights, n_slots):
     n_tokens = routes.shape[1]
     return pl.pallas_call(
         weights_body,
-        out_shape=[jax.ShapeDtypeStruct((n_slots, n_tokens), BF16)] * 2,
+        out_shape=jax.ShapeDtypeStruct((2 * n_tokens, n_slots), BF16),
+        compiler_params=ALL_VMEM,
         cost_estimate=pl.CostEstimate(flops=1 << 27, bytes_accessed=1 << 20, transcendentals=0),
         name="weights",
     )(routes, route_weights)
@@ -384,7 +439,7 @@
 def expert_apply(rows, w_gate, w_up, w_down, dtype, n_rows=None):
     n_rows, width = n_rows or rows.shape[0], rows.shape[1]
     hidden = w_gate.shape[1]
-    tile = min(256, n_rows)
+    tile = min(512, n_rows)
     return pl.pallas_call(
         expert_body,
         grid=(n_rows // tile,),
@@ -399,26 +454,26 @@
         cost_estimate=pl.CostEstimate(
             flops=6 * n_rows * width * hidden, bytes_accessed=14 << 20, transcendentals=0
         ),
+        compiler_params=ALL_VMEM,
         name="expert",
     )(rows, w_gate, w_up, w_down)
 
 
-def combine_body(high_ref, low_ref, rows_ref, shared_ref, out_ref):
-    rows = rows_ref[...]
-    total = dot_tn(high_ref[...], rows) + dot_tn(low_ref[...], rows) + shared_ref[...]
-    out_ref[...] = total.astype(BF16)
-
-
-def combine(high, low, rows, shared):
-    n_slots, n_tokens = high.shape
-    width = rows.shape[1]
+def combine_body(weight_ref, rows_ref, shared_ref, out_ref):
+    both = dot(weight_ref[...], rows_ref[...])
+    n_tokens = out_ref.shape[0]
+    out_ref[...] = (both[:n_tokens] + both[n_tokens:] + shared_ref[...]).astype(BF16)
+
+
+def combine(weights, rows, shared):
+    n_slots, width = rows.shape
+    n_tokens = shared.shape[0]
     tile = width // 4
     return pl.pallas_call(
         combine_body,
         grid=(width // tile,),
         in_specs=[
-            pl.BlockSpec((n_slots, n_tokens), lambda i: (0, 0)),
-            pl.BlockSpec((n_slots, n_tokens), lambda i: (0, 0)),
+            pl.BlockSpec((2 * n_tokens, n_slots), lambda i: (0, 0)),
             pl.BlockSpec((n_slots, tile), lambda i: (0, i)),
             pl.BlockSpec((n_tokens, tile), lambda i: (0, i)),
         ],
@@ -427,8 +482,9 @@
         cost_estimate=pl.CostEstimate(
             flops=4 * n_tokens * n_slots * width, bytes_accessed=6 << 20, transcendentals=0
         ),
+        compiler_params=ALL_VMEM,
         name="combine",
-    )(high, low, rows, shared)
+    )(weights, rows, shared)
 
 
 def exchange(x, axes):
@@ -464,17 +520,19 @@
     message = norm(moe_input, norm_gain, routes)
     messages = all_shifts(message, "tp")
 
-    pieces = end_state(key_rows, value_rows, log_decay)
-    pieces = exchange(pieces, EP)
-    pieces = prefixes(pieces)
-    incoming = exchange(pieces, EP).reshape(-1, DV)
+    state = end_state(key_rows, value_rows, log_decay)
+    before = None
+    for axis in reversed(EP):
+        travelled = all_shifts(state, axis)
+        before, *state = join(axis, travelled, before, axis == EP[0])
+        state = state[0] if state else None
 
     outgoing = dispatch(messages, experts * CAP)
     received = exchange(outgoing.reshape(places, tp * CAP, width), EP)
 
     own, other = gather_projection(out_proj)
 
-    retained = mixer(query_rows, key_rows, value_rows, gate_rows, log_decay, incoming)
+    retained = mixer(query_rows, key_rows, value_rows, gate_rows, log_decay, before)
     retained = retained.reshape(tp, n_rows // tp, -1)
     place = lax.axis_index("tp")
     heads = []
@@ -483,7 +541,7 @@
         heads.append(shift(block, "tp", d))
 
     shared = expert_apply(message, shared_gate, shared_up, shared_down, F32, n_tokens)
-    high, low = slot_weights(routes, route_weights, experts * CAP)
+    weights = slot_weights(routes, route_weights, experts * CAP)
 
     served = expert_apply(
         received.reshape(-1, width), expert_gate[0], expert_up[0], expert_down[0], BF16
@@ -491,7 +549,7 @@
     returned = exchange(served.reshape(experts, CAP, width), EP_TP)
 
     mixer_out = project(retained, heads, out_proj, own, other)
-    moe_out = combine(high, low, returned.reshape(-1, width), shared)
+    moe_out = combine(weights, returned.reshape(-1, width), shared)
     return (mixer_out, moe_out)
 
 

time: 265 us -> 263 us (level)
  blocking collectives: 0 us -> 60.5 us
  waiting for transfers between devices: 123 us -> 75.2 us
  starting transfers between devices: 72.1 us -> 52.1 us
  Pallas kernels: 62 us -> 66.9 us
    all_to_all x0 -> x1, blocking collectives: none -> 60.5 us  [exchange(): return lax.all_to_all(x, axes, split_axis=0, concat_axis=0, tiled=True)]
    all_to_all x4 -> x1, waiting for transfers between devices: 49 us -> 0.01 us  [exchange(): return lax.all_to_all(x, axes, split_axis=0, concat_axis=0, tiled=True)]
    all_to_all x4 -> x1, starting transfers between devices: 35.8 us -> 5.81 us  [exchange(): return lax.all_to_all(x, axes, split_axis=0, concat_axis=0, tiled=True)]
    ppermute x12 -> x21, starting transfers between devices: 36.4 us -> 46.3 us  [shift(): return lax.ppermute(x, axis, [(k, (k + d) % peers) for k in range(peers)])]
    pallas_call x3 -> x5, Pallas kernels: 10.2 us -> 15 us  [the longest x1 6.57 us: dispatch(): pl.pallas_call(dispatch_body, grid=(width // tile,), in_specs=[pl.BlockSp...]
    unnamed x18 -> x4, local copies, waits for them, and re-layouts: 3.46 us -> 0.01 us
    ppermute x12 -> x21, waiting for transfers between devices: 73.8 us -> 75.2 us  [shift(): return lax.ppermute(x, axis, [(k, (k + d) % peers) for k in range(peers)])]
  transfers between devices with their start and end apart: 16 -> 22, of which waited for: 7 -> 9; matrix products, arithmetic and copies ran while one was open for 1% -> 3% of each run, Pallas kernels for 21% -> 16%
where the time goes in v3:
time: 263 us; the launch traced here: 262 us
  waiting for transfers between devices  75.2 us (29%)
  Pallas kernels  66.9 us (25%)
  blocking collectives  60.5 us (23%)
  starting transfers between devices  52.1 us (20%)
  local copies, waits for them, and re-layouts  6.67 us (3%)
    ppermute x21, waiting for transfers between devices, shift(): return lax.ppermute(x, axis, [(k, (k + d) % peers) for k in range(peers)])  75.2 us
    all_to_all x1, blocking collectives, exchange(): return lax.all_to_all(x, axes, split_axis=0, concat_axis=0, tiled=True)  60.5 us
    ppermute x21, starting transfers between devices, shift(): return lax.ppermute(x, axis, [(k, (k + d) % peers) for k in range(peers)])  46.3 us
    pallas_call x2, Pallas kernels, expert_apply(): pl.pallas_call(expert_body, grid=(n_rows // tile,), in_specs=[pl.BlockSpe...  16.9 us
    pallas_call x1, Pallas kernels, mixer(): pl.pallas_call(mixer_body, grid=(n_rows // tile,), in_specs=[pl.BlockSpec...  12.7 us
    pallas_call x1, Pallas kernels, project(): pl.pallas_call(project_body, in_specs=[pl.BlockSpec(memory_space=pl.ANY)]...  9.99 us
    pallas_call x1, Pallas kernels, dispatch(): pl.pallas_call(dispatch_body, grid=(width // tile,), in_specs=[pl.BlockSp...  6.57 us
    pallas_call x3, Pallas kernels, join(): pl.pallas_call(functools.partial(join_body, axis, peers, before is None,...  6.32 us
  transfers between devices with their start and end apart: 22, of which 9 were waited for; matrix products, arithmetic and copies ran while one was open for 3% of the time, Pallas kernels for 16%

profile of v3, /device:TPU:1, one launch (start us, length us, event | category | flops | bytes accessed | tf_op | source)
XLA Modules:
  0.0 262.1 jit_solution(5517571208528792223)
XLA Ops:
  0.6 2.1 norm.1.refs_0_.x_ref
  2.7 2.0 collective-permute-start.18
  4.8 2.5 collective-permute-start.19
  8.4 10.6 %collective-permute-done.18.refs_1_ = bf16[144,2048]{1,0:T(8,128)(2,1)} collective-permute-done((bf16[144,2048]{1,0:T(8,128)(2,1)}, bf16[144,2048]{1,0:T(8,128)(2,1)}, u32[]{:S(2)}, u32[]{:S(2)}) %collective-permute-start.18) | collective-permute-done | bytes 589856 | tf_op jit(solution)/shard_map/ppermute | solution.py:183
  19.0 13.9 %collective-permute-done.19.refs_2_ = bf16[144,2048]{1,0:T(8,128)(2,1)} collective-permute-done((bf16[144,2048]{1,0:T(8,128)(2,1)}, bf16[144,2048]{1,0:T(8,128)(2,1)}, u32[]{:S(2)}, u32[]{:S(2)}) %collective-permute-start.19) | collective-permute-done | bytes 589856 | tf_op jit(solution)/shard_map/ppermute | solution.py:183
  32.9 6.6 %dispatch.1 = bf16[1024,2048]{1,0:T(8,128)(2,1)} custom-call(bf16[144,2048]{1,0:T(8,128)(2,1)} %norm.1.refs_0_.x_ref, bf16[144,2048]{1,0:T(8,128)(2,1)} %collective-permute-done.18.refs_1_, bf16[144,2048]{1,0:T(8,128)(2,1)} %collective-permute-done.19.refs_2_, bf16[144,2048]{1,0:T(8,128)(2,1)} %collective-permute-done.20.refs_3_), custom_call_target="tpu_custom_call" | custom-call | flops 2147483648 | bytes 6291456 | tf_op jit(solution)/shard_map/dispatch/pallas_call | solution.py:386
  39.5 60.5 %all_to_all.10 = bf16[32,32,2048]{2,1,0:T(8,128)(2,1)} all-to-all(bf16[32,32,2048]{2,1,0:T(8,128)(2,1)} %bitcast.20), channel_id=1, replica_groups=mesh['ep_0'=4,'ep_1'=4,'ep_2'=2,'tp'=4] {'ep_0','ep_1','ep_2'}, dimensions={0} | all-to-all | bytes 8388608 | tf_op jit(solution)/shard_map/all_to_all | solution.py:491
  100.0 11.7 %expert.2 = bf16[1024,2048]{1,0:T(8,128)(2,1)} custom-call(bf16[1024,2048]{1,0:T(8,128)(2,1)} %bitcast.21, bf16[2048,512]{1,0:T(8,128)(2,1)} %bitcast.26, bf16[2048,512]{1,0:T(8,128)(2,1)} %bitcast.27, bf16[512,2048]{1,0:T(8,128)(2,1)} %bitcast.28), custom_call_target="tpu_custom_call" | custom-call | flops 6442450944 | bytes 14680064 | tf_op jit(solution)/shard_map/expert/pallas_call | solution.py:443
  111.7 5.8 %all-to-all-start.1 = ((bf16[128,8,2048]{2,1,0:T(8,128)(2,1)}), bf16[128,8,2048]{2,1,0:T(8,128)(2,1)}, u32[]{:S(2)}, u32[]{:S(2)}) async-start(bf16[128,8,2048]{2,1,0:T(8,128)(2,1)} %bitcast.19), calls=%async_computation.1 | async-start | bytes 8388608 | tf_op jit(solution)/shard_map/all_to_all | solution.py:491
  117.5 5.2 %end_state.1.refs_0_ = bf16[2,144,256]{2,1,0:T(8,128)(2,1)} custom-call(bf16[2048,256]{1,0:T(8,128)(2,1)} %k_ref.3, bf16[2048,512]{1,0:T(8,128)(2,1)} %v_ref.3, f32[2,2048]{1,0:T(2,128)} %a_ref.3), custom_call_target="tpu_custom_call" | custom-call | flops 268435456 | bytes 4194304 | tf_op jit(solution)/shard_map/end_state/pallas_call | solution.py:114
  125.2 1.8 join.3
  127.6 2.4 collective-permute-start.2
  131.2 2.3 constant_dynamic-slice_fusion
  136.1 31.4 %collective-permute-done.1.refs_1_ = bf16[2,144,256]{2,1,0:T(8,128)(2,1)} collective-permute-done((bf16[2,144,256]{2,1,0:T(8,128)(2,1)}, bf16[2,144,256]{2,1,0:T(8,128)(2,1)}, u32[]{:S(2)}, u32[]{:S(2)}) %collective-permute-start.1) | collective-permute-done | bytes 147488 | tf_op jit(solution)/shard_map/ppermute | solution.py:183
  167.5 3.8 %collective-permute-done.2.refs_2_ = bf16[2,144,256]{2,1,0:T(8,128)(2,1)} collective-permute-done((bf16[2,144,256]{2,1,0:T(8,128)(2,1)}, bf16[2,144,256]{2,1,0:T(8,128)(2,1)}, u32[]{:S(2)}, u32[]{:S(2)}) %collective-permute-start.2) | collective-permute-done | bytes 147488 | tf_op jit(solution)/shard_map/ppermute | solution.py:183
  171.3 2.3 join.4
  175.1 2.9 %collective-permute-start.5 = (bf16[2,144,256]{2,1,0:T(8,128)(2,1)}, bf16[2,144,256]{2,1,0:T(8,128)(2,1)}, u32[]{:S(2)}, u32[]{:S(2)}) collective-permute-start(bf16[2,144,256]{2,1,0:T(8,128)(2,1)} %get-tuple-element.8.refs_0_), channel_id=1, source_target_pairs={{0,64},{32,96},{64,0},{96,32},{1,65},{33,97},{65,1},{97,33},{2,66}... | collective-permute-start | bytes 442376 | tf_op jit(solution)/shard_map/ppermute | solution.py:183
  180.4 4.1 %collective-permute-done.5.refs_2_ = bf16[2,144,256]{2,1,0:T(8,128)(2,1)} collective-permute-done((bf16[2,144,256]{2,1,0:T(8,128)(2,1)}, bf16[2,144,256]{2,1,0:T(8,128)(2,1)}, u32[]{:S(2)}, u32[]{:S(2)}) %collective-permute-start.5) | collective-permute-done | bytes 147488 | tf_op jit(solution)/shard_map/ppermute | solution.py:183
  184.5 2.2 join.5.first_ref
  186.6 12.7 %mixer.1 = bf16[2048,512]{1,0:T(8,128)(2,1)} custom-call(bf16[2048,256]{1,0:T(8,128)(2,1)} %q_ref.1, bf16[2048,256]{1,0:T(8,128)(2,1)} %k_ref.3, bf16[2048,512]{1,0:T(8,128)(2,1)} %v_ref.3, bf16[2048,512]{1,0:T(8,128)(2,1)} %g_ref.1, f32[2,2048]{1,0:T(2,128)} %a_ref.3, f32[2,136,256]{2,1,0:T(8,128)} %join.5.first_ref), custom_call_target="tpu_custom_call" | custom-call | flops 1610612736 | bytes 8388608 | tf_op jit(solution)/shard_map/mixer/pallas_call | solution.py:227
  199.3 2.3 dynamic-slice_bitcast_fusion
  201.6 1.5 collective-permute-start.7
  203.1 2.2 collective-permute-start.8
  207.5 2.7 %collective-permute-start.13 = (bf16[256,1024]{1,0:T(8,128)(2,1)S(1)}, bf16[256,1024]{1,0:T(8,128)(2,1)}, u32[]{:S(2)}, u32[]{:S(2)}) collective-permute-start(bf16[256,1024]{1,0:T(8,128)(2,1)S(1)} %slice.9), channel_id=1, source_target_pairs={{0,3},{1,0},{2,1},{3,2},{4,7},{5,4},{6,5},{7,6},{8,11},{9,8},{10,9... | collective-permute-start | bytes 1572872 | tf_op jit(solution)/shard_map/ppermute | solution.py:183
  210.2 2.9 %collective-permute-start.14 = (bf16[512,1024]{1,0:T(8,128)(2,1)}, bf16[512,1024]{1,0:T(8,128)(2,1)}, u32[]{:S(2)}, u32[]{:S(2)}) collective-permute-start(bf16[512,1024]{1,0:T(8,128)(2,1)} %collective-permute-done.10.refs_5_), channel_id=1, source_target_pairs={{0,4},{4,0},{1,5},{5,1},{2,6},{6,2},{3,7},{7,3},{8,12},{12,8},{9,1... | collective-permute-start | bytes 3145736 | tf_op jit(solution)/shard_map/ppermute | solution.py:183
  214.4 15.2 %collective-permute-start.17 = (bf16[512,1024]{1,0:T(8,128)(2,1)}, bf16[512,1024]{1,0:T(8,128)(2,1)}, u32[]{:S(2)}, u32[]{:S(2)}) collective-permute-start(bf16[512,1024]{1,0:T(8,128)(2,1)} %collective-permute-done.12.refs_8_), channel_id=1, source_target_pairs={{0,4},{4,0},{1,5},{5,1},{2,6},{6,2},{3,7},{7,3},{8,12},{12,8},{9,1... | collective-permute-start | bytes 3145736 | tf_op jit(solution)/shard_map/ppermute | solution.py:183
  229.6 7.4 %collective-permute-done.11.refs_6_ = bf16[256,1024]{1,0:T(8,128)(2,1)} collective-permute-done((bf16[256,1024]{1,0:T(8,128)(2,1)S(1)}, bf16[256,1024]{1,0:T(8,128)(2,1)}, u32[]{:S(2)}, u32[]{:S(2)}) %collective-permute-start.11) | collective-permute-done | bytes 524320 | tf_op jit(solution)/shard_map/ppermute | solution.py:183
  237.0 2.7 %collective-permute-start.15 = (bf16[256,1024]{1,0:T(8,128)(2,1)}, bf16[256,1024]{1,0:T(8,128)(2,1)}, u32[]{:S(2)}, u32[]{:S(2)}) collective-permute-start(bf16[256,1024]{1,0:T(8,128)(2,1)} %collective-permute-done.11.refs_6_), channel_id=1, source_target_pairs={{0,4},{4,0},{1,5},{5,1},{2,6},{6,2},{3,7},{7,3},{8,12},{12,8},{9,1... | collective-permute-start | bytes 1572872 | tf_op jit(solution)/shard_map/ppermute | solution.py:183
  239.8 2.1 weights.1.weight_ref
  241.9 5.1 %expert.3.shared_ref = f32[128,2048]{1,0:T(8,128)} custom-call(bf16[144,2048]{1,0:T(8,128)(2,1)} %norm.1.refs_0_.x_ref, bf16[2048,512]{1,0:T(8,128)(2,1)} %gate_ref.1, bf16[2048,512]{1,0:T(8,128)(2,1)} %up_ref.1, bf16[512,2048]{1,0:T(8,128)(2,1)} %down_ref.1), custom_call_target="tpu_custom_call" | custom-call | flops 805306368 | bytes 14680064 | tf_op jit(solution)/shard_map/expert/pallas_call | solution.py:443
  247.1 10.0 %project.1 = bf16[512,2048]{1,0:T(8,128)(2,1)} custom-call(bf16[4,512,512]{2,1,0:T(8,128)(2,1)} %bitcast.18, bf16[512,512]{1,0:T(8,128)(2,1)} %copy-done, bf16[512,512]{1,0:T(8,128)(2,1)} %copy-done.1, bf16[512,512]{1,0:T(8,128)(2,1)} %collective-permute-done.9.refs_3_, bf16[512,2048]{1,0:T(8,128)(2,1)} %refs_4_.1, ...), custom_call_target="tpu_custom_call" | custom-call | flops 4294967296 | bytes 12582912 | tf_op jit(solution)/shard_map/project/pallas_call | solution.py:293
  257.1 5.0 %combine.1 = bf16[128,2048]{1,0:T(8,128)(2,1)} custom-call(bf16[256,1024]{1,0:T(8,128)(2,1)} %weights.1.weight_ref, bf16[1024,2048]{1,0:T(8,128)(2,1)} %bitcast.13.rows_ref, f32[128,2048]{1,0:T(8,128)} %expert.3.shared_ref), custom_call_target="tpu_custom_call" | custom-call | flops 1073741824 | bytes 6291456 | tf_op jit(solution)/shard_map/combine/pallas_call | solution.py:472
  (33 shorter events, 15.5 us)
Async XLA Ops:
  2.7 16.3 %collective-permute-start.18 = (bf16[144,2048]{1,0:T(8,128)(2,1)}, bf16[144,2048]{1,0:T(8,128)(2,1)}, u32[]{:S(2)}, u32[]{:S(2)}) collective-permute-start(bf16[144,2048]{1,0:T(8,128)(2,1)} %norm.1.refs_0_.x_ref), channel_id=1, source_target_pairs={{0,1},{1,2},{2,3},{3,0},{4,5},{5,6},{6,7},{7,4},{8,9},{9,10},{10,1... | collective-permute-start | bytes 1769480 | tf_op jit(solution)/shard_map/ppermute | solution.py:183
  4.8 28.2 %collective-permute-start.19 = (bf16[144,2048]{1,0:T(8,128)(2,1)}, bf16[144,2048]{1,0:T(8,128)(2,1)}, u32[]{:S(2)}, u32[]{:S(2)}) collective-permute-start(bf16[144,2048]{1,0:T(8,128)(2,1)} %norm.1.refs_0_.x_ref), channel_id=1, source_target_pairs={{0,2},{1,3},{2,0},{3,1},{4,6},{5,7},{6,4},{7,5},{8,10},{9,11},{10,... | collective-permute-start | bytes 1769480 | tf_op jit(solution)/shard_map/ppermute | solution.py:183
  7.2 25.7 %collective-permute-start.20 = (bf16[144,2048]{1,0:T(8,128)(2,1)}, bf16[144,2048]{1,0:T(8,128)(2,1)}, u32[]{:S(2)}, u32[]{:S(2)}) collective-permute-start(bf16[144,2048]{1,0:T(8,128)(2,1)} %norm.1.refs_0_.x_ref), channel_id=1, source_target_pairs={{0,3},{1,0},{2,1},{3,2},{4,7},{5,4},{6,5},{7,6},{8,11},{9,8},{10,9... | collective-permute-start | bytes 1769480 | tf_op jit(solution)/shard_map/ppermute | solution.py:183
  111.7 145.4 %all-to-all-start.1 = ((bf16[128,8,2048]{2,1,0:T(8,128)(2,1)}), bf16[128,8,2048]{2,1,0:T(8,128)(2,1)}, u32[]{:S(2)}, u32[]{:S(2)}) async-start(bf16[128,8,2048]{2,1,0:T(8,128)(2,1)} %bitcast.19), calls=%async_computation.1 | async-start | bytes 8388608 | tf_op jit(solution)/shard_map/all_to_all | solution.py:491
  122.7 2.5 collective-permute-start
  127.0 40.5 %collective-permute-start.1 = (bf16[2,144,256]{2,1,0:T(8,128)(2,1)}, bf16[2,144,256]{2,1,0:T(8,128)(2,1)}, u32[]{:S(2)}, u32[]{:S(2)}) collective-permute-start(bf16[2,144,256]{2,1,0:T(8,128)(2,1)} %get-tuple-element.6.refs_0_), channel_id=1, source_target_pairs={{0,8},{8,16},{16,24},{24,0},{1,9},{9,17},{17,25},{25,1},{2,10},{10... | collective-permute-start | bytes 442376 | tf_op jit(solution)/shard_map/ppermute | solution.py:183
  127.6 43.7 %collective-permute-start.2 = (bf16[2,144,256]{2,1,0:T(8,128)(2,1)}, bf16[2,144,256]{2,1,0:T(8,128)(2,1)}, u32[]{:S(2)}, u32[]{:S(2)}) collective-permute-start(bf16[2,144,256]{2,1,0:T(8,128)(2,1)} %get-tuple-element.6.refs_0_), channel_id=1, source_target_pairs={{0,16},{8,24},{16,0},{24,8},{1,17},{9,25},{17,1},{25,9},{2,18},{10... | collective-permute-start | bytes 442376 | tf_op jit(solution)/shard_map/ppermute | solution.py:183
  130.1 41.2 %collective-permute-start.3 = (bf16[2,144,256]{2,1,0:T(8,128)(2,1)}, bf16[2,144,256]{2,1,0:T(8,128)(2,1)}, u32[]{:S(2)}, u32[]{:S(2)}) collective-permute-start(bf16[2,144,256]{2,1,0:T(8,128)(2,1)} %get-tuple-element.6.refs_0_), channel_id=1, source_target_pairs={{0,24},{8,0},{16,8},{24,16},{1,25},{9,1},{17,9},{25,17},{2,26},{10... | collective-permute-start | bytes 442376 | tf_op jit(solution)/shard_map/ppermute | solution.py:183
  133.5 71.8 %collective-permute-start.10 = (bf16[512,1024]{1,0:T(8,128)(2,1)}, bf16[512,1024]{1,0:T(8,128)(2,1)}, u32[]{:S(2)}, u32[]{:S(2)}) collective-permute-start(bf16[512,1024]{1,0:T(8,128)(2,1)} %constant_dynamic-slice_fusion), channel_id=1, source_target_pairs={{0,1},{1,2},{2,3},{3,0},{4,5},{5,6},{6,7},{7,4},{8,9},{9,10},{10,1... | collective-permute-start | bytes 3145736 | tf_op jit(solution)/shard_map/ppermute | solution.py:183
  134.7 71.8 %collective-permute-start.12 = (bf16[512,1024]{1,0:T(8,128)(2,1)}, bf16[512,1024]{1,0:T(8,128)(2,1)}, u32[]{:S(2)}, u32[]{:S(2)}) collective-permute-start(bf16[512,1024]{1,0:T(8,128)(2,1)} %constant_dynamic-slice_fusion), channel_id=1, source_target_pairs={{0,3},{1,0},{2,1},{3,2},{4,7},{5,4},{6,5},{7,6},{8,11},{9,8},{10,9... | collective-permute-start | bytes 3145736 | tf_op jit(solution)/shard_map/ppermute | solution.py:183
  173.6 6.8 %collective-permute-start.4 = (bf16[2,144,256]{2,1,0:T(8,128)(2,1)}, bf16[2,144,256]{2,1,0:T(8,128)(2,1)}, u32[]{:S(2)}, u32[]{:S(2)}) collective-permute-start(bf16[2,144,256]{2,1,0:T(8,128)(2,1)} %get-tuple-element.8.refs_0_), channel_id=1, source_target_pairs={{0,32},{32,64},{64,96},{96,0},{1,33},{33,65},{65,97},{97,1},{2,34}... | collective-permute-start | bytes 442376 | tf_op jit(solution)/shard_map/ppermute | solution.py:183
  175.1 9.4 %collective-permute-start.5 = (bf16[2,144,256]{2,1,0:T(8,128)(2,1)}, bf16[2,144,256]{2,1,0:T(8,128)(2,1)}, u32[]{:S(2)}, u32[]{:S(2)}) collective-permute-start(bf16[2,144,256]{2,1,0:T(8,128)(2,1)} %get-tuple-element.8.refs_0_), channel_id=1, source_target_pairs={{0,64},{32,96},{64,0},{96,32},{1,65},{33,97},{65,1},{97,33},{2,66}... | collective-permute-start | bytes 442376 | tf_op jit(solution)/shard_map/ppermute | solution.py:183
  178.0 6.4 %collective-permute-start.6 = (bf16[2,144,256]{2,1,0:T(8,128)(2,1)}, bf16[2,144,256]{2,1,0:T(8,128)(2,1)}, u32[]{:S(2)}, u32[]{:S(2)}) collective-permute-start(bf16[2,144,256]{2,1,0:T(8,128)(2,1)} %get-tuple-element.8.refs_0_), channel_id=1, source_target_pairs={{0,96},{32,0},{64,32},{96,64},{1,97},{33,1},{65,33},{97,65},{2,98}... | collective-permute-start | bytes 442376 | tf_op jit(solution)/shard_map/ppermute | solution.py:183
  201.6 12.9 %collective-permute-start.7 = (bf16[512,512]{1,0:T(8,128)(2,1)S(1)}, bf16[512,512]{1,0:T(8,128)(2,1)S(1)}, u32[]{:S(2)}, u32[]{:S(2)}) collective-permute-start(bf16[512,512]{1,0:T(8,128)(2,1)S(1)} %get-tuple-element.12), channel_id=1, source_target_pairs={{0,1},{1,2},{2,3},{3,0},{4,5},{5,6},{6,7},{7,4},{8,9},{9,10},{10,1... | collective-permute-start | bytes 1572872 | tf_op jit(solution)/shard_map/ppermute | solution.py:183
  203.1 26.6 %collective-permute-start.8 = (bf16[512,512]{1,0:T(8,128)(2,1)S(1)}, bf16[512,512]{1,0:T(8,128)(2,1)S(1)}, u32[]{:S(2)}, u32[]{:S(2)}) collective-permute-start(bf16[512,512]{1,0:T(8,128)(2,1)S(1)} %get-tuple-element.11), channel_id=1, source_target_pairs={{0,2},{1,3},{2,0},{3,1},{4,6},{5,7},{6,4},{7,5},{8,10},{9,11},{10,... | collective-permute-start | bytes 1572872 | tf_op jit(solution)/shard_map/ppermute | solution.py:183
  206.3 30.7 %collective-permute-start.11 = (bf16[256,1024]{1,0:T(8,128)(2,1)S(1)}, bf16[256,1024]{1,0:T(8,128)(2,1)}, u32[]{:S(2)}, u32[]{:S(2)}) collective-permute-start(bf16[256,1024]{1,0:T(8,128)(2,1)S(1)} %slice.8), channel_id=1, source_target_pairs={{0,1},{1,2},{2,3},{3,0},{4,5},{5,6},{6,7},{7,4},{8,9},{9,10},{10,1... | collective-permute-start | bytes 1572872 | tf_op jit(solution)/shard_map/ppermute | solution.py:183
  207.5 32.2 %collective-permute-start.13 = (bf16[256,1024]{1,0:T(8,128)(2,1)S(1)}, bf16[256,1024]{1,0:T(8,128)(2,1)}, u32[]{:S(2)}, u32[]{:S(2)}) collective-permute-start(bf16[256,1024]{1,0:T(8,128)(2,1)S(1)} %slice.9), channel_id=1, source_target_pairs={{0,3},{1,0},{2,1},{3,2},{4,7},{5,4},{6,5},{7,6},{8,11},{9,8},{10,9... | collective-permute-start | bytes 1572872 | tf_op jit(solution)/shard_map/ppermute | solution.py:183
  210.2 36.8 %collective-permute-start.14 = (bf16[512,1024]{1,0:T(8,128)(2,1)}, bf16[512,1024]{1,0:T(8,128)(2,1)}, u32[]{:S(2)}, u32[]{:S(2)}) collective-permute-start(bf16[512,1024]{1,0:T(8,128)(2,1)} %collective-permute-done.10.refs_5_), channel_id=1, source_target_pairs={{0,4},{4,0},{1,5},{5,1},{2,6},{6,2},{3,7},{7,3},{8,12},{12,8},{9,1... | collective-permute-start | bytes 3145736 | tf_op jit(solution)/shard_map/ppermute | solution.py:183
  214.4 25.3 %copy-start = (bf16[512,512]{1,0:T(8,128)(2,1)}, bf16[512,512]{1,0:T(8,128)(2,1)S(1)}, u32[]{:S(2)}) copy-start(bf16[512,512]{1,0:T(8,128)(2,1)S(1)} %collective-permute-done.7.refs_1_) | copy-start | bytes 1572868
  214.4 32.7 %collective-permute-start.17 = (bf16[512,1024]{1,0:T(8,128)(2,1)}, bf16[512,1024]{1,0:T(8,128)(2,1)}, u32[]{:S(2)}, u32[]{:S(2)}) collective-permute-start(bf16[512,1024]{1,0:T(8,128)(2,1)} %collective-permute-done.12.refs_8_), channel_id=1, source_target_pairs={{0,4},{4,0},{1,5},{5,1},{2,6},{6,2},{3,7},{7,3},{8,12},{12,8},{9,1... | collective-permute-start | bytes 3145736 | tf_op jit(solution)/shard_map/ppermute | solution.py:183
  229.6 10.2 %copy-start.1 = (bf16[512,512]{1,0:T(8,128)(2,1)}, bf16[512,512]{1,0:T(8,128)(2,1)S(1)}, u32[]{:S(2)}) copy-start(bf16[512,512]{1,0:T(8,128)(2,1)S(1)} %collective-permute-done.8.refs_2_) | copy-start | bytes 1572868
  229.6 17.4 %collective-permute-start.9 = (bf16[512,512]{1,0:T(8,128)(2,1)}, bf16[512,512]{1,0:T(8,128)(2,1)}, u32[]{:S(2)}, u32[]{:S(2)}) collective-permute-start(bf16[512,512]{1,0:T(8,128)(2,1)} %get-tuple-element.10), channel_id=1, source_target_pairs={{0,3},{1,0},{2,1},{3,2},{4,7},{5,4},{6,5},{7,6},{8,11},{9,8},{10,9... | collective-permute-start | bytes 1572872 | tf_op jit(solution)/shard_map/ppermute | solution.py:183
  237.0 10.1 %collective-permute-start.15 = (bf16[256,1024]{1,0:T(8,128)(2,1)}, bf16[256,1024]{1,0:T(8,128)(2,1)}, u32[]{:S(2)}, u32[]{:S(2)}) collective-permute-start(bf16[256,1024]{1,0:T(8,128)(2,1)} %collective-permute-done.11.refs_6_), channel_id=1, source_target_pairs={{0,4},{4,0},{1,5},{5,1},{2,6},{6,2},{3,7},{7,3},{8,12},{12,8},{9,1... | collective-permute-start | bytes 1572872 | tf_op jit(solution)/shard_map/ppermute | solution.py:183
  239.7 7.4 %collective-permute-start.16 = (bf16[256,1024]{1,0:T(8,128)(2,1)}, bf16[256,1024]{1,0:T(8,128)(2,1)}, u32[]{:S(2)}, u32[]{:S(2)}) collective-permute-start(bf16[256,1024]{1,0:T(8,128)(2,1)} %collective-permute-done.13.refs_7_), channel_id=1, source_target_pairs={{0,4},{4,0},{1,5},{5,1},{2,6},{6,2},{3,7},{7,3},{8,12},{12,8},{9,1... | collective-permute-start | bytes 1572872 | tf_op jit(solution)/shard_map/ppermute | solution.py:183

commit v4 on v3

--- a/solution.py
+++ b/solution.py
@@ -14,6 +14,7 @@
 BLOCK = 128
 CAP = 8
 NOTE = 16
+ROUTE = 8
 EP = ("ep_0", "ep_1", "ep_2")
 EP_TP = ("ep_0", "ep_1", "ep_2", "tp")
 EPS = 1e-06
@@ -58,22 +59,20 @@
     return sum(dot(part, pick) for part in thirds(a))
 
 
-def write_message(ref, h, state, total):
+def write_message(ref, state, total):
     whole = jnp.broadcast_to(total, (NOTE, DV))
-    high = whole.astype(BF16).astype(F32)
-    middle = (whole - high).astype(BF16).astype(F32)
+    high, middle, low = (part.astype(F32) for part in thirds(whole))
     row = iota((NOTE, DV), 0)
-    note = jnp.where(row == 0, high, jnp.where(row == 1, middle, whole - high - middle))
-    ref[h, :DK] = state.astype(BF16)
-    ref[h, DK:] = note.astype(BF16)
-
-
-def read_message(ref, k, h):
-    note = ref[k, h, DK:].astype(F32)
-    return ref[k, h, :DK].astype(F32), note[0:1] + note[1:2] + note[2:3]
-
-
-def end_state_body(k_ref, v_ref, a_ref, out_ref, state, total):
+    ref[:DK] = state.astype(BF16)
+    ref[DK:] = jnp.where(row == 0, high, jnp.where(row == 1, middle, low)).astype(BF16)
+
+
+def read_message(ref):
+    note = ref[DK:].astype(F32)
+    return ref[:DK].astype(F32), note[0:1] + note[1:2] + note[2:3]
+
+
+def end_state_body(k_ref, v_ref, a_ref, keep_ref, give_ref, state, total):
     step = pl.program_id(0)
 
     @pl.when(step == 0)
@@ -104,8 +103,9 @@
 
     @pl.when(step == pl.num_programs(0) - 1)
     def _():
-        for h in range(n_heads):
-            write_message(out_ref, h, state[h], total[h, 0:1, 0:1])
+        core = lax.axis_index("ep_2")
+        write_message(keep_ref, state[core], total[core][0:1, 0:1])
+        write_message(give_ref, state[1 - core], total[1 - core][0:1, 0:1])
 
 
 def end_state(key_rows, value_rows, log_decay):
@@ -119,8 +119,8 @@
             pl.BlockSpec((tile, n_heads * DV), lambda i: (i, 0)),
             pl.BlockSpec((n_heads, tile), lambda i: (0, i)),
         ],
-        out_specs=pl.BlockSpec((n_heads, DK + NOTE, DV), lambda i: (0, 0, 0)),
-        out_shape=jax.ShapeDtypeStruct((n_heads, DK + NOTE, DV), BF16),
+        out_specs=[pl.BlockSpec((DK + NOTE, DV), lambda i: (0, 0))] * 2,
+        out_shape=[jax.ShapeDtypeStruct((DK + NOTE, DV), BF16)] * 2,
         scratch_shapes=[
             pltpu.VMEM((n_heads, DK, DV), F32),
             pltpu.VMEM((n_heads, 8, 128), F32),
@@ -133,49 +133,88 @@
     )(key_rows, value_rows, log_decay)
 
 
-def join_body(axis, peers, first, last, *refs):
-    messages, refs = refs[:peers], refs[peers:]
-    if not first:
-        before_ref, refs = refs[0], refs[1:]
-    ordered = refs[-1]
-    me = lax.axis_index(axis)
+def join_cores_body(keep_ref, got_ref, out_ref):
+    core = lax.axis_index("ep_2")
+    keep, kept = read_message(keep_ref)
+    got, gone = read_message(got_ref)
+    first = core == 0
+    joined = jnp.where(first, keep * jnp.exp(gone) + got, got * jnp.exp(kept) + keep)
+    write_message(out_ref, joined, kept + gone)
+
+
+def join_cores(keep, got):
+    return pl.pallas_call(
+        join_cores_body,
+        out_shape=jax.ShapeDtypeStruct(keep.shape, BF16),
+        compiler_params=ALL_VMEM,
+        name="join_cores",
+    )(keep, got)
+
+
+def join(axis, messages, ordered):
+    peers, me = len(messages), lax.axis_index(axis)
     for d in range(peers):
         ordered[(me - d + peers) % peers] = messages[d][...]
-    for h in range(refs[0].shape[0]):
-        running, ahead = jnp.zeros((DK, DV), F32), jnp.zeros((DK, DV), F32)
-        total, ahead_total = jnp.zeros((1, DV), F32), jnp.zeros((1, DV), F32)
-        for k in range(peers):
-            ahead = jnp.where(k == me, running, ahead)
-            ahead_total = jnp.where(k == me, total, ahead_total)
-            if last and k == peers - 1:
-                break
-            state, gone = read_message(ordered, k, h)
-            running = running * jnp.exp(gone) + state
-            total = total + gone
-        if not first:
-            gone = before_ref[h, DK : DK + 1]
-            ahead = ahead * jnp.exp(gone) + before_ref[h, :DK]
-            ahead_total = ahead_total + gone
-        refs[0][h, :DK] = ahead
-        refs[0][h, DK:] = jnp.broadcast_to(ahead_total, (8, DV))
-        if not last:
-            write_message(refs[1], h, running, total)
-
-
-def join(axis, messages, before, last):
-    peers = len(messages)
-    n_heads = messages[0].shape[0]
-    out = [jax.ShapeDtypeStruct((n_heads, DK + 8, DV), F32)]
-    if not last:
-        out.append(jax.ShapeDtypeStruct(messages[0].shape, BF16))
-    return pl.pallas_call(
-        functools.partial(join_body, axis, peers, before is None, last),
-        out_shape=out,
-        scratch_shapes=[pltpu.VMEM((peers,) + messages[0].shape, BF16)],
-        cost_estimate=pl.CostEstimate(flops=1 << 22, bytes_accessed=2 << 20, transcendentals=0),
-        compiler_params=ALL_VMEM,
-        name="join",
-    )(*messages, *([] if before is None else [before]))
+    running, ahead = jnp.zeros((DK, DV), F32), jnp.zeros((DK, DV), F32)
+    total, ahead_total = jnp.zeros((1, DV), F32), jnp.zeros((1, DV), F32)
+    for k in range(peers):
+        ahead = jnp.where(k == me, running, ahead)
+        ahead_total = jnp.where(k == me, total, ahead_total)
+        state, gone = read_message(ordered.at[k])
+        running = running * jnp.exp(gone) + state
+        total = total + gone
+    return ahead, ahead_total, running, total
+
+
+def join_plane_body(*refs):
+    messages, (before_ref, all_ref, ordered) = refs[:-3], refs[-3:]
+    ahead, gone, running, total = join("ep_1", messages, ordered)
+    before_ref[:DK] = ahead
+    before_ref[DK:] = jnp.broadcast_to(gone, (8, DV))
+    write_message(all_ref, running, total)
+
+
+def join_plane(messages):
+    shape = messages[0].shape
+    return pl.pallas_call(
+        join_plane_body,
+        out_shape=[
+            jax.ShapeDtypeStruct((DK + 8, DV), F32),
+            jax.ShapeDtypeStruct(shape, BF16),
+        ],
+        scratch_shapes=[pltpu.VMEM((len(messages),) + shape, BF16)],
+        compiler_params=ALL_VMEM,
+        cost_estimate=pl.CostEstimate(flops=1 << 22, bytes_accessed=1 << 20, transcendentals=0),
+        name="join_plane",
+    )(*messages)
+
+
+def join_last_body(*refs):
+    messages, (before_ref, keep_ref, got_ref, mine_ref, theirs_ref, ordered) = refs[:-6], refs[-6:]
+    ahead, _, _, _ = join("ep_0", messages, ordered)
+    gone = before_ref[DK : DK + 1]
+    first = ahead * jnp.exp(gone) + before_ref[:DK]
+    keep, kept = read_message(keep_ref)
+    got, gone = read_message(got_ref)
+    low = lax.axis_index("ep_2") == 0
+    second = first * jnp.exp(jnp.where(low, kept, gone)) + jnp.where(low, keep, got)
+    mine_ref[...] = jnp.where(low, first, second)
+    theirs_ref[...] = jnp.where(low, second, first).astype(BF16)
+
+
+def join_last(messages, before, keep, got):
+    shape = messages[0].shape
+    return pl.pallas_call(
+        join_last_body,
+        out_shape=[
+            jax.ShapeDtypeStruct((DK, DV), F32),
+            jax.ShapeDtypeStruct((DK, DV), BF16),
+        ],
+        scratch_shapes=[pltpu.VMEM((len(messages),) + shape, BF16)],
+        compiler_params=ALL_VMEM,
+        cost_estimate=pl.CostEstimate(flops=1 << 22, bytes_accessed=1 << 20, transcendentals=0),
+        name="join_last",
+    )(*messages, before, keep, got)
 
 
 def shift(x, axis, d):
@@ -187,10 +226,12 @@
     return [x] + [shift(x, axis, d) for d in range(1, lax.axis_size(axis))]
 
 
-def mixer_body(q_ref, k_ref, v_ref, g_ref, a_ref, first_ref, out_ref, state):
+def mixer_body(q_ref, k_ref, v_ref, g_ref, a_ref, mine_ref, theirs_ref, out_ref, state):
     @pl.when(pl.program_id(0) == 0)
     def _():
-        state[...] = first_ref[:, :DK]
+        core = lax.axis_index("ep_2")
+        state[core] = mine_ref[...]
+        state[1 - core] = theirs_ref[...].astype(F32)
 
     n_heads = a_ref.shape[0]
     t, m = iota((BLOCK, BLOCK), 0), iota((BLOCK, BLOCK), 1)
@@ -221,7 +262,7 @@
             out_ref[rows, h * DV : (h + 1) * DV] = (silu(gate) * normed).astype(BF16)
 
 
-def mixer(query_rows, key_rows, value_rows, gate_rows, log_decay, incoming):
+def mixer(query_rows, key_rows, value_rows, gate_rows, log_decay, mine, theirs):
     n_rows, n_heads = query_rows.shape[0], log_decay.shape[0]
     tile = min(256, n_rows)
     return pl.pallas_call(
@@ -233,7 +274,8 @@
             pl.BlockSpec((tile, n_heads * DV), lambda i: (i, 0)),
             pl.BlockSpec((tile, n_heads * DV), lambda i: (i, 0)),
             pl.BlockSpec((n_heads, tile), lambda i: (0, i)),
-            pl.BlockSpec((n_heads, DK + 8, DV), lambda i: (0, 0, 0)),
+            pl.BlockSpec((DK, DV), lambda i: (0, 0)),
+            pl.BlockSpec((DK, DV), lambda i: (0, 0)),
         ],
         out_specs=pl.BlockSpec((tile, n_heads * DV), lambda i: (i, 0)),
         out_shape=jax.ShapeDtypeStruct((n_rows, n_heads * DV), BF16),
@@ -243,7 +285,7 @@
         ),
         compiler_params=ALL_VMEM,
         name="mixer",
-    )(query_rows, key_rows, value_rows, gate_rows, log_decay, incoming)
+    )(query_rows, key_rows, value_rows, gate_rows, log_decay, mine, theirs)
 
 
 def project_body(*refs):
@@ -323,12 +365,12 @@
     n_tokens = x.shape[0]
     mean = jnp.mean(x * x, axis=1, keepdims=True)
     out_ref[:n_tokens] = (x * lax.rsqrt(mean + EPS) * gain_ref[...]).astype(BF16)
-    row = iota((NOTE, n_tokens), 0)
-    note = jnp.zeros((NOTE, n_tokens), F32)
+    row = iota((ROUTE, n_tokens), 0)
+    note = jnp.zeros((ROUTE, n_tokens), F32)
     for k in range(route_ref.shape[0]):
         note = jnp.where(row == k, route_ref[k : k + 1].astype(F32), note)
     out_ref[n_tokens:, :n_tokens] = note.astype(BF16)
-    rest = (NOTE, x.shape[1] - n_tokens)
+    rest = (ROUTE, x.shape[1] - n_tokens)
     out_ref[n_tokens:, n_tokens:] = jnp.zeros(rest, BF16)
 
 
@@ -336,7 +378,7 @@
     n_tokens, width = moe_input.shape
     return pl.pallas_call(
         norm_body,
-        out_shape=jax.ShapeDtypeStruct((n_tokens + NOTE, width), BF16),
+        out_shape=jax.ShapeDtypeStruct((n_tokens + ROUTE, width), BF16),
         compiler_params=ALL_VMEM,
         name="norm",
     )(moe_input, norm_gain.reshape(1, width), routes)
@@ -348,54 +390,68 @@
     return jnp.where(hits > 0.0, rank, none).astype(BF16)
 
 
-def dispatch_body(*refs):
-    messages, out_ref, picks = refs[:-2], refs[-2], refs[-1]
-    groups = len(messages)
-    n_slots = out_ref.shape[0]
-    each = groups * CAP
-    experts = n_slots // each
-    n_tokens = messages[0].shape[0] - NOTE
-
-    @pl.when(pl.program_id(0) == 0)
-    def _():
-        x = lax.axis_index("tp")
-        expert = (iota((experts, n_tokens), 0) * groups + x).astype(F32)
-        shape = (n_slots, experts)
-        low = iota(shape, 1) * each
-        row = iota(shape, 0)
-        owner = jnp.where((row >= low) & (row < low + each), 1.0, 0.0).astype(BF16)
-        slot = iota((n_slots, n_tokens), 0)
-        spot = slot & (each - 1)
-        for d in range(groups):
-            named = messages[d][n_tokens:, :n_tokens].astype(F32)
-            hits = jnp.zeros((experts, n_tokens), F32)
-            for k in range(4):
-                hits = jnp.where(named[k : k + 1] == expert, 1.0, hits)
-            start = ((x - d + groups) % groups) * CAP
-            rank = dot(owner, ranked(hits, n_tokens, 64.0))
-            pick = jnp.where(rank == (spot - start).astype(F32), 1.0, 0.0).astype(BF16)
-            picks[:, d * n_tokens : (d + 1) * n_tokens] = pick
-
-    rows = jnp.concatenate([message[:n_tokens] for message in messages], axis=0)
-    out_ref[...] = dot(picks[...], rows).astype(BF16)
-
-
-def dispatch(messages, n_slots):
-    n_rows, width = messages[0].shape
-    groups, tile = len(messages), width // 4
-    return pl.pallas_call(
-        dispatch_body,
-        grid=(width // tile,),
-        in_specs=[pl.BlockSpec((n_rows, tile), lambda i: (0, i))] * groups,
-        out_specs=pl.BlockSpec((n_slots, tile), lambda i: (0, i)),
-        out_shape=jax.ShapeDtypeStruct((n_slots, width), BF16),
-        scratch_shapes=[pltpu.VMEM((n_slots, groups * (n_rows - NOTE)), BF16)],
+def slot_owners(n_slots):
+    shape = (n_slots, n_slots // CAP)
+    return jnp.where(iota(shape, 0) // CAP == iota(shape, 1), 1.0, 0.0).astype(BF16)
+
+
+def picks_of(note, n_slots):
+    n_tokens = note.shape[1]
+    experts = n_slots // CAP
+    line = lax.axis_size("tp")
+    expert = (iota((experts, n_tokens), 0) * line + lax.axis_index("tp")).astype(F32)
+    hits = jnp.zeros((experts, n_tokens), F32)
+    for k in range(4):
+        hits = jnp.where(note[k : k + 1] == expert, 1.0, hits)
+    place = (iota((n_slots, n_tokens), 0) & (CAP - 1)).astype(F32)
+    here = dot(slot_owners(n_slots), ranked(hits, n_tokens)) == place
+    return jnp.where(here, 1.0, 0.0).astype(BF16)
+
+
+def dispatch_body(shifts, *refs):
+    n = len(shifts)
+    messages, (out_ref, held, made, sems) = refs[:n], refs[-4:]
+    experts, line, _, width = out_ref.shape
+    n_tokens = held.shape[1] - ROUTE
+    me = lax.axis_index("tp")
+    arrive, leave = [], []
+    for i, d in enumerate(shifts):
+        to = out_ref.at[:, (me - d + line) % line]
+        arrive.append(pltpu.make_async_copy(messages[i], held.at[i], sems.at[0, i]))
+        leave.append(pltpu.make_async_copy(made.at[i], to, sems.at[1, i]))
+    for copy in arrive:
+        copy.start()
+    for i in range(n):
+        arrive[i].wait()
+        pick = picks_of(held[i, n_tokens:, :n_tokens].astype(F32), experts * CAP)
+        rows = dot(pick, held[i, :n_tokens])
+        made[i] = rows.reshape(experts, CAP, width).astype(BF16)
+        leave[i].start()
+    for copy in leave:
+        copy.wait()
+
+
+def dispatch(messages, shifts, experts, outgoing=None):
+    n, (n_rows, width) = len(messages), messages[0].shape
+    arrays = list(messages) + ([] if outgoing is None else [outgoing])
+    shape = (experts, lax.axis_size("tp"), CAP, width)
+    return pl.pallas_call(
+        functools.partial(dispatch_body, shifts),
+        in_specs=[pl.BlockSpec(memory_space=pl.ANY)] * len(arrays),
+        out_specs=pl.BlockSpec(memory_space=pl.ANY),
+        out_shape=jax.ShapeDtypeStruct(shape, BF16),
+        scratch_shapes=[
+            pltpu.VMEM((n, n_rows, width), BF16),
+            pltpu.VMEM((n, experts, CAP, width), BF16),
+            pltpu.SemaphoreType.DMA((2, n)),
+        ],
+        input_output_aliases={} if outgoing is None else {n: 0},
         compiler_params=ALL_VMEM,
         cost_estimate=pl.CostEstimate(
-            flops=1024 * n_slots * width, bytes_accessed=6 << 20, transcendentals=0
+            flops=256 * n * experts * CAP * width, bytes_accessed=2 * n << 20, transcendentals=0
         ),
         name="dispatch",
-    )(*messages)
+    )(*arrays)
 
 
 def weights_body(route_ref, weight_ref, out_ref):
@@ -468,7 +524,7 @@
 def combine(weights, rows, shared):
     n_slots, width = rows.shape
     n_tokens = shared.shape[0]
-    tile = width // 4
+    tile = width // 2
     return pl.pallas_call(
         combine_body,
         grid=(width // tile,),
@@ -520,19 +576,22 @@
     message = norm(moe_input, norm_gain, routes)
     messages = all_shifts(message, "tp")
 
-    state = end_state(key_rows, value_rows, log_decay)
-    before = None
-    for axis in reversed(EP):
-        travelled = all_shifts(state, axis)
-        before, *state = join(axis, travelled, before, axis == EP[0])
-        state = state[0] if state else None
-
-    outgoing = dispatch(messages, experts * CAP)
+    keep, give = end_state(key_rows, value_rows, log_decay)
+    got = shift(give, "ep_2", 1)
+    pair = join_cores(keep, got)
+    pairs = all_shifts(pair, "ep_1")
+    before, plane = join_plane(pairs)
+    planes = all_shifts(plane, "ep_0")
+    mine, give = join_last(planes, before, keep, got)
+    theirs = shift(give, "ep_2", 1)
+
+    outgoing = dispatch(messages[:1], (0,), places)
+    outgoing = dispatch(messages[1:], (1, 2, 3), places, outgoing)
     received = exchange(outgoing.reshape(places, tp * CAP, width), EP)
 
     own, other = gather_projection(out_proj)
 
-    retained = mixer(query_rows, key_rows, value_rows, gate_rows, log_decay, before)
+    retained = mixer(query_rows, key_rows, value_rows, gate_rows, log_decay, mine, theirs)
     retained = retained.reshape(tp, n_rows // tp, -1)
     place = lax.axis_index("tp")
     heads = []

time: 263 us -> 258 us (0.981)
  starting transfers between devices: 52.1 us -> 48.8 us
    ppermute x21 -> x22, starting transfers between devices: 46.3 us -> 42.9 us  [shift(): return lax.ppermute(x, axis, [(k, (k + d) % peers) for k in range(peers)])]
    pallas_call x5 -> x6, Pallas kernels: 15 us -> 14.2 us  [the longest x2 6.81 us: dispatch(): pl.pallas_call(functools.partial(dispatch_body, shifts), in_specs=[pl.Blo...]
    ppermute x21 -> x22, waiting for transfers between devices: 75.2 us -> 75 us  [shift(): return lax.ppermute(x, axis, [(k, (k + d) % peers) for k in range(peers)])]
  transfers between devices with their start and end apart: 22 -> 23, of which waited for: 9 -> 11; matrix products, arithmetic and copies ran while one was open for 3% -> 3% of each run, Pallas kernels for 16% -> 17%
where the time goes in v4:
time: 258 us; the launch traced here: 257 us
  waiting for transfers between devices  75 us (29%)
  Pallas kernels  65.7 us (25%)
  blocking collectives  60.5 us (23%)
  starting transfers between devices  48.8 us (19%)
  local copies, waits for them, and re-layouts  6.67 us (3%)
    ppermute x22, waiting for transfers between devices, shift(): return lax.ppermute(x, axis, [(k, (k + d) % peers) for k in range(peers)])  75 us
    all_to_all x1, blocking collectives, exchange(): return lax.all_to_all(x, axes, split_axis=0, concat_axis=0, tiled=True)  60.5 us
    ppermute x22, starting transfers between devices, shift(): return lax.ppermute(x, axis, [(k, (k + d) % peers) for k in range(peers)])  42.9 us
    pallas_call x2, Pallas kernels, expert_apply(): pl.pallas_call(expert_body, grid=(n_rows // tile,), in_specs=[pl.BlockSpe...  16.9 us
    pallas_call x1, Pallas kernels, mixer(): pl.pallas_call(mixer_body, grid=(n_rows // tile,), in_specs=[pl.BlockSpec...  12.7 us
    pallas_call x1, Pallas kernels, project(): pl.pallas_call(project_body, in_specs=[pl.BlockSpec(memory_space=pl.ANY)]...  9.96 us
    pallas_call x2, Pallas kernels, dispatch(): pl.pallas_call(functools.partial(dispatch_body, shifts), in_specs=[pl.Blo...  6.81 us
    all_to_all x1, starting transfers between devices, exchange(): return lax.all_to_all(x, axes, split_axis=0, concat_axis=0, tiled=True)  5.87 us
  transfers between devices with their start and end apart: 23, of which 11 were waited for; matrix products, arithmetic and copies ran while one was open for 3% of the time, Pallas kernels for 17%

profile of v4, /device:TPU:1, one launch (start us, length us, event | category | flops | bytes accessed | tf_op | source)
XLA Modules:
  0.0 257.4 jit_solution(2701525492527422947)
XLA Ops:
  0.6 2.1 norm.1.refs_0_.x_ref
  2.7 2.0 collective-permute-start.19
  4.8 2.5 collective-permute-start.20
  8.4 2.7 %dispatch.2.refs_3_ = bf16[32,4,8,2048]{3,2,1,0:T(8,128)(2,1)} custom-call(bf16[136,2048]{1,0:T(8,128)(2,1)} %norm.1.refs_0_.x_ref), custom_call_target="tpu_custom_call" | custom-call | flops 134217728 | bytes 2097152 | tf_op jit(solution)/shard_map/dispatch/pallas_call | solution.py:438
  11.1 7.2 %collective-permute-done.19.refs_0_ = bf16[136,2048]{1,0:T(8,128)(2,1)} collective-permute-done((bf16[136,2048]{1,0:T(8,128)(2,1)}, bf16[136,2048]{1,0:T(8,128)(2,1)}, u32[]{:S(2)}, u32[]{:S(2)}) %collective-permute-start.19) | collective-permute-done | bytes 557088 | tf_op jit(solution)/shard_map/ppermute | solution.py:222
  18.3 13.2 %collective-permute-done.20.refs_1_ = bf16[136,2048]{1,0:T(8,128)(2,1)} collective-permute-done((bf16[136,2048]{1,0:T(8,128)(2,1)}, bf16[136,2048]{1,0:T(8,128)(2,1)}, u32[]{:S(2)}, u32[]{:S(2)}) %collective-permute-start.20) | collective-permute-done | bytes 557088 | tf_op jit(solution)/shard_map/ppermute | solution.py:222
  31.5 4.1 %dispatch.3 = bf16[32,4,8,2048]{3,2,1,0:T(8,128)(2,1)} custom-call(bf16[136,2048]{1,0:T(8,128)(2,1)} %collective-permute-done.19.refs_0_, bf16[136,2048]{1,0:T(8,128)(2,1)} %collective-permute-done.20.refs_1_, bf16[136,2048]{1,0:T(8,128)(2,1)} %collective-permute-done.21.refs_2_, ...), custom_call_target="tpu_custom_call", output_to_operand_aliasing={{}: (3, {})} | custom-call | flops 402653184 | bytes 6291456 | tf_op jit(solution)/shard_map/dispatch/pallas_call | solution.py:438
  35.6 60.5 %all_to_all.10 = bf16[32,32,2048]{2,1,0:T(8,128)(2,1)} all-to-all(bf16[32,32,2048]{2,1,0:T(8,128)(2,1)} %bitcast.17), channel_id=1, replica_groups=mesh['ep_0'=4,'ep_1'=4,'ep_2'=2,'tp'=4] {'ep_0','ep_1','ep_2'}, dimensions={0} | all-to-all | bytes 8388608 | tf_op jit(solution)/shard_map/all_to_all | solution.py:547
  96.1 11.7 %expert.2 = bf16[1024,2048]{1,0:T(8,128)(2,1)} custom-call(bf16[1024,2048]{1,0:T(8,128)(2,1)} %bitcast.21, bf16[2048,512]{1,0:T(8,128)(2,1)} %bitcast.26, bf16[2048,512]{1,0:T(8,128)(2,1)} %bitcast.27, bf16[512,2048]{1,0:T(8,128)(2,1)} %bitcast.28), custom_call_target="tpu_custom_call" | custom-call | flops 6442450944 | bytes 14680064 | tf_op jit(solution)/shard_map/expert/pallas_call | solution.py:499
  107.8 5.9 %all-to-all-start.1 = ((bf16[128,8,2048]{2,1,0:T(8,128)(2,1)}), bf16[128,8,2048]{2,1,0:T(8,128)(2,1)}, u32[]{:S(2)}, u32[]{:S(2)}) async-start(bf16[128,8,2048]{2,1,0:T(8,128)(2,1)} %bitcast.20), calls=%async_computation.1 | async-start | bytes 8388608 | tf_op jit(solution)/shard_map/all_to_all | solution.py:547
  113.7 5.2 %end_state.1 = (bf16[144,256]{1,0:T(8,128)(2,1)}, bf16[144,256]{1,0:T(8,128)(2,1)}) custom-call(bf16[2048,256]{1,0:T(8,128)(2,1)} %k_ref.3, bf16[2048,512]{1,0:T(8,128)(2,1)} %v_ref.3, f32[2,2048]{1,0:T(2,128)} %a_ref.3), custom_call_target="tpu_custom_call" | custom-call | flops 268435456 | bytes 4194304 | tf_op jit(solution)/shard_map/end_state/pallas_call | solution.py:114
  120.0 2.3 constant_dynamic-slice_fusion
  122.9 2.1 collective-permute-start.13
  127.2 2.4 collective-permute-start.2
  130.8 30.8 %collective-permute-done.1.refs_1_ = bf16[144,256]{1,0:T(8,128)(2,1)} collective-permute-done((bf16[144,256]{1,0:T(8,128)(2,1)}, bf16[144,256]{1,0:T(8,128)(2,1)}, u32[]{:S(2)}, u32[]{:S(2)}) %collective-permute-start.1) | collective-permute-done | bytes 73760 | tf_op jit(solution)/shard_map/ppermute | solution.py:222
  161.6 2.4 collective-permute-done.2.refs_2_
  167.2 2.9 %collective-permute-start.5 = (bf16[144,256]{1,0:T(8,128)(2,1)}, bf16[144,256]{1,0:T(8,128)(2,1)}, u32[]{:S(2)}, u32[]{:S(2)}) collective-permute-start(bf16[144,256]{1,0:T(8,128)(2,1)} %get-tuple-element.10.refs_0_), channel_id=1, source_target_pairs={{0,64},{32,96},{64,0},{96,32},{1,65},{33,97},{65,1},{97,33},{2,66}... | collective-permute-start | bytes 221192 | tf_op jit(solution)/shard_map/ppermute | solution.py:222
  171.3 1.8 collective-permute-done.5.refs_2_
  174.4 2.0 join_last.1
  176.4 2.2 collective-permute-start.7
  179.9 12.7 %mixer.1 = bf16[2048,512]{1,0:T(8,128)(2,1)} custom-call(bf16[2048,256]{1,0:T(8,128)(2,1)} %q_ref.1, bf16[2048,256]{1,0:T(8,128)(2,1)} %k_ref.3, bf16[2048,512]{1,0:T(8,128)(2,1)} %v_ref.3, bf16[2048,512]{1,0:T(8,128)(2,1)} %g_ref.1, f32[2,2048]{1,0:T(2,128)} %a_ref.3, f32[128,256]{1,0:T(8,128)} %get-tuple-element.12.mine_ref, ...), custom_call_target="tpu_custom_call" | custom-call | flops 1610612736 | bytes 8388608 | tf_op jit(solution)/shard_map/mixer/pallas_call | solution.py:268
  192.5 2.3 dynamic-slice_bitcast_fusion
  194.8 2.4 collective-permute-start.10
  199.7 2.5 collective-permute-start.14
  203.4 4.7 %collective-permute-done.10.refs_3_ = bf16[512,512]{1,0:T(8,128)(2,1)S(1)} collective-permute-done((bf16[512,512]{1,0:T(8,128)(2,1)S(1)}, bf16[512,512]{1,0:T(8,128)(2,1)S(1)}, u32[]{:S(2)}, u32[]{:S(2)}) %collective-permute-start.10) | collective-permute-done | bytes 524320 | tf_op jit(solution)/shard_map/ppermute | solution.py:222
  208.2 2.0 collective-permute-start.18
  212.7 10.9 %collective-permute-done.12.refs_6_ = bf16[256,1024]{1,0:T(8,128)(2,1)} collective-permute-done((bf16[256,1024]{1,0:T(8,128)(2,1)S(1)}, bf16[256,1024]{1,0:T(8,128)(2,1)}, u32[]{:S(2)}, u32[]{:S(2)}) %collective-permute-start.12) | collective-permute-done | bytes 524320 | tf_op jit(solution)/shard_map/ppermute | solution.py:222
  223.6 11.8 %collective-permute-start.16 = (bf16[256,1024]{1,0:T(8,128)(2,1)}, bf16[256,1024]{1,0:T(8,128)(2,1)}, u32[]{:S(2)}, u32[]{:S(2)}) collective-permute-start(bf16[256,1024]{1,0:T(8,128)(2,1)} %collective-permute-done.12.refs_6_), channel_id=1, source_target_pairs={{0,4},{4,0},{1,5},{5,1},{2,6},{6,2},{3,7},{7,3},{8,12},{12,8},{9,1... | collective-permute-start | bytes 1572872 | tf_op jit(solution)/shard_map/ppermute | solution.py:222
  235.5 2.1 weights.1.weight_ref
  237.6 5.1 %expert.3.shared_ref = f32[128,2048]{1,0:T(8,128)} custom-call(bf16[136,2048]{1,0:T(8,128)(2,1)} %norm.1.refs_0_.x_ref, bf16[2048,512]{1,0:T(8,128)(2,1)} %gate_ref.1, bf16[2048,512]{1,0:T(8,128)(2,1)} %up_ref.1, bf16[512,2048]{1,0:T(8,128)(2,1)} %down_ref.1), custom_call_target="tpu_custom_call" | custom-call | flops 805306368 | bytes 14680064 | tf_op jit(solution)/shard_map/expert/pallas_call | solution.py:499
  242.8 10.0 %project.1 = bf16[512,2048]{1,0:T(8,128)(2,1)} custom-call(bf16[4,512,512]{2,1,0:T(8,128)(2,1)} %bitcast.19, bf16[512,512]{1,0:T(8,128)(2,1)} %copy-done.1, bf16[512,512]{1,0:T(8,128)(2,1)} %collective-permute-done.9.refs_2_, bf16[512,512]{1,0:T(8,128)(2,1)} %copy-done, bf16[512,2048]{1,0:T(8,128)(2,1)} %refs_4_.1, ...), custom_call_target="tpu_custom_call" | custom-call | flops 4294967296 | bytes 12582912 | tf_op jit(solution)/shard_map/project/pallas_call | solution.py:335
  252.7 4.6 %combine.1 = bf16[128,2048]{1,0:T(8,128)(2,1)} custom-call(bf16[256,1024]{1,0:T(8,128)(2,1)} %weights.1.weight_ref, bf16[1024,2048]{1,0:T(8,128)(2,1)} %bitcast.13.rows_ref, f32[128,2048]{1,0:T(8,128)} %expert.3.shared_ref), custom_call_target="tpu_custom_call" | custom-call | flops 1073741824 | bytes 6291456 | tf_op jit(solution)/shard_map/combine/pallas_call | solution.py:528
  (36 shorter events, 19.5 us)
Async XLA Ops:
  2.7 15.6 %collective-permute-start.19 = (bf16[136,2048]{1,0:T(8,128)(2,1)}, bf16[136,2048]{1,0:T(8,128)(2,1)}, u32[]{:S(2)}, u32[]{:S(2)}) collective-permute-start(bf16[136,2048]{1,0:T(8,128)(2,1)} %norm.1.refs_0_.x_ref), channel_id=1, source_target_pairs={{0,1},{1,2},{2,3},{3,0},{4,5},{5,6},{6,7},{7,4},{8,9},{9,10},{10,1... | collective-permute-start | bytes 1671176 | tf_op jit(solution)/shard_map/ppermute | solution.py:222
  4.8 26.7 %collective-permute-start.20 = (bf16[136,2048]{1,0:T(8,128)(2,1)}, bf16[136,2048]{1,0:T(8,128)(2,1)}, u32[]{:S(2)}, u32[]{:S(2)}) collective-permute-start(bf16[136,2048]{1,0:T(8,128)(2,1)} %norm.1.refs_0_.x_ref), channel_id=1, source_target_pairs={{0,2},{1,3},{2,0},{3,1},{4,6},{5,7},{6,4},{7,5},{8,10},{9,11},{10,... | collective-permute-start | bytes 1671176 | tf_op jit(solution)/shard_map/ppermute | solution.py:222
  7.2 24.3 %collective-permute-start.21 = (bf16[136,2048]{1,0:T(8,128)(2,1)}, bf16[136,2048]{1,0:T(8,128)(2,1)}, u32[]{:S(2)}, u32[]{:S(2)}) collective-permute-start(bf16[136,2048]{1,0:T(8,128)(2,1)} %norm.1.refs_0_.x_ref), channel_id=1, source_target_pairs={{0,3},{1,0},{2,1},{3,2},{4,7},{5,4},{6,5},{7,6},{8,11},{9,8},{10,9... | collective-permute-start | bytes 1671176 | tf_op jit(solution)/shard_map/ppermute | solution.py:222
  107.8 144.9 %all-to-all-start.1 = ((bf16[128,8,2048]{2,1,0:T(8,128)(2,1)}), bf16[128,8,2048]{2,1,0:T(8,128)(2,1)}, u32[]{:S(2)}, u32[]{:S(2)}) async-start(bf16[128,8,2048]{2,1,0:T(8,128)(2,1)} %bitcast.20), calls=%async_computation.1 | async-start | bytes 8388608 | tf_op jit(solution)/shard_map/all_to_all | solution.py:547
  118.9 6.1 %collective-permute-start = (bf16[144,256]{1,0:T(8,128)(2,1)}, bf16[144,256]{1,0:T(8,128)(2,1)}, u32[]{:S(2)}, u32[]{:S(2)}) collective-permute-start(bf16[144,256]{1,0:T(8,128)(2,1)} %get-tuple-element.9), channel_id=1, source_target_pairs={{0,4},{4,0},{1,5},{5,1},{2,6},{6,2},{3,7},{7,3},{8,12},{12,8},{9,1... | collective-permute-start | bytes 221192 | tf_op jit(solution)/shard_map/ppermute | solution.py:222
  122.3 74.9 %collective-permute-start.11 = (bf16[512,1024]{1,0:T(8,128)(2,1)}, bf16[512,1024]{1,0:T(8,128)(2,1)}, u32[]{:S(2)}, u32[]{:S(2)}) collective-permute-start(bf16[512,1024]{1,0:T(8,128)(2,1)} %constant_dynamic-slice_fusion), channel_id=1, source_target_pairs={{0,1},{1,2},{2,3},{3,0},{4,5},{5,6},{6,7},{7,4},{8,9},{9,10},{10,1... | collective-permute-start | bytes 3145736 | tf_op jit(solution)/shard_map/ppermute | solution.py:222
  122.9 75.7 %collective-permute-start.13 = (bf16[512,1024]{1,0:T(8,128)(2,1)}, bf16[512,1024]{1,0:T(8,128)(2,1)}, u32[]{:S(2)}, u32[]{:S(2)}) collective-permute-start(bf16[512,1024]{1,0:T(8,128)(2,1)} %constant_dynamic-slice_fusion), channel_id=1, source_target_pairs={{0,3},{1,0},{2,1},{3,2},{4,7},{5,4},{6,5},{7,6},{8,11},{9,8},{10,9... | collective-permute-start | bytes 3145736 | tf_op jit(solution)/shard_map/ppermute | solution.py:222
  126.6 35.0 %collective-permute-start.1 = (bf16[144,256]{1,0:T(8,128)(2,1)}, bf16[144,256]{1,0:T(8,128)(2,1)}, u32[]{:S(2)}, u32[]{:S(2)}) collective-permute-start(bf16[144,256]{1,0:T(8,128)(2,1)} %join_cores.1.refs_0_), channel_id=1, source_target_pairs={{0,8},{8,16},{16,24},{24,0},{1,9},{9,17},{17,25},{25,1},{2,10},{10... | collective-permute-start | bytes 221192 | tf_op jit(solution)/shard_map/ppermute | solution.py:222
  127.2 36.8 %collective-permute-start.2 = (bf16[144,256]{1,0:T(8,128)(2,1)}, bf16[144,256]{1,0:T(8,128)(2,1)}, u32[]{:S(2)}, u32[]{:S(2)}) collective-permute-start(bf16[144,256]{1,0:T(8,128)(2,1)} %join_cores.1.refs_0_), channel_id=1, source_target_pairs={{0,16},{8,24},{16,0},{24,8},{1,17},{9,25},{17,1},{25,9},{2,18},{10... | collective-permute-start | bytes 221192 | tf_op jit(solution)/shard_map/ppermute | solution.py:222
  129.6 34.3 %collective-permute-start.3 = (bf16[144,256]{1,0:T(8,128)(2,1)}, bf16[144,256]{1,0:T(8,128)(2,1)}, u32[]{:S(2)}, u32[]{:S(2)}) collective-permute-start(bf16[144,256]{1,0:T(8,128)(2,1)} %join_cores.1.refs_0_), channel_id=1, source_target_pairs={{0,24},{8,0},{16,8},{24,16},{1,25},{9,1},{17,9},{25,17},{2,26},{10... | collective-permute-start | bytes 221192 | tf_op jit(solution)/shard_map/ppermute | solution.py:222
  165.7 5.6 %collective-permute-start.4 = (bf16[144,256]{1,0:T(8,128)(2,1)}, bf16[144,256]{1,0:T(8,128)(2,1)}, u32[]{:S(2)}, u32[]{:S(2)}) collective-permute-start(bf16[144,256]{1,0:T(8,128)(2,1)} %get-tuple-element.10.refs_0_), channel_id=1, source_target_pairs={{0,32},{32,64},{64,96},{96,0},{1,33},{33,65},{65,97},{97,1},{2,34}... | collective-permute-start | bytes 221192 | tf_op jit(solution)/shard_map/ppermute | solution.py:222
  167.2 5.9 %collective-permute-start.5 = (bf16[144,256]{1,0:T(8,128)(2,1)}, bf16[144,256]{1,0:T(8,128)(2,1)}, u32[]{:S(2)}, u32[]{:S(2)}) collective-permute-start(bf16[144,256]{1,0:T(8,128)(2,1)} %get-tuple-element.10.refs_0_), channel_id=1, source_target_pairs={{0,64},{32,96},{64,0},{96,32},{1,65},{33,97},{65,1},{97,33},{2,66}... | collective-permute-start | bytes 221192 | tf_op jit(solution)/shard_map/ppermute | solution.py:222
  170.1 4.3 %collective-permute-start.6 = (bf16[144,256]{1,0:T(8,128)(2,1)}, bf16[144,256]{1,0:T(8,128)(2,1)}, u32[]{:S(2)}, u32[]{:S(2)}) collective-permute-start(bf16[144,256]{1,0:T(8,128)(2,1)} %get-tuple-element.10.refs_0_), channel_id=1, source_target_pairs={{0,96},{32,0},{64,32},{96,64},{1,97},{33,1},{65,33},{97,65},{2,98}... | collective-permute-start | bytes 221192 | tf_op jit(solution)/shard_map/ppermute | solution.py:222
  176.4 3.5 %collective-permute-start.7 = (bf16[128,256]{1,0:T(8,128)(2,1)}, bf16[128,256]{1,0:T(8,128)(2,1)}, u32[]{:S(2)}, u32[]{:S(2)}) collective-permute-start(bf16[128,256]{1,0:T(8,128)(2,1)} %get-tuple-element.13), channel_id=1, source_target_pairs={{0,4},{4,0},{1,5},{5,1},{2,6},{6,2},{3,7},{7,3},{8,12},{12,8},{9,1... | collective-permute-start | bytes 196616 | tf_op jit(solution)/shard_map/ppermute | solution.py:222
  194.8 13.4 %collective-permute-start.10 = (bf16[512,512]{1,0:T(8,128)(2,1)S(1)}, bf16[512,512]{1,0:T(8,128)(2,1)S(1)}, u32[]{:S(2)}, u32[]{:S(2)}) collective-permute-start(bf16[512,512]{1,0:T(8,128)(2,1)S(1)} %get-tuple-element.14), channel_id=1, source_target_pairs={{0,3},{1,0},{2,1},{3,2},{4,7},{5,4},{6,5},{7,6},{8,11},{9,8},{10,9... | collective-permute-start | bytes 1572872 | tf_op jit(solution)/shard_map/ppermute | solution.py:222
  197.2 14.1 %collective-permute-start.8 = (bf16[512,512]{1,0:T(8,128)(2,1)S(1)}, bf16[512,512]{1,0:T(8,128)(2,1)S(1)}, u32[]{:S(2)}, u32[]{:S(2)}) collective-permute-start(bf16[512,512]{1,0:T(8,128)(2,1)S(1)} %get-tuple-element.16), channel_id=1, source_target_pairs={{0,1},{1,2},{2,3},{3,0},{4,5},{5,6},{6,7},{7,4},{8,9},{9,10},{10,1... | collective-permute-start | bytes 1572872 | tf_op jit(solution)/shard_map/ppermute | solution.py:222
  198.3 25.2 %collective-permute-start.12 = (bf16[256,1024]{1,0:T(8,128)(2,1)S(1)}, bf16[256,1024]{1,0:T(8,128)(2,1)}, u32[]{:S(2)}, u32[]{:S(2)}) collective-permute-start(bf16[256,1024]{1,0:T(8,128)(2,1)S(1)} %slice.8), channel_id=1, source_target_pairs={{0,1},{1,2},{2,3},{3,0},{4,5},{5,6},{6,7},{7,4},{8,9},{9,10},{10,1... | collective-permute-start | bytes 1572872 | tf_op jit(solution)/shard_map/ppermute | solution.py:222
  199.7 35.7 %collective-permute-start.14 = (bf16[256,1024]{1,0:T(8,128)(2,1)S(1)}, bf16[256,1024]{1,0:T(8,128)(2,1)}, u32[]{:S(2)}, u32[]{:S(2)}) collective-permute-start(bf16[256,1024]{1,0:T(8,128)(2,1)S(1)} %slice.9), channel_id=1, source_target_pairs={{0,3},{1,0},{2,1},{3,2},{4,7},{5,4},{6,5},{7,6},{8,11},{9,8},{10,9... | collective-permute-start | bytes 1572872 | tf_op jit(solution)/shard_map/ppermute | solution.py:222
  202.2 40.5 %collective-permute-start.15 = (bf16[512,1024]{1,0:T(8,128)(2,1)}, bf16[512,1024]{1,0:T(8,128)(2,1)}, u32[]{:S(2)}, u32[]{:S(2)}) collective-permute-start(bf16[512,1024]{1,0:T(8,128)(2,1)} %collective-permute-done.11.refs_5_), channel_id=1, source_target_pairs={{0,4},{4,0},{1,5},{5,1},{2,6},{6,2},{3,7},{7,3},{8,12},{12,8},{9,1... | collective-permute-start | bytes 3145736 | tf_op jit(solution)/shard_map/ppermute | solution.py:222
  208.2 27.2 %copy-start = (bf16[512,512]{1,0:T(8,128)(2,1)}, bf16[512,512]{1,0:T(8,128)(2,1)S(1)}, u32[]{:S(2)}) copy-start(bf16[512,512]{1,0:T(8,128)(2,1)S(1)} %collective-permute-done.10.refs_3_) | copy-start | bytes 1572868
  208.2 34.6 %collective-permute-start.18 = (bf16[512,1024]{1,0:T(8,128)(2,1)}, bf16[512,1024]{1,0:T(8,128)(2,1)}, u32[]{:S(2)}, u32[]{:S(2)}) collective-permute-start(bf16[512,1024]{1,0:T(8,128)(2,1)} %collective-permute-done.13.refs_8_), channel_id=1, source_target_pairs={{0,4},{4,0},{1,5},{5,1},{2,6},{6,2},{3,7},{7,3},{8,12},{12,8},{9,1... | collective-permute-start | bytes 3145736 | tf_op jit(solution)/shard_map/ppermute | solution.py:222
  211.3 24.2 %copy-start.1 = (bf16[512,512]{1,0:T(8,128)(2,1)}, bf16[512,512]{1,0:T(8,128)(2,1)S(1)}, u32[]{:S(2)}) copy-start(bf16[512,512]{1,0:T(8,128)(2,1)S(1)} %collective-permute-done.8.refs_1_) | copy-start | bytes 1572868
  211.3 31.4 %collective-permute-start.9 = (bf16[512,512]{1,0:T(8,128)(2,1)}, bf16[512,512]{1,0:T(8,128)(2,1)}, u32[]{:S(2)}, u32[]{:S(2)}) collective-permute-start(bf16[512,512]{1,0:T(8,128)(2,1)} %get-tuple-element.15), channel_id=1, source_target_pairs={{0,2},{1,3},{2,0},{3,1},{4,6},{5,7},{6,4},{7,5},{8,10},{9,11},{10,... | collective-permute-start | bytes 1572872 | tf_op jit(solution)/shard_map/ppermute | solution.py:222
  223.6 19.2 %collective-permute-start.16 = (bf16[256,1024]{1,0:T(8,128)(2,1)}, bf16[256,1024]{1,0:T(8,128)(2,1)}, u32[]{:S(2)}, u32[]{:S(2)}) collective-permute-start(bf16[256,1024]{1,0:T(8,128)(2,1)} %collective-permute-done.12.refs_6_), channel_id=1, source_target_pairs={{0,4},{4,0},{1,5},{5,1},{2,6},{6,2},{3,7},{7,3},{8,12},{12,8},{9,1... | collective-permute-start | bytes 1572872 | tf_op jit(solution)/shard_map/ppermute | solution.py:222
  235.4 7.4 %collective-permute-start.17 = (bf16[256,1024]{1,0:T(8,128)(2,1)}, bf16[256,1024]{1,0:T(8,128)(2,1)}, u32[]{:S(2)}, u32[]{:S(2)}) collective-permute-start(bf16[256,1024]{1,0:T(8,128)(2,1)} %collective-permute-done.14.refs_7_), channel_id=1, source_target_pairs={{0,4},{4,0},{1,5},{5,1},{2,6},{6,2},{3,7},{7,3},{8,12},{12,8},{9,1... | collective-permute-start | bytes 1572872 | tf_op jit(solution)/shard_map/ppermute | solution.py:222

commit v5 on v4

--- a/solution.py
+++ b/solution.py
@@ -492,6 +492,30 @@
     out_ref[...] = dot(hidden, down_ref[...]).astype(out_ref.dtype)
 
 
+def expert_held(rows, w_gate, w_up, w_down):
+    n_rows, width = rows.shape
+    hidden = w_gate.shape[1]
+    tile = 256
+    w_gate = pltpu.with_memory_space_constraint(w_gate, pltpu.VMEM)
+    return pl.pallas_call(
+        expert_body,
+        grid=(n_rows // tile,),
+        in_specs=[
+            pl.BlockSpec((tile, width), lambda i: (i, 0)),
+            pl.BlockSpec(memory_space=pltpu.VMEM),
+            pl.BlockSpec((width, hidden), lambda i: (0, 0)),
+            pl.BlockSpec((hidden, width), lambda i: (0, 0)),
+        ],
+        out_specs=pl.BlockSpec((tile, width), lambda i: (i, 0)),
+        out_shape=jax.ShapeDtypeStruct((n_rows, width), BF16),
+        compiler_params=pltpu.CompilerParams(vmem_limit_bytes=62500000),
+        cost_estimate=pl.CostEstimate(
+            flops=6 * n_rows * width * hidden, bytes_accessed=12 << 20, transcendentals=0
+        ),
+        name="expert",
+    )(rows, w_gate, w_up, w_down)
+
+
 def expert_apply(rows, w_gate, w_up, w_down, dtype, n_rows=None):
     n_rows, width = n_rows or rows.shape[0], rows.shape[1]
     hidden = w_gate.shape[1]
@@ -602,9 +626,7 @@
     shared = expert_apply(message, shared_gate, shared_up, shared_down, F32, n_tokens)
     weights = slot_weights(routes, route_weights, experts * CAP)
 
-    served = expert_apply(
-        received.reshape(-1, width), expert_gate[0], expert_up[0], expert_down[0], BF16
-    )
+    served = expert_held(received.reshape(-1, width), expert_gate[0], expert_up[0], expert_down[0])
     returned = exchange(served.reshape(experts, CAP, width), EP_TP)
 
     mixer_out = project(retained, heads, out_proj, own, other)

time: 258 us -> 258 us (level)
    pallas_call x2 -> x1, Pallas kernels: 16.9 us -> 5.13 us  [expert_apply(): pl.pallas_call(expert_body, grid=(n_rows // tile,), in_specs=[pl.BlockSpe...]
    pallas_call x0 -> x1, Pallas kernels: none -> 11.2 us  [expert_held(): pl.pallas_call(expert_body, grid=(n_rows // tile,), in_specs=[pl.BlockSpe...]
where the time goes in v5:
time: 258 us; the launch traced here: 257 us
  waiting for transfers between devices  74.7 us (29%)
  Pallas kernels  65.2 us (25%)
  blocking collectives  60.6 us (23%)
  starting transfers between devices  49 us (19%)
  local copies, waits for them, and re-layouts  6.68 us (3%)
    ppermute x22, waiting for transfers between devices, shift(): return lax.ppermute(x, axis, [(k, (k + d) % peers) for k in range(peers)])  74.7 us
    all_to_all x1, blocking collectives, exchange(): return lax.all_to_all(x, axes, split_axis=0, concat_axis=0, tiled=True)  60.6 us
    ppermute x22, starting transfers between devices, shift(): return lax.ppermute(x, axis, [(k, (k + d) % peers) for k in range(peers)])  43.2 us
    pallas_call x1, Pallas kernels, mixer(): pl.pallas_call(mixer_body, grid=(n_rows // tile,), in_specs=[pl.BlockSpec...  12.7 us
    pallas_call x1, Pallas kernels, expert_held(): pl.pallas_call(expert_body, grid=(n_rows // tile,), in_specs=[pl.BlockSpe...  11.2 us
    pallas_call x1, Pallas kernels, project(): pl.pallas_call(project_body, in_specs=[pl.BlockSpec(memory_space=pl.ANY)]...  9.98 us
    pallas_call x2, Pallas kernels, dispatch(): pl.pallas_call(functools.partial(dispatch_body, shifts), in_specs=[pl.Blo...  6.89 us
    all_to_all x1, starting transfers between devices, exchange(): return lax.all_to_all(x, axes, split_axis=0, concat_axis=0, tiled=True)  5.83 us
  transfers between devices with their start and end apart: 23, of which 11 were waited for; matrix products, arithmetic and copies ran while one was open for 3% of the time, Pallas kernels for 17%

profile of v5, /device:TPU:1, one launch (start us, length us, event | category | flops | bytes accessed | tf_op | source)
XLA Modules:
  0.0 256.9 jit_solution(16488922521899514898)
XLA Ops:
  0.6 2.1 norm.1.refs_0_.x_ref
  2.7 2.0 collective-permute-start.19
  4.8 2.5 collective-permute-start.20
  8.4 2.8 %dispatch.2.refs_3_ = bf16[32,4,8,2048]{3,2,1,0:T(8,128)(2,1)} custom-call(bf16[136,2048]{1,0:T(8,128)(2,1)} %norm.1.refs_0_.x_ref), custom_call_target="tpu_custom_call" | custom-call | flops 134217728 | bytes 2097152 | tf_op jit(solution)/shard_map/dispatch/pallas_call | solution.py:438
  11.2 7.1 %collective-permute-done.19.refs_0_ = bf16[136,2048]{1,0:T(8,128)(2,1)} collective-permute-done((bf16[136,2048]{1,0:T(8,128)(2,1)}, bf16[136,2048]{1,0:T(8,128)(2,1)}, u32[]{:S(2)}, u32[]{:S(2)}) %collective-permute-start.19) | collective-permute-done | bytes 557088 | tf_op jit(solution)/shard_map/ppermute | solution.py:222
  18.3 13.2 %collective-permute-done.20.refs_1_ = bf16[136,2048]{1,0:T(8,128)(2,1)} collective-permute-done((bf16[136,2048]{1,0:T(8,128)(2,1)}, bf16[136,2048]{1,0:T(8,128)(2,1)}, u32[]{:S(2)}, u32[]{:S(2)}) %collective-permute-start.20) | collective-permute-done | bytes 557088 | tf_op jit(solution)/shard_map/ppermute | solution.py:222
  31.5 4.1 %dispatch.3 = bf16[32,4,8,2048]{3,2,1,0:T(8,128)(2,1)} custom-call(bf16[136,2048]{1,0:T(8,128)(2,1)} %collective-permute-done.19.refs_0_, bf16[136,2048]{1,0:T(8,128)(2,1)} %collective-permute-done.20.refs_1_, bf16[136,2048]{1,0:T(8,128)(2,1)} %collective-permute-done.21.refs_2_, ...), custom_call_target="tpu_custom_call", output_to_operand_aliasing={{}: (3, {})} | custom-call | flops 402653184 | bytes 6291456 | tf_op jit(solution)/shard_map/dispatch/pallas_call | solution.py:438
  35.6 60.6 %all_to_all.10 = bf16[32,32,2048]{2,1,0:T(8,128)(2,1)} all-to-all(bf16[32,32,2048]{2,1,0:T(8,128)(2,1)} %bitcast.18), channel_id=1, replica_groups=mesh['ep_0'=4,'ep_1'=4,'ep_2'=2,'tp'=4] {'ep_0','ep_1','ep_2'}, dimensions={0} | all-to-all | bytes 8388608 | tf_op jit(solution)/shard_map/all_to_all | solution.py:571
  96.3 11.2 %expert.2 = bf16[1024,2048]{1,0:T(8,128)(2,1)} custom-call(bf16[1024,2048]{1,0:T(8,128)(2,1)} %bitcast.22, bf16[2048,512]{1,0:T(8,128)(2,1)S(1)} %bitcast.17, bf16[2048,512]{1,0:T(8,128)(2,1)} %bitcast.27, bf16[512,2048]{1,0:T(8,128)(2,1)} %bitcast.28), custom_call_target="tpu_custom_call" | custom-call | flops 6442450944 | bytes 12582912 | tf_op jit(solution)/shard_map/expert/pallas_call | solution.py:500
  107.4 5.8 %all-to-all-start.1 = ((bf16[128,8,2048]{2,1,0:T(8,128)(2,1)}), bf16[128,8,2048]{2,1,0:T(8,128)(2,1)}, u32[]{:S(2)}, u32[]{:S(2)}) async-start(bf16[128,8,2048]{2,1,0:T(8,128)(2,1)} %bitcast.21), calls=%async_computation.1 | async-start | bytes 8388608 | tf_op jit(solution)/shard_map/all_to_all | solution.py:571
  113.3 5.2 %end_state.1 = (bf16[144,256]{1,0:T(8,128)(2,1)}, bf16[144,256]{1,0:T(8,128)(2,1)}) custom-call(bf16[2048,256]{1,0:T(8,128)(2,1)} %k_ref.3, bf16[2048,512]{1,0:T(8,128)(2,1)} %v_ref.3, f32[2,2048]{1,0:T(2,128)} %a_ref.3), custom_call_target="tpu_custom_call" | custom-call | flops 268435456 | bytes 4194304 | tf_op jit(solution)/shard_map/end_state/pallas_call | solution.py:114
  119.6 2.3 constant_dynamic-slice_fusion
  122.5 2.1 collective-permute-start.13
  126.8 2.4 collective-permute-start.2
  130.4 30.8 %collective-permute-done.1.refs_1_ = bf16[144,256]{1,0:T(8,128)(2,1)} collective-permute-done((bf16[144,256]{1,0:T(8,128)(2,1)}, bf16[144,256]{1,0:T(8,128)(2,1)}, u32[]{:S(2)}, u32[]{:S(2)}) %collective-permute-start.1) | collective-permute-done | bytes 73760 | tf_op jit(solution)/shard_map/ppermute | solution.py:222
  161.1 2.4 collective-permute-done.2.refs_2_
  166.7 2.9 %collective-permute-start.5 = (bf16[144,256]{1,0:T(8,128)(2,1)}, bf16[144,256]{1,0:T(8,128)(2,1)}, u32[]{:S(2)}, u32[]{:S(2)}) collective-permute-start(bf16[144,256]{1,0:T(8,128)(2,1)} %get-tuple-element.10.refs_0_), channel_id=1, source_target_pairs={{0,64},{32,96},{64,0},{96,32},{1,65},{33,97},{65,1},{97,33},{2,66}... | collective-permute-start | bytes 221192 | tf_op jit(solution)/shard_map/ppermute | solution.py:222
  170.8 1.8 collective-permute-done.5.refs_2_
  174.0 2.0 join_last.1
  176.0 2.2 collective-permute-start.7
  179.4 12.7 %mixer.1 = bf16[2048,512]{1,0:T(8,128)(2,1)} custom-call(bf16[2048,256]{1,0:T(8,128)(2,1)} %q_ref.1, bf16[2048,256]{1,0:T(8,128)(2,1)} %k_ref.3, bf16[2048,512]{1,0:T(8,128)(2,1)} %v_ref.3, bf16[2048,512]{1,0:T(8,128)(2,1)} %g_ref.1, f32[2,2048]{1,0:T(2,128)} %a_ref.3, f32[128,256]{1,0:T(8,128)} %get-tuple-element.12.mine_ref, ...), custom_call_target="tpu_custom_call" | custom-call | flops 1610612736 | bytes 8388608 | tf_op jit(solution)/shard_map/mixer/pallas_call | solution.py:268
  192.1 2.3 dynamic-slice_bitcast_fusion
  194.4 2.4 collective-permute-start.10
  199.4 2.5 collective-permute-start.14
  203.2 4.5 %collective-permute-done.10.refs_3_ = bf16[512,512]{1,0:T(8,128)(2,1)S(1)} collective-permute-done((bf16[512,512]{1,0:T(8,128)(2,1)S(1)}, bf16[512,512]{1,0:T(8,128)(2,1)S(1)}, u32[]{:S(2)}, u32[]{:S(2)}) %collective-permute-start.10) | collective-permute-done | bytes 524320 | tf_op jit(solution)/shard_map/ppermute | solution.py:222
  207.7 2.0 collective-permute-start.18
  212.2 10.9 %collective-permute-done.12.refs_6_ = bf16[256,1024]{1,0:T(8,128)(2,1)} collective-permute-done((bf16[256,1024]{1,0:T(8,128)(2,1)S(1)}, bf16[256,1024]{1,0:T(8,128)(2,1)}, u32[]{:S(2)}, u32[]{:S(2)}) %collective-permute-start.12) | collective-permute-done | bytes 524320 | tf_op jit(solution)/shard_map/ppermute | solution.py:222
  223.1 11.8 %collective-permute-start.16 = (bf16[256,1024]{1,0:T(8,128)(2,1)}, bf16[256,1024]{1,0:T(8,128)(2,1)}, u32[]{:S(2)}, u32[]{:S(2)}) collective-permute-start(bf16[256,1024]{1,0:T(8,128)(2,1)} %collective-permute-done.12.refs_6_), channel_id=1, source_target_pairs={{0,4},{4,0},{1,5},{5,1},{2,6},{6,2},{3,7},{7,3},{8,12},{12,8},{9,1... | collective-permute-start | bytes 1572872 | tf_op jit(solution)/shard_map/ppermute | solution.py:222
  235.0 2.1 weights.1.weight_ref
  237.1 5.1 %expert.3.shared_ref = f32[128,2048]{1,0:T(8,128)} custom-call(bf16[136,2048]{1,0:T(8,128)(2,1)} %norm.1.refs_0_.x_ref, bf16[2048,512]{1,0:T(8,128)(2,1)} %gate_ref.1, bf16[2048,512]{1,0:T(8,128)(2,1)} %up_ref.1, bf16[512,2048]{1,0:T(8,128)(2,1)} %down_ref.1), custom_call_target="tpu_custom_call" | custom-call | flops 805306368 | bytes 14680064 | tf_op jit(solution)/shard_map/expert/pallas_call | solution.py:523
  242.3 10.0 %project.1 = bf16[512,2048]{1,0:T(8,128)(2,1)} custom-call(bf16[4,512,512]{2,1,0:T(8,128)(2,1)} %bitcast.20, bf16[512,512]{1,0:T(8,128)(2,1)} %copy-done.2, bf16[512,512]{1,0:T(8,128)(2,1)} %collective-permute-done.9.refs_2_, bf16[512,512]{1,0:T(8,128)(2,1)} %copy-done.1, bf16[512,2048]{1,0:T(8,128)(2,1)} %refs_4_.1, ...), custom_call_target="tpu_custom_call" | custom-call | flops 4294967296 | bytes 12582912 | tf_op jit(solution)/shard_map/project/pallas_call | solution.py:335
  252.3 4.6 %combine.1 = bf16[128,2048]{1,0:T(8,128)(2,1)} custom-call(bf16[256,1024]{1,0:T(8,128)(2,1)} %weights.1.weight_ref, bf16[1024,2048]{1,0:T(8,128)(2,1)} %bitcast.13.rows_ref, f32[128,2048]{1,0:T(8,128)} %expert.3.shared_ref), custom_call_target="tpu_custom_call" | custom-call | flops 1073741824 | bytes 6291456 | tf_op jit(solution)/shard_map/combine/pallas_call | solution.py:552
  (38 shorter events, 19.7 us)
Async XLA Ops:
  2.7 15.6 %collective-permute-start.19 = (bf16[136,2048]{1,0:T(8,128)(2,1)}, bf16[136,2048]{1,0:T(8,128)(2,1)}, u32[]{:S(2)}, u32[]{:S(2)}) collective-permute-start(bf16[136,2048]{1,0:T(8,128)(2,1)} %norm.1.refs_0_.x_ref), channel_id=1, source_target_pairs={{0,1},{1,2},{2,3},{3,0},{4,5},{5,6},{6,7},{7,4},{8,9},{9,10},{10,1... | collective-permute-start | bytes 1671176 | tf_op jit(solution)/shard_map/ppermute | solution.py:222
  4.8 26.7 %collective-permute-start.20 = (bf16[136,2048]{1,0:T(8,128)(2,1)}, bf16[136,2048]{1,0:T(8,128)(2,1)}, u32[]{:S(2)}, u32[]{:S(2)}) collective-permute-start(bf16[136,2048]{1,0:T(8,128)(2,1)} %norm.1.refs_0_.x_ref), channel_id=1, source_target_pairs={{0,2},{1,3},{2,0},{3,1},{4,6},{5,7},{6,4},{7,5},{8,10},{9,11},{10,... | collective-permute-start | bytes 1671176 | tf_op jit(solution)/shard_map/ppermute | solution.py:222
  7.2 24.3 %collective-permute-start.21 = (bf16[136,2048]{1,0:T(8,128)(2,1)}, bf16[136,2048]{1,0:T(8,128)(2,1)}, u32[]{:S(2)}, u32[]{:S(2)}) collective-permute-start(bf16[136,2048]{1,0:T(8,128)(2,1)} %norm.1.refs_0_.x_ref), channel_id=1, source_target_pairs={{0,3},{1,0},{2,1},{3,2},{4,7},{5,4},{6,5},{7,6},{8,11},{9,8},{10,9... | collective-permute-start | bytes 1671176 | tf_op jit(solution)/shard_map/ppermute | solution.py:222
  35.6 60.6 %copy-start = (bf16[1,2048,512]{2,1,0:T(8,128)(2,1)S(1)}, bf16[1,2048,512]{2,1,0:T(8,128)(2,1)}, u32[]{:S(2)}) copy-start(bf16[1,2048,512]{2,1,0:T(8,128)(2,1)} %param.26) | copy-start | bytes 6291460
  107.4 144.9 %all-to-all-start.1 = ((bf16[128,8,2048]{2,1,0:T(8,128)(2,1)}), bf16[128,8,2048]{2,1,0:T(8,128)(2,1)}, u32[]{:S(2)}, u32[]{:S(2)}) async-start(bf16[128,8,2048]{2,1,0:T(8,128)(2,1)} %bitcast.21), calls=%async_computation.1 | async-start | bytes 8388608 | tf_op jit(solution)/shard_map/all_to_all | solution.py:571
  118.4 6.1 %collective-permute-start = (bf16[144,256]{1,0:T(8,128)(2,1)}, bf16[144,256]{1,0:T(8,128)(2,1)}, u32[]{:S(2)}, u32[]{:S(2)}) collective-permute-start(bf16[144,256]{1,0:T(8,128)(2,1)} %get-tuple-element.9), channel_id=1, source_target_pairs={{0,4},{4,0},{1,5},{5,1},{2,6},{6,2},{3,7},{7,3},{8,12},{12,8},{9,1... | collective-permute-start | bytes 221192 | tf_op jit(solution)/shard_map/ppermute | solution.py:222
  121.9 74.9 %collective-permute-start.11 = (bf16[512,1024]{1,0:T(8,128)(2,1)}, bf16[512,1024]{1,0:T(8,128)(2,1)}, u32[]{:S(2)}, u32[]{:S(2)}) collective-permute-start(bf16[512,1024]{1,0:T(8,128)(2,1)} %constant_dynamic-slice_fusion), channel_id=1, source_target_pairs={{0,1},{1,2},{2,3},{3,0},{4,5},{5,6},{6,7},{7,4},{8,9},{9,10},{10,1... | collective-permute-start | bytes 3145736 | tf_op jit(solution)/shard_map/ppermute | solution.py:222
  122.5 75.9 %collective-permute-start.13 = (bf16[512,1024]{1,0:T(8,128)(2,1)}, bf16[512,1024]{1,0:T(8,128)(2,1)}, u32[]{:S(2)}, u32[]{:S(2)}) collective-permute-start(bf16[512,1024]{1,0:T(8,128)(2,1)} %constant_dynamic-slice_fusion), channel_id=1, source_target_pairs={{0,3},{1,0},{2,1},{3,2},{4,7},{5,4},{6,5},{7,6},{8,11},{9,8},{10,9... | collective-permute-start | bytes 3145736 | tf_op jit(solution)/shard_map/ppermute | solution.py:222
  126.2 35.0 %collective-permute-start.1 = (bf16[144,256]{1,0:T(8,128)(2,1)}, bf16[144,256]{1,0:T(8,128)(2,1)}, u32[]{:S(2)}, u32[]{:S(2)}) collective-permute-start(bf16[144,256]{1,0:T(8,128)(2,1)} %join_cores.1.refs_0_), channel_id=1, source_target_pairs={{0,8},{8,16},{16,24},{24,0},{1,9},{9,17},{17,25},{25,1},{2,10},{10... | collective-permute-start | bytes 221192 | tf_op jit(solution)/shard_map/ppermute | solution.py:222
  126.8 36.8 %collective-permute-start.2 = (bf16[144,256]{1,0:T(8,128)(2,1)}, bf16[144,256]{1,0:T(8,128)(2,1)}, u32[]{:S(2)}, u32[]{:S(2)}) collective-permute-start(bf16[144,256]{1,0:T(8,128)(2,1)} %join_cores.1.refs_0_), channel_id=1, source_target_pairs={{0,16},{8,24},{16,0},{24,8},{1,17},{9,25},{17,1},{25,9},{2,18},{10... | collective-permute-start | bytes 221192 | tf_op jit(solution)/shard_map/ppermute | solution.py:222
  129.2 34.3 %collective-permute-start.3 = (bf16[144,256]{1,0:T(8,128)(2,1)}, bf16[144,256]{1,0:T(8,128)(2,1)}, u32[]{:S(2)}, u32[]{:S(2)}) collective-permute-start(bf16[144,256]{1,0:T(8,128)(2,1)} %join_cores.1.refs_0_), channel_id=1, source_target_pairs={{0,24},{8,0},{16,8},{24,16},{1,25},{9,1},{17,9},{25,17},{2,26},{10... | collective-permute-start | bytes 221192 | tf_op jit(solution)/shard_map/ppermute | solution.py:222
  165.3 5.6 %collective-permute-start.4 = (bf16[144,256]{1,0:T(8,128)(2,1)}, bf16[144,256]{1,0:T(8,128)(2,1)}, u32[]{:S(2)}, u32[]{:S(2)}) collective-permute-start(bf16[144,256]{1,0:T(8,128)(2,1)} %get-tuple-element.10.refs_0_), channel_id=1, source_target_pairs={{0,32},{32,64},{64,96},{96,0},{1,33},{33,65},{65,97},{97,1},{2,34}... | collective-permute-start | bytes 221192 | tf_op jit(solution)/shard_map/ppermute | solution.py:222
  166.7 5.9 %collective-permute-start.5 = (bf16[144,256]{1,0:T(8,128)(2,1)}, bf16[144,256]{1,0:T(8,128)(2,1)}, u32[]{:S(2)}, u32[]{:S(2)}) collective-permute-start(bf16[144,256]{1,0:T(8,128)(2,1)} %get-tuple-element.10.refs_0_), channel_id=1, source_target_pairs={{0,64},{32,96},{64,0},{96,32},{1,65},{33,97},{65,1},{97,33},{2,66}... | collective-permute-start | bytes 221192 | tf_op jit(solution)/shard_map/ppermute | solution.py:222
  169.7 4.3 %collective-permute-start.6 = (bf16[144,256]{1,0:T(8,128)(2,1)}, bf16[144,256]{1,0:T(8,128)(2,1)}, u32[]{:S(2)}, u32[]{:S(2)}) collective-permute-start(bf16[144,256]{1,0:T(8,128)(2,1)} %get-tuple-element.10.refs_0_), channel_id=1, source_target_pairs={{0,96},{32,0},{64,32},{96,64},{1,97},{33,1},{65,33},{97,65},{2,98}... | collective-permute-start | bytes 221192 | tf_op jit(solution)/shard_map/ppermute | solution.py:222
  176.0 3.5 %collective-permute-start.7 = (bf16[128,256]{1,0:T(8,128)(2,1)}, bf16[128,256]{1,0:T(8,128)(2,1)}, u32[]{:S(2)}, u32[]{:S(2)}) collective-permute-start(bf16[128,256]{1,0:T(8,128)(2,1)} %get-tuple-element.13), channel_id=1, source_target_pairs={{0,4},{4,0},{1,5},{5,1},{2,6},{6,2},{3,7},{7,3},{8,12},{12,8},{9,1... | collective-permute-start | bytes 196616 | tf_op jit(solution)/shard_map/ppermute | solution.py:222
  194.4 13.4 %collective-permute-start.10 = (bf16[512,512]{1,0:T(8,128)(2,1)S(1)}, bf16[512,512]{1,0:T(8,128)(2,1)S(1)}, u32[]{:S(2)}, u32[]{:S(2)}) collective-permute-start(bf16[512,512]{1,0:T(8,128)(2,1)S(1)} %get-tuple-element.14), channel_id=1, source_target_pairs={{0,3},{1,0},{2,1},{3,2},{4,7},{5,4},{6,5},{7,6},{8,11},{9,8},{10,9... | collective-permute-start | bytes 1572872 | tf_op jit(solution)/shard_map/ppermute | solution.py:222
  196.8 14.1 %collective-permute-start.8 = (bf16[512,512]{1,0:T(8,128)(2,1)S(1)}, bf16[512,512]{1,0:T(8,128)(2,1)S(1)}, u32[]{:S(2)}, u32[]{:S(2)}) collective-permute-start(bf16[512,512]{1,0:T(8,128)(2,1)S(1)} %get-tuple-element.16), channel_id=1, source_target_pairs={{0,1},{1,2},{2,3},{3,0},{4,5},{5,6},{6,7},{7,4},{8,9},{9,10},{10,1... | collective-permute-start | bytes 1572872 | tf_op jit(solution)/shard_map/ppermute | solution.py:222
  197.9 25.2 %collective-permute-start.12 = (bf16[256,1024]{1,0:T(8,128)(2,1)S(1)}, bf16[256,1024]{1,0:T(8,128)(2,1)}, u32[]{:S(2)}, u32[]{:S(2)}) collective-permute-start(bf16[256,1024]{1,0:T(8,128)(2,1)S(1)} %slice.8), channel_id=1, source_target_pairs={{0,1},{1,2},{2,3},{3,0},{4,5},{5,6},{6,7},{7,4},{8,9},{9,10},{10,1... | collective-permute-start | bytes 1572872 | tf_op jit(solution)/shard_map/ppermute | solution.py:222
  199.4 35.5 %collective-permute-start.14 = (bf16[256,1024]{1,0:T(8,128)(2,1)S(1)}, bf16[256,1024]{1,0:T(8,128)(2,1)}, u32[]{:S(2)}, u32[]{:S(2)}) collective-permute-start(bf16[256,1024]{1,0:T(8,128)(2,1)S(1)} %slice.9), channel_id=1, source_target_pairs={{0,3},{1,0},{2,1},{3,2},{4,7},{5,4},{6,5},{7,6},{8,11},{9,8},{10,9... | collective-permute-start | bytes 1572872 | tf_op jit(solution)/shard_map/ppermute | solution.py:222
  202.0 40.3 %collective-permute-start.15 = (bf16[512,1024]{1,0:T(8,128)(2,1)}, bf16[512,1024]{1,0:T(8,128)(2,1)}, u32[]{:S(2)}, u32[]{:S(2)}) collective-permute-start(bf16[512,1024]{1,0:T(8,128)(2,1)} %collective-permute-done.11.refs_5_), channel_id=1, source_target_pairs={{0,4},{4,0},{1,5},{5,1},{2,6},{6,2},{3,7},{7,3},{8,12},{12,8},{9,1... | collective-permute-start | bytes 3145736 | tf_op jit(solution)/shard_map/ppermute | solution.py:222
  207.7 27.2 %copy-start.1 = (bf16[512,512]{1,0:T(8,128)(2,1)}, bf16[512,512]{1,0:T(8,128)(2,1)S(1)}, u32[]{:S(2)}) copy-start(bf16[512,512]{1,0:T(8,128)(2,1)S(1)} %collective-permute-done.10.refs_3_) | copy-start | bytes 1572868
  207.7 34.6 %collective-permute-start.18 = (bf16[512,1024]{1,0:T(8,128)(2,1)}, bf16[512,1024]{1,0:T(8,128)(2,1)}, u32[]{:S(2)}, u32[]{:S(2)}) collective-permute-start(bf16[512,1024]{1,0:T(8,128)(2,1)} %collective-permute-done.13.refs_8_), channel_id=1, source_target_pairs={{0,4},{4,0},{1,5},{5,1},{2,6},{6,2},{3,7},{7,3},{8,12},{12,8},{9,1... | collective-permute-start | bytes 3145736 | tf_op jit(solution)/shard_map/ppermute | solution.py:222
  210.9 24.2 %copy-start.2 = (bf16[512,512]{1,0:T(8,128)(2,1)}, bf16[512,512]{1,0:T(8,128)(2,1)S(1)}, u32[]{:S(2)}) copy-start(bf16[512,512]{1,0:T(8,128)(2,1)S(1)} %collective-permute-done.8.refs_1_) | copy-start | bytes 1572868
  210.9 31.4 %collective-permute-start.9 = (bf16[512,512]{1,0:T(8,128)(2,1)}, bf16[512,512]{1,0:T(8,128)(2,1)}, u32[]{:S(2)}, u32[]{:S(2)}) collective-permute-start(bf16[512,512]{1,0:T(8,128)(2,1)} %get-tuple-element.15), channel_id=1, source_target_pairs={{0,2},{1,3},{2,0},{3,1},{4,6},{5,7},{6,4},{7,5},{8,10},{9,11},{10,... | collective-permute-start | bytes 1572872 | tf_op jit(solution)/shard_map/ppermute | solution.py:222
  223.1 19.2 %collective-permute-start.16 = (bf16[256,1024]{1,0:T(8,128)(2,1)}, bf16[256,1024]{1,0:T(8,128)(2,1)}, u32[]{:S(2)}, u32[]{:S(2)}) collective-permute-start(bf16[256,1024]{1,0:T(8,128)(2,1)} %collective-permute-done.12.refs_6_), channel_id=1, source_target_pairs={{0,4},{4,0},{1,5},{5,1},{2,6},{6,2},{3,7},{7,3},{8,12},{12,8},{9,1... | collective-permute-start | bytes 1572872 | tf_op jit(solution)/shard_map/ppermute | solution.py:222
  234.9 7.4 %collective-permute-start.17 = (bf16[256,1024]{1,0:T(8,128)(2,1)}, bf16[256,1024]{1,0:T(8,128)(2,1)}, u32[]{:S(2)}, u32[]{:S(2)}) collective-permute-start(bf16[256,1024]{1,0:T(8,128)(2,1)} %collective-permute-done.14.refs_7_), channel_id=1, source_target_pairs={{0,4},{4,0},{1,5},{5,1},{2,6},{6,2},{3,7},{7,3},{8,12},{12,8},{9,1... | collective-permute-start | bytes 1572872 | tf_op jit(solution)/shard_map/ppermute | solution.py:222

commit v6 on v5

--- a/solution.py
+++ b/solution.py
@@ -539,30 +539,39 @@
     )(rows, w_gate, w_up, w_down)
 
 
-def combine_body(weight_ref, rows_ref, shared_ref, out_ref):
+def combine_body(weight_ref, rows_ref, shared_ref, out_ref, total):
     both = dot(weight_ref[...], rows_ref[...])
     n_tokens = out_ref.shape[0]
-    out_ref[...] = (both[:n_tokens] + both[n_tokens:] + shared_ref[...]).astype(BF16)
+    part = both[:n_tokens] + both[n_tokens:]
+
+    @pl.when(pl.program_id(0) == 0)
+    def _():
+        total[...] = part + shared_ref[...]
+
+    @pl.when(pl.program_id(0) == 1)
+    def _():
+        out_ref[...] = (total[...] + part).astype(BF16)
 
 
 def combine(weights, rows, shared):
     n_slots, width = rows.shape
     n_tokens = shared.shape[0]
-    tile = width // 2
+    tile = n_slots // 2
     return pl.pallas_call(
         combine_body,
-        grid=(width // tile,),
+        grid=(2,),
         in_specs=[
-            pl.BlockSpec((2 * n_tokens, n_slots), lambda i: (0, 0)),
-            pl.BlockSpec((n_slots, tile), lambda i: (0, i)),
-            pl.BlockSpec((n_tokens, tile), lambda i: (0, i)),
-        ],
-        out_specs=pl.BlockSpec((n_tokens, tile), lambda i: (0, i)),
+            pl.BlockSpec((2 * n_tokens, tile), lambda i: (0, i)),
+            pl.BlockSpec((tile, width), lambda i: (i, 0)),
+            pl.BlockSpec((n_tokens, width), lambda i: (0, 0)),
+        ],
+        out_specs=pl.BlockSpec((n_tokens, width), lambda i: (0, 0)),
         out_shape=jax.ShapeDtypeStruct((n_tokens, width), BF16),
+        scratch_shapes=[pltpu.VMEM((n_tokens, width), F32)],
+        compiler_params=ALL_VMEM,
         cost_estimate=pl.CostEstimate(
             flops=4 * n_tokens * n_slots * width, bytes_accessed=6 << 20, transcendentals=0
         ),
-        compiler_params=ALL_VMEM,
         name="combine",
     )(weights, rows, shared)
 

time: 258 us -> 257 us (level)
  no operation moved by 1% of the time
where the time goes in v6:
time: 257 us
  waiting for transfers between devices  74.7 us (29%)
  Pallas kernels  65 us (25%)
  blocking collectives  60.6 us (24%)
  starting transfers between devices  49 us (19%)
  local copies, waits for them, and re-layouts  6.68 us (3%)
    ppermute x22, waiting for transfers between devices, shift(): return lax.ppermute(x, axis, [(k, (k + d) % peers) for k in range(peers)])  74.7 us
    all_to_all x1, blocking collectives, exchange(): return lax.all_to_all(x, axes, split_axis=0, concat_axis=0, tiled=True)  60.6 us
    ppermute x22, starting transfers between devices, shift(): return lax.ppermute(x, axis, [(k, (k + d) % peers) for k in range(peers)])  43.2 us
    pallas_call x1, Pallas kernels, mixer(): pl.pallas_call(mixer_body, grid=(n_rows // tile,), in_specs=[pl.BlockSpec...  12.7 us
    pallas_call x1, Pallas kernels, expert_held(): pl.pallas_call(expert_body, grid=(n_rows // tile,), in_specs=[pl.BlockSpe...  11.2 us
    pallas_call x1, Pallas kernels, project(): pl.pallas_call(project_body, in_specs=[pl.BlockSpec(memory_space=pl.ANY)]...  9.98 us
    pallas_call x2, Pallas kernels, dispatch(): pl.pallas_call(functools.partial(dispatch_body, shifts), in_specs=[pl.Blo...  6.89 us
    all_to_all x1, starting transfers between devices, exchange(): return lax.all_to_all(x, axes, split_axis=0, concat_axis=0, tiled=True)  5.83 us
  transfers between devices with their start and end apart: 23, of which 11 were waited for; matrix products, arithmetic and copies ran while one was open for 3% of the time, Pallas kernels for 17%

profile of v6, /device:TPU:1, one launch (start us, length us, event | category | flops | bytes accessed | tf_op | source)
XLA Modules:
  0.0 256.7 jit_solution(4419148174592174340)
XLA Ops:
  0.6 2.1 norm.1.refs_0_.x_ref
  2.7 2.0 collective-permute-start.19
  4.8 2.5 collective-permute-start.20
  8.4 2.8 %dispatch.2.refs_3_ = bf16[32,4,8,2048]{3,2,1,0:T(8,128)(2,1)} custom-call(bf16[136,2048]{1,0:T(8,128)(2,1)} %norm.1.refs_0_.x_ref), custom_call_target="tpu_custom_call" | custom-call | flops 134217728 | bytes 2097152 | tf_op jit(solution)/shard_map/dispatch/pallas_call | solution.py:438
  11.2 7.1 %collective-permute-done.19.refs_0_ = bf16[136,2048]{1,0:T(8,128)(2,1)} collective-permute-done((bf16[136,2048]{1,0:T(8,128)(2,1)}, bf16[136,2048]{1,0:T(8,128)(2,1)}, u32[]{:S(2)}, u32[]{:S(2)}) %collective-permute-start.19) | collective-permute-done | bytes 557088 | tf_op jit(solution)/shard_map/ppermute | solution.py:222
  18.3 13.2 %collective-permute-done.20.refs_1_ = bf16[136,2048]{1,0:T(8,128)(2,1)} collective-permute-done((bf16[136,2048]{1,0:T(8,128)(2,1)}, bf16[136,2048]{1,0:T(8,128)(2,1)}, u32[]{:S(2)}, u32[]{:S(2)}) %collective-permute-start.20) | collective-permute-done | bytes 557088 | tf_op jit(solution)/shard_map/ppermute | solution.py:222
  31.5 4.1 %dispatch.3 = bf16[32,4,8,2048]{3,2,1,0:T(8,128)(2,1)} custom-call(bf16[136,2048]{1,0:T(8,128)(2,1)} %collective-permute-done.19.refs_0_, bf16[136,2048]{1,0:T(8,128)(2,1)} %collective-permute-done.20.refs_1_, bf16[136,2048]{1,0:T(8,128)(2,1)} %collective-permute-done.21.refs_2_, ...), custom_call_target="tpu_custom_call", output_to_operand_aliasing={{}: (3, {})} | custom-call | flops 402653184 | bytes 6291456 | tf_op jit(solution)/shard_map/dispatch/pallas_call | solution.py:438
  35.6 60.6 %all_to_all.10 = bf16[32,32,2048]{2,1,0:T(8,128)(2,1)} all-to-all(bf16[32,32,2048]{2,1,0:T(8,128)(2,1)} %bitcast.18), channel_id=1, replica_groups=mesh['ep_0'=4,'ep_1'=4,'ep_2'=2,'tp'=4] {'ep_0','ep_1','ep_2'}, dimensions={0} | all-to-all | bytes 8388608 | tf_op jit(solution)/shard_map/all_to_all | solution.py:580
  96.3 11.2 %expert.2 = bf16[1024,2048]{1,0:T(8,128)(2,1)} custom-call(bf16[1024,2048]{1,0:T(8,128)(2,1)} %bitcast.22, bf16[2048,512]{1,0:T(8,128)(2,1)S(1)} %bitcast.17, bf16[2048,512]{1,0:T(8,128)(2,1)} %bitcast.27, bf16[512,2048]{1,0:T(8,128)(2,1)} %bitcast.28), custom_call_target="tpu_custom_call" | custom-call | flops 6442450944 | bytes 12582912 | tf_op jit(solution)/shard_map/expert/pallas_call | solution.py:500
  107.4 5.8 %all-to-all-start.1 = ((bf16[128,8,2048]{2,1,0:T(8,128)(2,1)}), bf16[128,8,2048]{2,1,0:T(8,128)(2,1)}, u32[]{:S(2)}, u32[]{:S(2)}) async-start(bf16[128,8,2048]{2,1,0:T(8,128)(2,1)} %bitcast.21), calls=%async_computation.1 | async-start | bytes 8388608 | tf_op jit(solution)/shard_map/all_to_all | solution.py:580
  113.3 5.2 %end_state.1 = (bf16[144,256]{1,0:T(8,128)(2,1)}, bf16[144,256]{1,0:T(8,128)(2,1)}) custom-call(bf16[2048,256]{1,0:T(8,128)(2,1)} %k_ref.3, bf16[2048,512]{1,0:T(8,128)(2,1)} %v_ref.3, f32[2,2048]{1,0:T(2,128)} %a_ref.3), custom_call_target="tpu_custom_call" | custom-call | flops 268435456 | bytes 4194304 | tf_op jit(solution)/shard_map/end_state/pallas_call | solution.py:114
  119.6 2.3 constant_dynamic-slice_fusion
  122.5 2.1 collective-permute-start.13
  126.8 2.4 collective-permute-start.2
  130.4 30.8 %collective-permute-done.1.refs_1_ = bf16[144,256]{1,0:T(8,128)(2,1)} collective-permute-done((bf16[144,256]{1,0:T(8,128)(2,1)}, bf16[144,256]{1,0:T(8,128)(2,1)}, u32[]{:S(2)}, u32[]{:S(2)}) %collective-permute-start.1) | collective-permute-done | bytes 73760 | tf_op jit(solution)/shard_map/ppermute | solution.py:222
  161.1 2.4 collective-permute-done.2.refs_2_
  166.7 2.9 %collective-permute-start.5 = (bf16[144,256]{1,0:T(8,128)(2,1)}, bf16[144,256]{1,0:T(8,128)(2,1)}, u32[]{:S(2)}, u32[]{:S(2)}) collective-permute-start(bf16[144,256]{1,0:T(8,128)(2,1)} %get-tuple-element.10.refs_0_), channel_id=1, source_target_pairs={{0,64},{32,96},{64,0},{96,32},{1,65},{33,97},{65,1},{97,33},{2,66}... | collective-permute-start | bytes 221192 | tf_op jit(solution)/shard_map/ppermute | solution.py:222
  170.8 1.8 collective-permute-done.5.refs_2_
  174.0 2.0 join_last.1
  176.0 2.2 collective-permute-start.7
  179.4 12.7 %mixer.1 = bf16[2048,512]{1,0:T(8,128)(2,1)} custom-call(bf16[2048,256]{1,0:T(8,128)(2,1)} %q_ref.1, bf16[2048,256]{1,0:T(8,128)(2,1)} %k_ref.3, bf16[2048,512]{1,0:T(8,128)(2,1)} %v_ref.3, bf16[2048,512]{1,0:T(8,128)(2,1)} %g_ref.1, f32[2,2048]{1,0:T(2,128)} %a_ref.3, f32[128,256]{1,0:T(8,128)} %get-tuple-element.12.mine_ref, ...), custom_call_target="tpu_custom_call" | custom-call | flops 1610612736 | bytes 8388608 | tf_op jit(solution)/shard_map/mixer/pallas_call | solution.py:268
  192.1 2.3 dynamic-slice_bitcast_fusion
  194.4 2.4 collective-permute-start.10
  199.4 2.5 collective-permute-start.14
  203.2 4.5 %collective-permute-done.10.refs_3_ = bf16[512,512]{1,0:T(8,128)(2,1)S(1)} collective-permute-done((bf16[512,512]{1,0:T(8,128)(2,1)S(1)}, bf16[512,512]{1,0:T(8,128)(2,1)S(1)}, u32[]{:S(2)}, u32[]{:S(2)}) %collective-permute-start.10) | collective-permute-done | bytes 524320 | tf_op jit(solution)/shard_map/ppermute | solution.py:222
  207.7 2.0 collective-permute-start.18
  212.2 10.9 %collective-permute-done.12.refs_6_ = bf16[256,1024]{1,0:T(8,128)(2,1)} collective-permute-done((bf16[256,1024]{1,0:T(8,128)(2,1)S(1)}, bf16[256,1024]{1,0:T(8,128)(2,1)}, u32[]{:S(2)}, u32[]{:S(2)}) %collective-permute-start.12) | collective-permute-done | bytes 524320 | tf_op jit(solution)/shard_map/ppermute | solution.py:222
  223.1 11.8 %collective-permute-start.16 = (bf16[256,1024]{1,0:T(8,128)(2,1)}, bf16[256,1024]{1,0:T(8,128)(2,1)}, u32[]{:S(2)}, u32[]{:S(2)}) collective-permute-start(bf16[256,1024]{1,0:T(8,128)(2,1)} %collective-permute-done.12.refs_6_), channel_id=1, source_target_pairs={{0,4},{4,0},{1,5},{5,1},{2,6},{6,2},{3,7},{7,3},{8,12},{12,8},{9,1... | collective-permute-start | bytes 1572872 | tf_op jit(solution)/shard_map/ppermute | solution.py:222
  235.0 2.1 weights.1.weight_ref
  237.1 5.1 %expert.3.shared_ref = f32[128,2048]{1,0:T(8,128)} custom-call(bf16[136,2048]{1,0:T(8,128)(2,1)} %norm.1.refs_0_.x_ref, bf16[2048,512]{1,0:T(8,128)(2,1)} %gate_ref.1, bf16[2048,512]{1,0:T(8,128)(2,1)} %up_ref.1, bf16[512,2048]{1,0:T(8,128)(2,1)} %down_ref.1), custom_call_target="tpu_custom_call" | custom-call | flops 805306368 | bytes 14680064 | tf_op jit(solution)/shard_map/expert/pallas_call | solution.py:523
  242.3 10.0 %project.1 = bf16[512,2048]{1,0:T(8,128)(2,1)} custom-call(bf16[4,512,512]{2,1,0:T(8,128)(2,1)} %bitcast.20, bf16[512,512]{1,0:T(8,128)(2,1)} %copy-done.2, bf16[512,512]{1,0:T(8,128)(2,1)} %collective-permute-done.9.refs_2_, bf16[512,512]{1,0:T(8,128)(2,1)} %copy-done.1, bf16[512,2048]{1,0:T(8,128)(2,1)} %refs_4_.1, ...), custom_call_target="tpu_custom_call" | custom-call | flops 4294967296 | bytes 12582912 | tf_op jit(solution)/shard_map/project/pallas_call | solution.py:335
  252.3 4.4 %combine.1 = bf16[128,2048]{1,0:T(8,128)(2,1)} custom-call(bf16[256,1024]{1,0:T(8,128)(2,1)} %weights.1.weight_ref, bf16[1024,2048]{1,0:T(8,128)(2,1)} %bitcast.13.rows_ref, f32[128,2048]{1,0:T(8,128)} %expert.3.shared_ref), custom_call_target="tpu_custom_call" | custom-call | flops 1073741824 | bytes 6291456 | tf_op jit(solution)/shard_map/combine/pallas_call | solution.py:560
  (38 shorter events, 19.7 us)
Async XLA Ops:
  2.7 15.6 %collective-permute-start.19 = (bf16[136,2048]{1,0:T(8,128)(2,1)}, bf16[136,2048]{1,0:T(8,128)(2,1)}, u32[]{:S(2)}, u32[]{:S(2)}) collective-permute-start(bf16[136,2048]{1,0:T(8,128)(2,1)} %norm.1.refs_0_.x_ref), channel_id=1, source_target_pairs={{0,1},{1,2},{2,3},{3,0},{4,5},{5,6},{6,7},{7,4},{8,9},{9,10},{10,1... | collective-permute-start | bytes 1671176 | tf_op jit(solution)/shard_map/ppermute | solution.py:222
  4.8 26.7 %collective-permute-start.20 = (bf16[136,2048]{1,0:T(8,128)(2,1)}, bf16[136,2048]{1,0:T(8,128)(2,1)}, u32[]{:S(2)}, u32[]{:S(2)}) collective-permute-start(bf16[136,2048]{1,0:T(8,128)(2,1)} %norm.1.refs_0_.x_ref), channel_id=1, source_target_pairs={{0,2},{1,3},{2,0},{3,1},{4,6},{5,7},{6,4},{7,5},{8,10},{9,11},{10,... | collective-permute-start | bytes 1671176 | tf_op jit(solution)/shard_map/ppermute | solution.py:222
  7.2 24.3 %collective-permute-start.21 = (bf16[136,2048]{1,0:T(8,128)(2,1)}, bf16[136,2048]{1,0:T(8,128)(2,1)}, u32[]{:S(2)}, u32[]{:S(2)}) collective-permute-start(bf16[136,2048]{1,0:T(8,128)(2,1)} %norm.1.refs_0_.x_ref), channel_id=1, source_target_pairs={{0,3},{1,0},{2,1},{3,2},{4,7},{5,4},{6,5},{7,6},{8,11},{9,8},{10,9... | collective-permute-start | bytes 1671176 | tf_op jit(solution)/shard_map/ppermute | solution.py:222
  35.6 60.6 %copy-start = (bf16[1,2048,512]{2,1,0:T(8,128)(2,1)S(1)}, bf16[1,2048,512]{2,1,0:T(8,128)(2,1)}, u32[]{:S(2)}) copy-start(bf16[1,2048,512]{2,1,0:T(8,128)(2,1)} %param.26) | copy-start | bytes 6291460
  107.4 144.9 %all-to-all-start.1 = ((bf16[128,8,2048]{2,1,0:T(8,128)(2,1)}), bf16[128,8,2048]{2,1,0:T(8,128)(2,1)}, u32[]{:S(2)}, u32[]{:S(2)}) async-start(bf16[128,8,2048]{2,1,0:T(8,128)(2,1)} %bitcast.21), calls=%async_computation.1 | async-start | bytes 8388608 | tf_op jit(solution)/shard_map/all_to_all | solution.py:580
  118.4 6.1 %collective-permute-start = (bf16[144,256]{1,0:T(8,128)(2,1)}, bf16[144,256]{1,0:T(8,128)(2,1)}, u32[]{:S(2)}, u32[]{:S(2)}) collective-permute-start(bf16[144,256]{1,0:T(8,128)(2,1)} %get-tuple-element.9), channel_id=1, source_target_pairs={{0,4},{4,0},{1,5},{5,1},{2,6},{6,2},{3,7},{7,3},{8,12},{12,8},{9,1... | collective-permute-start | bytes 221192 | tf_op jit(solution)/shard_map/ppermute | solution.py:222
  121.9 74.9 %collective-permute-start.11 = (bf16[512,1024]{1,0:T(8,128)(2,1)}, bf16[512,1024]{1,0:T(8,128)(2,1)}, u32[]{:S(2)}, u32[]{:S(2)}) collective-permute-start(bf16[512,1024]{1,0:T(8,128)(2,1)} %constant_dynamic-slice_fusion), channel_id=1, source_target_pairs={{0,1},{1,2},{2,3},{3,0},{4,5},{5,6},{6,7},{7,4},{8,9},{9,10},{10,1... | collective-permute-start | bytes 3145736 | tf_op jit(solution)/shard_map/ppermute | solution.py:222
  122.5 75.9 %collective-permute-start.13 = (bf16[512,1024]{1,0:T(8,128)(2,1)}, bf16[512,1024]{1,0:T(8,128)(2,1)}, u32[]{:S(2)}, u32[]{:S(2)}) collective-permute-start(bf16[512,1024]{1,0:T(8,128)(2,1)} %constant_dynamic-slice_fusion), channel_id=1, source_target_pairs={{0,3},{1,0},{2,1},{3,2},{4,7},{5,4},{6,5},{7,6},{8,11},{9,8},{10,9... | collective-permute-start | bytes 3145736 | tf_op jit(solution)/shard_map/ppermute | solution.py:222
  126.2 35.0 %collective-permute-start.1 = (bf16[144,256]{1,0:T(8,128)(2,1)}, bf16[144,256]{1,0:T(8,128)(2,1)}, u32[]{:S(2)}, u32[]{:S(2)}) collective-permute-start(bf16[144,256]{1,0:T(8,128)(2,1)} %join_cores.1.refs_0_), channel_id=1, source_target_pairs={{0,8},{8,16},{16,24},{24,0},{1,9},{9,17},{17,25},{25,1},{2,10},{10... | collective-permute-start | bytes 221192 | tf_op jit(solution)/shard_map/ppermute | solution.py:222
  126.8 36.8 %collective-permute-start.2 = (bf16[144,256]{1,0:T(8,128)(2,1)}, bf16[144,256]{1,0:T(8,128)(2,1)}, u32[]{:S(2)}, u32[]{:S(2)}) collective-permute-start(bf16[144,256]{1,0:T(8,128)(2,1)} %join_cores.1.refs_0_), channel_id=1, source_target_pairs={{0,16},{8,24},{16,0},{24,8},{1,17},{9,25},{17,1},{25,9},{2,18},{10... | collective-permute-start | bytes 221192 | tf_op jit(solution)/shard_map/ppermute | solution.py:222
  129.2 34.3 %collective-permute-start.3 = (bf16[144,256]{1,0:T(8,128)(2,1)}, bf16[144,256]{1,0:T(8,128)(2,1)}, u32[]{:S(2)}, u32[]{:S(2)}) collective-permute-start(bf16[144,256]{1,0:T(8,128)(2,1)} %join_cores.1.refs_0_), channel_id=1, source_target_pairs={{0,24},{8,0},{16,8},{24,16},{1,25},{9,1},{17,9},{25,17},{2,26},{10... | collective-permute-start | bytes 221192 | tf_op jit(solution)/shard_map/ppermute | solution.py:222
  165.3 5.6 %collective-permute-start.4 = (bf16[144,256]{1,0:T(8,128)(2,1)}, bf16[144,256]{1,0:T(8,128)(2,1)}, u32[]{:S(2)}, u32[]{:S(2)}) collective-permute-start(bf16[144,256]{1,0:T(8,128)(2,1)} %get-tuple-element.10.refs_0_), channel_id=1, source_target_pairs={{0,32},{32,64},{64,96},{96,0},{1,33},{33,65},{65,97},{97,1},{2,34}... | collective-permute-start | bytes 221192 | tf_op jit(solution)/shard_map/ppermute | solution.py:222
  166.7 5.9 %collective-permute-start.5 = (bf16[144,256]{1,0:T(8,128)(2,1)}, bf16[144,256]{1,0:T(8,128)(2,1)}, u32[]{:S(2)}, u32[]{:S(2)}) collective-permute-start(bf16[144,256]{1,0:T(8,128)(2,1)} %get-tuple-element.10.refs_0_), channel_id=1, source_target_pairs={{0,64},{32,96},{64,0},{96,32},{1,65},{33,97},{65,1},{97,33},{2,66}... | collective-permute-start | bytes 221192 | tf_op jit(solution)/shard_map/ppermute | solution.py:222
  169.7 4.3 %collective-permute-start.6 = (bf16[144,256]{1,0:T(8,128)(2,1)}, bf16[144,256]{1,0:T(8,128)(2,1)}, u32[]{:S(2)}, u32[]{:S(2)}) collective-permute-start(bf16[144,256]{1,0:T(8,128)(2,1)} %get-tuple-element.10.refs_0_), channel_id=1, source_target_pairs={{0,96},{32,0},{64,32},{96,64},{1,97},{33,1},{65,33},{97,65},{2,98}... | collective-permute-start | bytes 221192 | tf_op jit(solution)/shard_map/ppermute | solution.py:222
  176.0 3.5 %collective-permute-start.7 = (bf16[128,256]{1,0:T(8,128)(2,1)}, bf16[128,256]{1,0:T(8,128)(2,1)}, u32[]{:S(2)}, u32[]{:S(2)}) collective-permute-start(bf16[128,256]{1,0:T(8,128)(2,1)} %get-tuple-element.13), channel_id=1, source_target_pairs={{0,4},{4,0},{1,5},{5,1},{2,6},{6,2},{3,7},{7,3},{8,12},{12,8},{9,1... | collective-permute-start | bytes 196616 | tf_op jit(solution)/shard_map/ppermute | solution.py:222
  194.4 13.4 %collective-permute-start.10 = (bf16[512,512]{1,0:T(8,128)(2,1)S(1)}, bf16[512,512]{1,0:T(8,128)(2,1)S(1)}, u32[]{:S(2)}, u32[]{:S(2)}) collective-permute-start(bf16[512,512]{1,0:T(8,128)(2,1)S(1)} %get-tuple-element.14), channel_id=1, source_target_pairs={{0,3},{1,0},{2,1},{3,2},{4,7},{5,4},{6,5},{7,6},{8,11},{9,8},{10,9... | collective-permute-start | bytes 1572872 | tf_op jit(solution)/shard_map/ppermute | solution.py:222
  196.8 14.1 %collective-permute-start.8 = (bf16[512,512]{1,0:T(8,128)(2,1)S(1)}, bf16[512,512]{1,0:T(8,128)(2,1)S(1)}, u32[]{:S(2)}, u32[]{:S(2)}) collective-permute-start(bf16[512,512]{1,0:T(8,128)(2,1)S(1)} %get-tuple-element.16), channel_id=1, source_target_pairs={{0,1},{1,2},{2,3},{3,0},{4,5},{5,6},{6,7},{7,4},{8,9},{9,10},{10,1... | collective-permute-start | bytes 1572872 | tf_op jit(solution)/shard_map/ppermute | solution.py:222
  197.9 25.2 %collective-permute-start.12 = (bf16[256,1024]{1,0:T(8,128)(2,1)S(1)}, bf16[256,1024]{1,0:T(8,128)(2,1)}, u32[]{:S(2)}, u32[]{:S(2)}) collective-permute-start(bf16[256,1024]{1,0:T(8,128)(2,1)S(1)} %slice.8), channel_id=1, source_target_pairs={{0,1},{1,2},{2,3},{3,0},{4,5},{5,6},{6,7},{7,4},{8,9},{9,10},{10,1... | collective-permute-start | bytes 1572872 | tf_op jit(solution)/shard_map/ppermute | solution.py:222
  199.4 35.5 %collective-permute-start.14 = (bf16[256,1024]{1,0:T(8,128)(2,1)S(1)}, bf16[256,1024]{1,0:T(8,128)(2,1)}, u32[]{:S(2)}, u32[]{:S(2)}) collective-permute-start(bf16[256,1024]{1,0:T(8,128)(2,1)S(1)} %slice.9), channel_id=1, source_target_pairs={{0,3},{1,0},{2,1},{3,2},{4,7},{5,4},{6,5},{7,6},{8,11},{9,8},{10,9... | collective-permute-start | bytes 1572872 | tf_op jit(solution)/shard_map/ppermute | solution.py:222
  202.0 40.3 %collective-permute-start.15 = (bf16[512,1024]{1,0:T(8,128)(2,1)}, bf16[512,1024]{1,0:T(8,128)(2,1)}, u32[]{:S(2)}, u32[]{:S(2)}) collective-permute-start(bf16[512,1024]{1,0:T(8,128)(2,1)} %collective-permute-done.11.refs_5_), channel_id=1, source_target_pairs={{0,4},{4,0},{1,5},{5,1},{2,6},{6,2},{3,7},{7,3},{8,12},{12,8},{9,1... | collective-permute-start | bytes 3145736 | tf_op jit(solution)/shard_map/ppermute | solution.py:222
  207.7 27.2 %copy-start.1 = (bf16[512,512]{1,0:T(8,128)(2,1)}, bf16[512,512]{1,0:T(8,128)(2,1)S(1)}, u32[]{:S(2)}) copy-start(bf16[512,512]{1,0:T(8,128)(2,1)S(1)} %collective-permute-done.10.refs_3_) | copy-start | bytes 1572868
  207.7 34.6 %collective-permute-start.18 = (bf16[512,1024]{1,0:T(8,128)(2,1)}, bf16[512,1024]{1,0:T(8,128)(2,1)}, u32[]{:S(2)}, u32[]{:S(2)}) collective-permute-start(bf16[512,1024]{1,0:T(8,128)(2,1)} %collective-permute-done.13.refs_8_), channel_id=1, source_target_pairs={{0,4},{4,0},{1,5},{5,1},{2,6},{6,2},{3,7},{7,3},{8,12},{12,8},{9,1... | collective-permute-start | bytes 3145736 | tf_op jit(solution)/shard_map/ppermute | solution.py:222
  210.9 24.2 %copy-start.2 = (bf16[512,512]{1,0:T(8,128)(2,1)}, bf16[512,512]{1,0:T(8,128)(2,1)S(1)}, u32[]{:S(2)}) copy-start(bf16[512,512]{1,0:T(8,128)(2,1)S(1)} %collective-permute-done.8.refs_1_) | copy-start | bytes 1572868
  210.9 31.4 %collective-permute-start.9 = (bf16[512,512]{1,0:T(8,128)(2,1)}, bf16[512,512]{1,0:T(8,128)(2,1)}, u32[]{:S(2)}, u32[]{:S(2)}) collective-permute-start(bf16[512,512]{1,0:T(8,128)(2,1)} %get-tuple-element.15), channel_id=1, source_target_pairs={{0,2},{1,3},{2,0},{3,1},{4,6},{5,7},{6,4},{7,5},{8,10},{9,11},{10,... | collective-permute-start | bytes 1572872 | tf_op jit(solution)/shard_map/ppermute | solution.py:222
  223.1 19.2 %collective-permute-start.16 = (bf16[256,1024]{1,0:T(8,128)(2,1)}, bf16[256,1024]{1,0:T(8,128)(2,1)}, u32[]{:S(2)}, u32[]{:S(2)}) collective-permute-start(bf16[256,1024]{1,0:T(8,128)(2,1)} %collective-permute-done.12.refs_6_), channel_id=1, source_target_pairs={{0,4},{4,0},{1,5},{5,1},{2,6},{6,2},{3,7},{7,3},{8,12},{12,8},{9,1... | collective-permute-start | bytes 1572872 | tf_op jit(solution)/shard_map/ppermute | solution.py:222
  234.9 7.4 %collective-permute-start.17 = (bf16[256,1024]{1,0:T(8,128)(2,1)}, bf16[256,1024]{1,0:T(8,128)(2,1)}, u32[]{:S(2)}, u32[]{:S(2)}) collective-permute-start(bf16[256,1024]{1,0:T(8,128)(2,1)} %collective-permute-done.14.refs_7_), channel_id=1, source_target_pairs={{0,4},{4,0},{1,5},{5,1},{2,6},{6,2},{3,7},{7,3},{8,12},{12,8},{9,1... | collective-permute-start | bytes 1572872 | tf_op jit(solution)/shard_map/ppermute | solution.py:222
